TPU v7x, 256 devices: a whole 4x4x8 slice. The times are simulated.
256 devices in a mesh: sp: 64 (over z, x, core), tp: 4 (over y).
Axes of the slice: x: 4, y: 4, z: 8, core: 2. Of those that a mesh axis runs over, the one named last changes fastest.
Arguments:
- incoming_residual_stream: bfloat16 [32768, 2048], P(('sp', 'tp')), may hold values from -6 to 6
- result_valve: bfloat16 [32768, 2048], P('sp', 'tp'), may hold values from -6 to 6
- channel_feed_matrix: bfloat16 [32768, 2048], P('sp', 'tp'), may hold values from -6 to 6
- memory_feed_matrix: bfloat16 [32768, 512], P('sp', 'tp'), may hold values from -6 to 6
- memory_query_matrix: bfloat16 [32768, 512], P('sp', 'tp'), may hold values from -6 to 6
- unsoftened_deltas: float32 [32768, 32], P('sp', 'tp'), may hold values from -2.7 to 2.7
- delta_offset: float32 [32], P('tp'), may hold values from -4.5 to -3.5
- channel_fading_speed: float32 [32], P('tp'), as said below
- extra_log_fading: float32 [32768, 32], P('sp', 'tp'), may hold values from -0.7 to 0
- bypass_factor: float32 [32], P('tp'), may hold values from 0.1 to 1.9
- channel_feed_kernel: bfloat16 [4, 2048], P(None, 'tp'), may hold values from -3 to 3
- memory_feed_kernel: bfloat16 [4, 512], P(None, 'tp'), may hold values from -3 to 3
- memory_query_kernel: bfloat16 [4, 512], P(None, 'tp'), may hold values from -3 to 3
- cluster_scaling_vector: float32 [2048], P('tp'), may hold values from 0.1 to 1.9
- mixer_result_matrix: bfloat16 [2048, 2048], P('tp'), may hold values from -0.125 to 0.125
- initial_scaling_vector: float32 [2048], replicated, may hold values from 0.1 to 1.9
- valve_matrix: bfloat16 [2048, 5632], P('sp', 'tp'), may hold values from -0.125 to 0.125
- widen_matrix: bfloat16 [2048, 5632], P('sp', 'tp'), may hold values from -0.125 to 0.125
- shrink_matrix: bfloat16 [5632, 2048], P('tp', 'sp'), may hold values from -0.078125 to 0.078125
- valve_filter_kernel: bfloat16 [3, 5632], P(None, 'tp'), may hold values from -3.5 to 3.5
- widen_filter_kernel: bfloat16 [3, 5632], P(None, 'tp'), may hold values from -3.5 to 3.5
- latter_scaling_vector: float32 [2048], replicated, may hold values from 0.1 to 1.9
Outputs:
- layer_out: bfloat16 [32768, 2048], P(('sp', 'tp'))
Inputs may be any that keep to these rules, and one draw needn't show every extreme that they name: `channel_fading_speed`: positive.
All inputs are finite; a program needn't handle non-finite values.
Results may differ from a plain program's by a relative error of at most 0.02.
Values may be sent and summed in bfloat16 or wider, within the bound.
No kernel may reach another device: no remote copies, remote signals or barrier semaphores. Data moves between devices by JAX's collectives and lax.ppermute only.
A program may use at most 128 MiB of HBM per device.

v0:
```python
import jax
import jax.numpy as jnp
from jax import lax
from jax.experimental import pallas as pl
from jax.experimental.pallas import tpu as pltpu
from jax.sharding import Mesh
from jax.sharding import PartitionSpec as P

HEAD_DIM = 64
STATE = 128
CONV = 4
FCONV = 3
BLOCK = 128
SP = ("sp_0", "sp_1", "sp_2")
SP_TP = ("sp_0", "sp_1", "sp_2", "tp")

EPSILON = 1e-05
ALPHA = 2.0**0.25
F32 = jnp.float32
BF16 = jnp.bfloat16
NEG = -1e30

ROWS = 512
CH = 512
NH = 8
QUARTER = 128
HALFCH = 256
D = 2048
HALF = 1024
FFL = 1408

VMEM = pl.BlockSpec(memory_space=pltpu.VMEM)
SMEM = pl.BlockSpec(memory_space=pltpu.SMEM)
ANY = pl.BlockSpec(memory_space=pl.ANY)
HIGHEST = lax.Precision.HIGHEST
MIB = 1024 * 1024


def limit(mib):
    return pltpu.CompilerParams(vmem_limit_bytes=mib * MIB)


def close(value):
    return pltpu.with_memory_space_constraint(value, pltpu.VMEM)


def close_out(shape, kind):
    return pltpu.VMEM(shape, kind)


def away(*values):
    return tuple(pltpu.with_memory_space_constraint(value, pltpu.HBM) for value in values)


def away_out(shape, kind):
    return pltpu.HBM(shape, kind)


def dot(a, b):
    return jnp.dot(a, b, preferred_element_type=F32)


def dot_nt(a, b, precision=None):
    return lax.dot_general(
        a, b, (((1,), (1,)), ((), ())), precision=precision, preferred_element_type=F32
    )


def silu(v):
    return v / (1.0 + jnp.exp(-v))


def lane_pairs(column_of, rows):
    low = lax.broadcasted_iota(jnp.int32, (rows, 128), 1) < HEAD_DIM
    slabs = []
    for q in range(NH // 2):
        first = jnp.broadcast_to(column_of[:, 2 * q : 2 * q + 1], (rows, 128))
        second = jnp.broadcast_to(column_of[:, 2 * q + 1 : 2 * q + 2], (rows, 128))
        slabs.append(jnp.where(low, first, second))
    return slabs


def eye(n):
    line = lax.broadcasted_iota(jnp.int32, (n, n), 0)
    lane = lax.broadcasted_iota(jnp.int32, (n, n), 1)
    return jnp.where(line == lane, 1.0, 0.0).astype(F32)


def columns(rows):
    return dot_nt(eye(BLOCK), rows, precision=HIGHEST)


def down_column(ref):
    return jnp.sum(eye(NH) * ref[...], axis=1, keepdims=True)


def decays(delta, extra, offset, speed):
    step_in = delta + offset
    step = jnp.maximum(step_in, 0.0) + jnp.log1p(jnp.exp(-jnp.abs(step_in)))
    return step, extra - speed * step


def running_sum(fading):
    line = lax.broadcasted_iota(jnp.int32, (BLOCK, BLOCK), 0)
    lane = lax.broadcasted_iota(jnp.int32, (BLOCK, BLOCK), 1)
    upper = jnp.where(line <= lane, 1.0, 0.0).astype(F32)
    return jnp.dot(fading, upper, precision=HIGHEST, preferred_element_type=F32)


def conv_at(pad, taps, start):
    total = None
    for k in range(CONV):
        term = taps[k : k + 1, :].astype(F32) * pad[pl.ds(start + 8 - CONV + 1 + k, BLOCK), :]
        total = term if total is None else total + term
    return silu(total)


def conv_next(pad, taps, block):
    pad[8 : 8 + BLOCK, :] = block.astype(F32)
    total = None
    for k in range(CONV):
        term = taps[k : k + 1, :].astype(F32) * pad[pl.ds(8 - CONV + 1 + k, BLOCK), :]
        total = term if total is None else total + term
    pad[0:8, :] = pad[BLOCK : BLOCK + 8, :]
    return silu(total)


def rim_kernel(x_ref, b_ref, c_ref, out_ref):
    out_ref[:, 0:CH] = x_ref[...]
    out_ref[:, CH : CH + STATE] = b_ref[...]
    out_ref[:, CH + STATE : CH + 2 * STATE] = c_ref[...]


def run_rim(x, b, c):
    last = lambda width: pl.BlockSpec((8, width), lambda i: (ROWS // 8 - 1, 0))
    return pl.pallas_call(
        rim_kernel,
        grid=(1,),
        out_shape=close_out((8, CH + 2 * STATE), BF16),
        in_specs=[last(CH), last(STATE), last(STATE)],
        out_specs=pl.BlockSpec((8, CH + 2 * STATE), lambda i: (0, 0)),
        name="rim",
    )(*away(x, b, c))


def state_kernel(
    x_ref, b_ref, rim_ref, xt_ref, bt_ref, delta_ref, extra_ref, offset_ref, speed_ref,
    x_out, b_out, state_out, msg_ref,
    xpad, bpad,
):
    xpad[0:8, :] = rim_ref[:, 0:CH].astype(F32)
    bpad[0:8, :] = rim_ref[:, CH : CH + STATE].astype(F32)
    xpad[8 : 8 + ROWS, :] = x_ref[...].astype(F32)
    bpad[8 : 8 + ROWS, :] = b_ref[...].astype(F32)
    step, fading = decays(
        delta_ref[...], extra_ref[...], down_column(offset_ref), down_column(speed_ref)
    )
    state = [jnp.zeros((STATE, 128), F32) for _ in range(NH // 2)]
    base = jnp.zeros((NH, 1), F32)
    for i in range(ROWS // BLOCK):
        start = i * BLOCK
        rows = pl.ds(start, BLOCK)
        here = slice(start, start + BLOCK)
        cum = running_sum(fading[:, here])
        last = cum[:, BLOCK - 1 : BLOCK]
        to_end = lane_pairs(columns(step[:, here] * jnp.exp(last - cum)), BLOCK)
        kept = lane_pairs(columns(jnp.broadcast_to(jnp.exp(last), (NH, BLOCK)))[0:1, :], 1)
        x_act = conv_at(xpad, xt_ref, start).astype(BF16)
        b_act = conv_at(bpad, bt_ref, start).astype(BF16)
        x_out[rows, :] = x_act
        b_out[rows, :] = b_act
        b_turned = b_act.astype(F32).T.astype(BF16)
        for q in range(NH // 2):
            cols = slice(q * 128, (q + 1) * 128)
            fresh = dot(b_turned, (x_act[:, cols].astype(F32) * to_end[q]).astype(BF16))
            state[q] = fresh if i == 0 else state[q] * kept[q] + fresh
            if i < ROWS // BLOCK - 1:
                state_out[i, :, cols] = state[q].astype(BF16)
        base = base + last
    totals = lane_pairs(columns(jnp.broadcast_to(base, (NH, BLOCK)))[0:1, :], 1)
    for q in range(NH // 2):
        block = slice(q * 16, (q + 1) * 16)
        msg_ref[block, 0:8, :] = state[q].reshape(16, 8, 128).astype(BF16)
        left = totals[q]
        parts = []
        for _ in range(3):
            part = left.astype(BF16)
            parts.append(part.astype(F32))
            left = left - part.astype(F32)
        line = lax.broadcasted_iota(jnp.int32, (8, 128), 0)
        packed = jnp.where(line == 0, parts[0], jnp.where(line == 1, parts[1], parts[2]))
        packed = jnp.where(line < 3, packed, 0.0).astype(BF16)
        msg_ref[block, 8:16, :] = jnp.broadcast_to(packed[None], (16, 8, 128))


def run_state(x, b, rim, xt, bt, delta, extra, offset, speed):
    return pl.pallas_call(
        state_kernel,
        out_shape=(
            away_out((ROWS, CH), BF16),
            away_out((ROWS, STATE), BF16),
            away_out((ROWS // BLOCK - 1, STATE, CH), BF16),
            close_out((64, 16, 128), BF16),
        ),
        compiler_params=limit(24),
        in_specs=[VMEM] * 9,
        out_specs=(VMEM,) * 4,
        scratch_shapes=[
            pltpu.VMEM((ROWS + 8, CH), F32),
            pltpu.VMEM((ROWS + 8, STATE), F32),
        ],
        name="local_state",
    )(*away(x, b), close(rim), *away(xt, bt, delta, extra, offset, speed))


def local_kernel(
    x_ref, b_ref, state_ref, c_ref, rim_ref, ct_ref, delta_ref, extra_ref, offset_ref, speed_ref,
    bypass_ref,
    y_ref, cact_ref, grow_ref,
    cpad,
):
    cpad[0:8, :] = rim_ref[:, CH + STATE : CH + 2 * STATE].astype(F32)
    offset = down_column(offset_ref)
    speed = down_column(speed_ref)
    bypass = lane_pairs(bypass_ref[...], 1)
    row = lax.broadcasted_iota(jnp.int32, (BLOCK, BLOCK), 0)
    col = lax.broadcasted_iota(jnp.int32, (BLOCK, BLOCK), 1)
    causal = row >= col
    low = col < HEAD_DIM

    def block_step(i, base):
        rows = pl.ds(pl.multiple_of(i * BLOCK, BLOCK), BLOCK)
        step, fading = decays(delta_ref[:, rows], extra_ref[:, rows], offset, speed)
        cum = running_sum(fading)
        turned = columns(jnp.concatenate([cum, jnp.exp(cum), jnp.exp(base + cum)], axis=0))
        grow_ref[rows, :] = turned[:, 2 * NH : 3 * NH]
        grown = lane_pairs(turned[:, NH : 2 * NH], BLOCK)
        c_act = conv_next(cpad, ct_ref, c_ref[rows, :]).astype(BF16)
        cact_ref[rows, :] = c_act
        affinity = dot_nt(c_act, b_ref[rows, :])
        for q in range(NH // 2):
            cols = slice(q * 128, (q + 1) * 128)
            x_here = x_ref[rows, cols]
            within = []
            for h in (2 * q, 2 * q + 1):
                between = turned[:, h : h + 1] - cum[h : h + 1, :]
                lag = jnp.exp(jnp.where(causal, between, NEG)) * step[h : h + 1, :]
                within.append(dot((affinity * lag).astype(BF16), x_here))
            total = jnp.where(low, within[0], within[1]) + bypass[q] * x_here.astype(F32)
            carried = dot(c_act, state_ref[jnp.maximum(i - 1, 0), :, cols]) * grown[q]
            y_ref[rows, cols] = total + jnp.where(i > 0, carried, 0.0)
        return base + cum[:, BLOCK - 1 : BLOCK]

    lax.fori_loop(0, ROWS // BLOCK, block_step, jnp.zeros((NH, 1), F32))


def run_local(x, b, states, c, rim, ct, delta, extra, offset, speed, bypass):
    return pl.pallas_call(
        local_kernel,
        out_shape=(
            away_out((ROWS, CH), F32),
            away_out((ROWS, STATE), BF16),
            away_out((ROWS, NH), F32),
        ),
        compiler_params=limit(24),
        in_specs=[VMEM] * 11,
        out_specs=(VMEM,) * 3,
        scratch_shapes=[pltpu.VMEM((BLOCK + 8, STATE), F32)],
        name="local_mixer",
    )(*away(x, b, states, c), close(rim), *away(ct, delta, extra, offset, speed, bypass))


def prefix_kernel(in_ref, out_ref):
    entering = jnp.zeros((8, 128), F32)
    for j in range(64):
        out_ref[j] = entering.astype(BF16)
        piece = in_ref[j].astype(F32)
        total = piece[8:9, :] + piece[9:10, :] + piece[10:11, :]
        entering = entering * jnp.exp(total) + piece[0:8, :]


def run_prefix(received):
    return pl.pallas_call(
        prefix_kernel,
        out_shape=close_out((64, 8, 128), BF16),
        compiler_params=limit(8),
        in_specs=[VMEM],
        out_specs=VMEM,
        name="state_prefix",
    )(close(received))


def gate_kernel(y_ref, cact_ref, grow_ref, in_ref, valve_ref, scale_ref, out_l, out_r, tail_ref):
    for i in range(ROWS // BLOCK):
        rows = pl.ds(i * BLOCK, BLOCK)
        grown = lane_pairs(grow_ref[rows, :], BLOCK)
        c_act = cact_ref[rows, :]
        gated = []
        square = jnp.zeros((BLOCK, 1), F32)
        for q in range(NH // 2):
            cols = slice(q * 128, (q + 1) * 128)
            entering = in_ref[q * 16 : (q + 1) * 16].astype(F32).reshape(STATE, 128).astype(BF16)
            y = y_ref[rows, cols] + dot(c_act, entering) * grown[q]
            y = y * silu(valve_ref[rows, cols].astype(F32))
            gated.append(y)
            square = square + jnp.sum(y * y, axis=-1, keepdims=True)
        factor = lax.rsqrt(square * (1.0 / CH) + EPSILON)
        for q in range(NH // 2):
            cols = slice(q * 128, (q + 1) * 128)
            half = (out_l, out_r)[q // 2]
            done = (gated[q] * factor * scale_ref[0:1, cols]).astype(BF16)
            half[rows, (q % 2) * 128 : (q % 2 + 1) * 128] = done
            if i == ROWS // BLOCK - 1:
                tail_ref[:, cols] = done[BLOCK - RIM :, :]


def run_gate(y, cact, grow, entering, valve, scale):
    return pl.pallas_call(
        gate_kernel,
        out_shape=(
            away_out((ROWS, HALFCH), BF16),
            away_out((ROWS, HALFCH), BF16),
            away_out((RIM, CH), BF16),
        ),
        compiler_params=limit(16),
        in_specs=[VMEM] * 6,
        out_specs=(VMEM,) * 3,
        name="gate_norm",
    )(*away(y, cact, grow), close(entering), *away(valve, scale))


RIM = 16
CHUNK = 512


def project_kernel(
    place_ref, scale_ref, near_l, far_r, across_l, across_r,
    own_l, own_r, near_r, far_l, own_t, near_t, far_t, across_t, res_t, own_w, near_w, far_w, across_w, other_w,
    own_res, near_res, far_res, across_res,
    out_ref,
    weight, early, tails, tail_res, res, total, w_sems, e_sems, t_sems, r_sems,
):
    core = place_ref[4]
    columns_of = (
        pl.ds(pl.multiple_of(core * HALF, HALF), HALF),
        pl.ds(pl.multiple_of((1 - core) * HALF, HALF), HALF),
    )
    others = [other_w.at[k * CH : (k + 1) * CH, :] for k in range(3)]
    arrived = ((near_w, far_w, across_w), others)
    copies = ([], [])
    for half in range(2):
        sources = (own_w.at[:, columns_of[half]], *arrived[half])
        for k, source in enumerate(sources):
            target = weight.at[half, k * CH : (k + 1) * CH, :]
            copies[half].append(pltpu.make_async_copy(source, target, w_sems.at[half, k]))
    res_copies = []
    for k, source in enumerate((own_res, near_res, far_res, across_res)):
        rows = pl.ds(pl.multiple_of(place_ref[k] * QUARTER, QUARTER), QUARTER)
        res_copies.append(pltpu.make_async_copy(source, res.at[rows, :], r_sems.at[k]))
    early_copies = [
        pltpu.make_async_copy(source, early.at[k], e_sems.at[k])
        for k, source in enumerate((own_l, own_r, near_r, far_l))
    ]
    early_copies += [
        pltpu.make_async_copy(source, tails.at[k], t_sems.at[k])
        for k, source in enumerate((own_t, near_t, far_t, across_t))
    ]
    early_copies.append(pltpu.make_async_copy(res_t, tail_res, t_sems.at[4]))
    acts = (early.at[0], early.at[1], near_l, early.at[2], early.at[3], far_r, across_l, across_r)
    for copy in early_copies + copies[0]:
        copy.start()
    for copy in early_copies + copies[0]:
        copy.wait()
    for copy in copies[1] + res_copies:
        copy.start()
    for half in range(2):
        if half == 1:
            for copy in copies[1]:
                copy.wait()
        for n in range(HALF // CHUNK):
            cols = slice(n * CHUNK, (n + 1) * CHUNK)
            part = None
            for k, act in enumerate(acts):
                side = slice((k % 2) * HALFCH, (k % 2 + 1) * HALFCH)
                lhs = jnp.concatenate([tails[k // 2, :, side], act[...]], axis=0)
                term = dot(lhs, weight[half, k * HALFCH : (k + 1) * HALFCH, cols])
                part = term if part is None else part + term
            start = pl.multiple_of((core if half == 0 else 1 - core) * HALF + n * CHUNK, CHUNK)
            total[:, pl.ds(start, CHUNK)] = part
    for copy in res_copies:
        copy.wait()

    def norm(values):
        centred = values - jnp.sum(values, axis=-1, keepdims=True) * (1.0 / D)
        spread = jnp.sum(centred * centred, axis=-1, keepdims=True) * (1.0 / D)
        return (centred * lax.rsqrt(spread + EPSILON) * scale_ref[...]).astype(BF16)

    out_ref[0:RIM, :] = norm(total[0:RIM, :] + ALPHA * tail_res[...].astype(F32))

    def norm_rows(i, carry):
        rows = pl.ds(pl.multiple_of(i * 64, 64), 64)
        shifted = pl.ds(pl.multiple_of(RIM + i * 64, 16), 64)
        out_ref[shifted, :] = norm(total[shifted, :] + ALPHA * res[rows, :].astype(F32))
        return carry

    lax.fori_loop(0, ROWS // 64, norm_rows, 0)


def run_project(place, scale, weights, acts, tails, residuals):
    return pl.pallas_call(
        project_kernel,
        out_shape=close_out((RIM + ROWS, D), BF16),
        in_specs=[SMEM] + [VMEM] * 5 + [ANY] * 18,
        out_specs=VMEM,
        scratch_shapes=[
            pltpu.VMEM((2, D, HALF), BF16),
            pltpu.VMEM((4, ROWS, HALFCH), BF16),
            pltpu.VMEM((4, RIM, CH), BF16),
            pltpu.VMEM((RIM, D), BF16),
            pltpu.VMEM((ROWS, D), BF16),
            pltpu.VMEM((RIM + ROWS, D), F32),
            pltpu.SemaphoreType.DMA((2, 4)),
            pltpu.SemaphoreType.DMA((4,)),
            pltpu.SemaphoreType.DMA((5,)),
            pltpu.SemaphoreType.DMA((4,)),
        ],
        compiler_params=limit(30),
        name="project_norm",
    )(
        place,
        *away(scale),
        *[close(acts[k]) for k in (2, 5, 6, 7)],
        *away(*[acts[k] for k in (0, 1, 3, 4)], *tails, *weights, *residuals),
    )


TILES = FFL // 128
NARROW = 512


def down_copies(w_ref, down, sems):
    return [
        pltpu.make_async_copy(
            w_ref.at[n * NARROW : (n + 1) * NARROW, 2 * FFL : 3 * FFL],
            down.at[n * NARROW : (n + 1) * NARROW, :],
            sems.at[n],
        )
        for n in range(D // NARROW)
    ]


def two_quarters(hid, place_ref, half):
    def rows_of(k):
        return hid[pl.ds(pl.multiple_of(place_ref[half, k] * QUARTER, QUARTER), QUARTER), :]

    return jnp.concatenate([rows_of(0), rows_of(1)], axis=0)


AHEAD = 4
STRIP = 512


def widen_kernel(
    sent_ref, gate_t, up_t, rows, w_ref,
    hid, down, send_l, send_r,
    wide, gate_pad, up_pad, wide_sems, down_sems,
):
    def wide_copies(j):
        at = j * 128
        if not isinstance(j, int):
            at = pl.multiple_of(at, 128)
        return (
            pltpu.make_async_copy(
                w_ref.at[:, pl.ds(at, 128)], wide.at[j, :, 0:128], wide_sems.at[j, 0]
            ),
            pltpu.make_async_copy(
                w_ref.at[:, pl.ds(FFL + at, 128)], wide.at[j, :, 128:256], wide_sems.at[j, 1]
            ),
        )

    downs = down_copies(w_ref, down, down_sems)
    for j in range(AHEAD):
        for copy in wide_copies(j):
            copy.start()

    def conv(pad, taps, at):
        total = None
        for k in range(FCONV):
            tap = taps[k : k + 1, pl.ds(at, 128)].astype(F32)
            term = tap * pad[pl.ds(RIM - FCONV + 1 + k, ROWS), :]
            total = term if total is None else total + term
        return total

    def tile(j, carry):
        for copy in wide_copies(j):
            copy.wait()

        @pl.when(j + AHEAD < TILES)
        def _():
            for copy in wide_copies(j + AHEAD):
                copy.start()

        @pl.when(j + AHEAD == TILES)
        def _():
            for copy in downs:
                copy.start()

        at = pl.multiple_of(j * 128, 128)
        both = dot(rows[...], wide[j]).astype(BF16).astype(F32)
        gate_pad[...] = both[:, 0:128]
        up_pad[...] = both[:, 128:256]
        hid[:, pl.ds(at, 128)] = (
            silu(conv(gate_pad, gate_t, at)) * conv(up_pad, up_t, at)
        ).astype(BF16)
        return carry

    lax.fori_loop(0, TILES, tile, 0)
    for copy in downs:
        copy.wait()
    send_l[...] = dot_nt(two_quarters(hid, sent_ref, 0), down[0:STRIP, :]).astype(BF16)
    send_r[...] = dot_nt(two_quarters(hid, sent_ref, 1), down[HALF : HALF + STRIP, :]).astype(BF16)


def run_widen(sent, rows, weights, gate_t, up_t):
    return pl.pallas_call(
        widen_kernel,
        out_shape=(
            close_out((ROWS, FFL), BF16),
            close_out((D, FFL), BF16),
            close_out((2 * QUARTER, STRIP), BF16),
            close_out((2 * QUARTER, STRIP), BF16),
        ),
        in_specs=[SMEM, VMEM, VMEM, VMEM, ANY],
        out_specs=(VMEM,) * 4,
        scratch_shapes=[
            pltpu.VMEM((TILES, D, 256), BF16),
            pltpu.VMEM((ROWS + RIM, 128), F32),
            pltpu.VMEM((ROWS + RIM, 128), F32),
            pltpu.SemaphoreType.DMA((TILES, 2)),
            pltpu.SemaphoreType.DMA((D // NARROW,)),
        ],
        compiler_params=limit(24),
        name="widen",
    )(sent, *away(gate_t, up_t), close(rows), *away(weights))


def sent_kernel(sent_ref, hid, down, send_l, send_r):
    send_l[...] = dot_nt(two_quarters(hid, sent_ref, 0), down[STRIP:HALF, :]).astype(BF16)
    send_r[...] = dot_nt(two_quarters(hid, sent_ref, 1), down[HALF + STRIP : D, :]).astype(BF16)


def run_sent(sent, hidden, down):
    return pl.pallas_call(
        sent_kernel,
        out_shape=(close_out((2 * QUARTER, STRIP), BF16),) * 2,
        in_specs=[SMEM, VMEM, VMEM],
        out_specs=(VMEM,) * 2,
        compiler_params=limit(8),
        name="shrink_sent",
    )(sent, close(hidden), close(down))


def held_kernel(held_ref, hid, down, own, pass_1, pass_2):
    for half in range(2):
        both = dot_nt(two_quarters(hid, held_ref, half), down[half * HALF : (half + 1) * HALF, :])
        own[:, half * HALF : (half + 1) * HALF] = both[0:QUARTER, :]
        pass_1[:, half * STRIP : (half + 1) * STRIP] = both[QUARTER:, 0:STRIP]
        pass_2[:, half * STRIP : (half + 1) * STRIP] = both[QUARTER:, STRIP:HALF]


def run_held(held, hidden, down):
    return pl.pallas_call(
        held_kernel,
        out_shape=(
            close_out((QUARTER, D), F32),
            close_out((QUARTER, HALF), F32),
            close_out((QUARTER, HALF), F32),
        ),
        in_specs=[SMEM, VMEM, VMEM],
        out_specs=(VMEM,) * 3,
        compiler_params=limit(8),
        name="shrink_held",
    )(held, close(hidden), close(down))


def add_kernel(passed, once_l, once_r, out_l, out_r):
    out_l[...] = (passed[:, 0:STRIP] + once_l[QUARTER:, :].astype(F32)).astype(BF16)
    out_r[...] = (passed[:, STRIP:] + once_r[QUARTER:, :].astype(F32)).astype(BF16)


def run_add(passed, once_l, once_r):
    return pl.pallas_call(
        add_kernel,
        out_shape=(close_out((QUARTER, STRIP), BF16),) * 2,
        in_specs=[VMEM] * 3,
        out_specs=(VMEM,) * 2,
        compiler_params=limit(8),
        name="round_sum",
    )(close(passed), close(once_l), close(once_r))


def last_norm_kernel(place_ref, own, l_1, r_1, l_2, r_2, ll_1, rr_1, ll_2, rr_2, res_ref, scale_ref, out_ref):
    for i in range(2):
        rows = slice(i * 64, (i + 1) * 64)
        kept = pl.ds(pl.multiple_of(RIM + place_ref[0] * QUARTER + i * 64, 16), 64)
        parts = []
        for k, (once, twice) in enumerate(((l_1, ll_1), (l_2, ll_2), (r_1, rr_1), (r_2, rr_2))):
            cols = slice(k * STRIP, (k + 1) * STRIP)
            part = own[rows, cols] + once[rows, :].astype(F32) + twice[rows, :].astype(F32)
            parts.append(part + ALPHA * res_ref[kept, cols].astype(F32))
        values = jnp.concatenate(parts, axis=1)
        centred = values - jnp.sum(values, axis=-1, keepdims=True) * (1.0 / D)
        spread = jnp.sum(centred * centred, axis=-1, keepdims=True) * (1.0 / D)
        out_ref[rows, :] = (centred * lax.rsqrt(spread + EPSILON) * scale_ref[...]).astype(BF16)


def run_last_norm(place, own, onces, twices, rows, scale):
    kept = [close(part) for part in (own, *onces, *twices, rows)]
    return pl.pallas_call(
        last_norm_kernel,
        out_shape=jax.ShapeDtypeStruct((QUARTER, D), BF16),
        in_specs=[SMEM] + [VMEM] * 11,
        out_specs=VMEM,
        compiler_params=limit(8),
        name="last_norm",
    )(place, *kept, *away(scale))


NEAR = [(0, 1), (1, 0), (2, 3), (3, 2)]
FAR = [(0, 3), (3, 0), (1, 2), (2, 1)]


def with_near(part):
    return lax.ppermute(part, "tp", NEAR)


def with_far(part):
    return lax.ppermute(part, "tp", FAR)


def forwarded(far_part, near_part):
    part = jnp.where(lax.axis_index("sp_2") == 0, far_part, near_part)
    pairs = [(i, j) for i, j in NEAR] + [(4 + i, 4 + j) for i, j in FAR]
    return lax.ppermute(part, ("sp_2", "tp"), pairs)


def with_core(part):
    return lax.ppermute(part, "sp_2", [(0, 1), (1, 0)])


def next_positions(shard):
    count = lax.axis_size(SP)
    return lax.ppermute(shard, SP, [(i, i + 1) for i in range(count - 1)])


def shards(
    incoming_residual_stream,
    result_valve,
    channel_feed_matrix,
    memory_feed_matrix,
    memory_query_matrix,
    unsoftened_deltas,
    delta_offset,
    channel_fading_speed,
    extra_log_fading,
    bypass_factor,
    channel_feed_kernel,
    memory_feed_kernel,
    memory_query_kernel,
    cluster_scaling_vector,
    mixer_result_matrix,
    initial_scaling_vector,
    valve_matrix,
    widen_matrix,
    shrink_matrix,
    valve_filter_kernel,
    widen_filter_kernel,
    latter_scaling_vector,
):
    own = lax.axis_index("tp").astype(jnp.int32)
    core = lax.axis_index("sp_2").astype(jnp.int32)
    near = own ^ 1
    far = 3 - own
    across = own ^ 2
    place = jnp.stack([own, near, far, across, core])
    sent = jnp.stack([jnp.stack([near, across]), jnp.stack([far, across])])
    held = jnp.stack([jnp.stack([own, far]), jnp.stack([own, near])])

    weights = lax.all_gather(
        jnp.concatenate([valve_matrix, widen_matrix, shrink_matrix.T], axis=1), SP, tiled=True
    )

    rim = run_rim(channel_feed_matrix, memory_feed_matrix, memory_query_matrix)
    _, projection, residual = lax.optimization_barrier(
        (rim, mixer_result_matrix, incoming_residual_stream)
    )
    rim = next_positions(rim)
    drives = (
        unsoftened_deltas.T,
        extra_log_fading.T,
        delta_offset.reshape(1, NH),
        channel_fading_speed.reshape(1, NH),
    )
    x_act, b_act, states, message = run_state(
        channel_feed_matrix,
        memory_feed_matrix,
        rim,
        channel_feed_kernel,
        memory_feed_kernel,
        *drives,
    )
    received = lax.all_to_all(message, SP, 0, 0, tiled=True)

    w_half = lax.dynamic_slice(projection, (0, core * HALF), (CH, HALF))
    w_near = with_near(w_half)
    w_far = with_far(w_half)
    res_near = with_near(residual)
    res_far = with_far(residual)

    y_local, c_act, grow = run_local(
        x_act,
        b_act,
        states,
        memory_query_matrix,
        rim,
        memory_query_kernel,
        *drives,
        bypass_factor.reshape(1, NH),
    )
    prefix = run_prefix(received)
    entering = lax.all_to_all(prefix, SP, 0, 0, tiled=True)
    late = lax.optimization_barrier((y_local, w_near, w_far, res_near, res_far))
    w_across = forwarded(late[2], late[1])
    res_across = forwarded(late[4], late[3])
    y_l, y_r, tail = run_gate(
        y_local, c_act, grow, entering, result_valve, cluster_scaling_vector.reshape(1, CH)
    )
    swap = lax.optimization_barrier((w_near, w_far, w_across, y_l))[:3]
    w_other = with_core(jnp.concatenate(swap, axis=0))
    tail_own = next_positions(tail)
    far_l = with_far(y_l)
    near_r = with_near(y_r)
    near_l = with_near(y_l)
    far_r = with_far(y_r)
    tail_near = with_near(tail_own)
    tail_far = with_far(tail_own)
    tail_across = forwarded(tail_far, tail_near)
    ends = [
        jnp.where(at == 3, part[QUARTER - RIM :], jnp.zeros((RIM, D), BF16))
        for at, part in ((own, residual), (near, res_near), (far, res_far), (across, res_across))
    ]
    res_tail = next_positions(ends[0] + ends[1] + ends[2] + ends[3])
    across_l = with_near(far_l)
    across_r = with_far(near_r)
    rows = run_project(
        place,
        initial_scaling_vector.reshape(1, D),
        (mixer_result_matrix, w_near, w_far, w_across, w_other),
        (y_l, y_r, near_l, near_r, far_l, far_r, across_l, across_r),
        (tail_own, tail_near, tail_far, tail_across, res_tail),
        (residual, res_near, res_far, res_across),
    )
    hidden, down, send_l1, send_r1 = run_widen(
        sent, rows, weights, valve_filter_kernel, widen_filter_kernel
    )
    l_1 = with_near(send_l1)
    r_1 = with_far(send_r1)
    send_l2, send_r2 = run_sent(sent, hidden, down)
    l_2 = with_near(send_l2)
    r_2 = with_far(send_r2)
    kept, pass_1, pass_2 = run_held(held, hidden, down)
    on_l1, on_r1 = run_add(pass_1, l_1, r_1)
    ll_1 = with_far(on_l1)
    rr_1 = with_near(on_r1)
    on_l2, on_r2 = run_add(pass_2, l_2, r_2)
    ll_2 = with_far(on_l2)
    rr_2 = with_near(on_r2)
    return run_last_norm(
        place,
        kept,
        (l_1, r_1, l_2, r_2),
        (ll_1, rr_1, ll_2, rr_2),
        rows,
        latter_scaling_vector.reshape(1, D),
    )


def solution(mesh):
    split = Mesh(mesh.devices.reshape(8, 4, 2, mesh.shape["tp"]), ("sp_0", "sp_1", "sp_2", "tp"))
    in_specs = (
        P(SP_TP, None),
        P(SP, "tp"),
        P(SP, "tp"),
        P(SP, "tp"),
        P(SP, "tp"),
        P(SP, "tp"),
        P("tp"),
        P("tp"),
        P(SP, "tp"),
        P("tp"),
        P(None, "tp"),
        P(None, "tp"),
        P(None, "tp"),
        P("tp"),
        P("tp", None),
        P(),
        P(SP, "tp"),
        P(SP, "tp"),
        P("tp", SP),
        P(None, "tp"),
        P(None, "tp"),
        P(),
    )
    out_specs = P(SP_TP, None)

    return jax.shard_map(
        shards, mesh=split, in_specs=in_specs, out_specs=out_specs, check_vma=False
    )
```

profile of v0, /device:TPU:32, one launch (start us, length us, event | category | flops | bytes accessed | tf_op | source)
XLA Modules:
  0.0 190.8 jit_solution(16548871123388964118)
XLA Ops:
  6.5 1.7 pad_maximum_fusion.1
  8.3 0.7 rim.1
  9.0 2.3 %constant_dynamic-slice_fusion = bf16[512,1024]{1,0:T(8,128)(2,1)} fusion(bf16[512,2048]{1,0:T(8,128)(2,1)} %own_w.1, s32[]{:T(128)S(6)} %select_n.63), kind=kLoop, calls=%fused_computation.17 | loop fusion | bytes 2097156 | tf_op jit(solution)/shard_map/dynamic_slice | solution.py:714
  11.3 1.6 collective-permute-start.13
  12.8 2.2 %collective-permute-start.14 = (bf16[512,1024]{1,0:T(8,128)(2,1)}, bf16[512,1024]{1,0:T(8,128)(2,1)S(1)}, u32[]{:S(2)}, u32[]{:S(2)}) collective-permute-start(bf16[512,1024]{1,0:T(8,128)(2,1)} %constant_dynamic-slice_fusion), channel_id=1, source_target_pairs={{0,3},{3,0},{1,2},{2,1},{4,7},{7,4},{5,6},{6,5},{8,11},{11,8},{9,1... | collective-permute-start | bytes 3145736 | tf_op jit(solution)/shard_map/ppermute | solution.py:638
  15.0 0.7 collective-permute-start.11
  15.7 0.6 collective-permute-start.12
  16.3 1.9 %collective-permute-start = (bf16[8,768]{1,0:T(8,128)(2,1)S(1)}, bf16[8,768]{1,0:T(8,128)(2,1)S(1)}, u32[]{:S(2)}, u32[]{:S(2)}) collective-permute-start(bf16[8,768]{1,0:T(8,128)(2,1)S(1)} %rim.1), channel_id=1, source_target_pairs={{0,4},{4,8},{8,12},{12,16},{16,20},{20,24},{24,28},{28,32},{32,36}... | collective-permute-start | bytes 36872 | tf_op jit(solution)/shard_map/ppermute | solution.py:653
  18.2 5.2 %collective-permute-done.rim_ref = bf16[8,768]{1,0:T(8,128)(2,1)S(1)} collective-permute-done((bf16[8,768]{1,0:T(8,128)(2,1)S(1)}, bf16[8,768]{1,0:T(8,128)(2,1)S(1)}, u32[]{:S(2)}, u32[]{:S(2)}) %collective-permute-start) | collective-permute-done | bytes 12320 | tf_op jit(solution)/shard_map/ppermute | solution.py:653
  23.4 5.6 %local_state.1 = (bf16[512,512]{1,0:T(8,128)(2,1)}, bf16[512,128]{1,0:T(8,128)(2,1)}, bf16[3,128,512]{2,1,0:T(8,128)(2,1)}, bf16[64,16,128]{2,1,0:T(8,128)(2,1)S(1)}) custom-call(bf16[512,512]{1,0:T(8,128)(2,1)} %x_ref.3, bf16[512,128]{1,0:T(8,128)(2,1)} %b_ref.3, bf16[8,768]{1,0:T(8,128)(2,1)S(1)} %collective-permute-done.rim_ref, bf16[4,512]{1,0:T(4,128)(2,1)} %xt_ref.1, ...), custom_call_target="tpu_custom_call" | custom-call | tf_op jit(solution)/shard_map/local_state/pallas_call | solution.py:197
  29.0 6.6 %local_mixer.1 = (f32[512,512]{1,0:T(8,128)}, bf16[512,128]{1,0:T(8,128)(2,1)}, f32[512,8]{1,0:T(8,128)}) custom-call(bf16[512,512]{1,0:T(8,128)(2,1)} %get-tuple-element.37.x_ref, bf16[512,128]{1,0:T(8,128)(2,1)} %get-tuple-element.38.b_ref, bf16[3,128,512]{2,1,0:T(8,128)(2,1)} %get-tuple-element.39.state_ref, bf16[512,128]{1,0:T(8,128)(2,1)} %c_ref.3, ...), custom_call_target="tpu_custom_call" | custom-call | tf_op jit(solution)/shard_map/local_mixer/pallas_call | solution.py:258
  35.7 11.9 %collective-permute-done.11.near_res = bf16[128,2048]{1,0:T(8,128)(2,1)S(1)} collective-permute-done((bf16[128,2048]{1,0:T(8,128)(2,1)}, bf16[128,2048]{1,0:T(8,128)(2,1)S(1)}, u32[]{:S(2)}, u32[]{:S(2)}) %collective-permute-start.11) | collective-permute-done | bytes 524320 | tf_op jit(solution)/shard_map/ppermute | solution.py:634
  47.6 2.5 %collective-permute-done.12.far_res = bf16[128,2048]{1,0:T(8,128)(2,1)S(1)} collective-permute-done((bf16[128,2048]{1,0:T(8,128)(2,1)}, bf16[128,2048]{1,0:T(8,128)(2,1)S(1)}, u32[]{:S(2)}, u32[]{:S(2)}) %collective-permute-start.12) | collective-permute-done | bytes 524320 | tf_op jit(solution)/shard_map/ppermute | solution.py:638
  50.1 0.1 broadcast_select_fusion
  50.3 0.1 collective-permute-start.17
  50.4 25.4 %all_to_all.10.in_ref = bf16[64,16,128]{2,1,0:T(8,128)(2,1)S(1)} all-to-all(bf16[64,16,128]{2,1,0:T(8,128)(2,1)S(1)} %get-tuple-element.43), channel_id=1, replica_groups=mesh['sp_0'=8,'sp_1'=4,'sp_2'=2,'tp'=4] {'sp_0','sp_1','sp_2'}, dimensions={0} | all-to-all | bytes 524288 | tf_op jit(solution)/shard_map/all_to_all | solution.py:712
  75.7 0.1 state_prefix.1
  75.9 17.6 %all_to_all.11.in_ref = bf16[64,8,128]{2,1,0:T(8,128)(2,1)S(1)} all-to-all(bf16[64,8,128]{2,1,0:T(8,128)(2,1)S(1)} %state_prefix.1), channel_id=1, replica_groups=mesh['sp_0'=8,'sp_1'=4,'sp_2'=2,'tp'=4] {'sp_0','sp_1','sp_2'}, dimensions={0} | all-to-all | bytes 262144 | tf_op jit(solution)/shard_map/all_to_all | solution.py:731
  93.5 3.6 %gate_norm.1 = (bf16[512,256]{1,0:T(8,128)(2,1)}, bf16[512,256]{1,0:T(8,128)(2,1)}, bf16[16,512]{1,0:T(8,128)(2,1)}) custom-call(f32[512,512]{1,0:T(8,128)} %get-tuple-element.40.y_ref, bf16[512,128]{1,0:T(8,128)(2,1)} %get-tuple-element.41.cact_ref, f32[512,8]{1,0:T(8,128)} %get-tuple-element.42.grow_ref, bf16[64,8,128]{2,1,0:T(8,128)(2,1)S(1)} %all_to_all.11.in_ref, ...), custom_call_target="tpu_custom_call" | custom-call | tf_op jit(solution)/shard_map/gate_norm/pallas_call | solution.py:318
  97.1 2.1 %pad_maximum_fusion = bf16[1536,1024]{1,0:T(8,128)(2,1)} fusion(bf16[512,1024]{1,0:T(8,128)(2,1)S(1)} %collective-permute-done.17.across_w, bf16[512,1024]{1,0:T(8,128)(2,1)S(1)} %collective-permute-done.14.far_w, bf16[512,1024]{1,0:T(8,128)(2,1)S(1)} %collective-permute-done.13.near_w), kind=kLoop, calls=%fused_computation | loop fusion | flops 9437184 | bytes 6291456 | tf_op jit(solution)/shard_map/concatenate | solution.py:739
  99.2 0.3 collective-permute-start.18
  99.5 2.0 %collective-permute-start.15 = (bf16[128,2048]{1,0:T(8,128)(2,1)S(1)}, bf16[128,2048]{1,0:T(8,128)(2,1)S(1)}, u32[]{:S(2)}, u32[]{:S(2)}) collective-permute-start(bf16[128,2048]{1,0:T(8,128)(2,1)S(1)} %broadcast_select_fusion.1), channel_id=1, source_target_pairs={{0,1},{1,0},{2,3},{3,2},{4,7},{7,4},{5,6},{6,5},{8,9},{9,8},{10,11... | collective-permute-start | bytes 1572872 | tf_op jit(solution)/shard_map/ppermute | solution.py:644
  101.5 1.9 %collective-permute-start.7 = (bf16[16,512]{1,0:T(8,128)(2,1)S(1)}, bf16[16,512]{1,0:T(8,128)(2,1)S(1)}, u32[]{:S(2)}, u32[]{:S(2)}) collective-permute-start(bf16[16,512]{1,0:T(8,128)(2,1)S(1)} %copy-done.14), channel_id=1, source_target_pairs={{0,4},{4,8},{8,12},{12,16},{16,20},{20,24},{24,28},{28,32},{32,36}... | collective-permute-start | bytes 49160 | tf_op jit(solution)/shard_map/ppermute | solution.py:653
  103.4 5.4 %collective-permute-done.7.own_t = bf16[16,512]{1,0:T(8,128)(2,1)S(1)} collective-permute-done((bf16[16,512]{1,0:T(8,128)(2,1)S(1)}, bf16[16,512]{1,0:T(8,128)(2,1)S(1)}, u32[]{:S(2)}, u32[]{:S(2)}) %collective-permute-start.7) | collective-permute-done | bytes 16416 | tf_op jit(solution)/shard_map/ppermute | solution.py:653
  108.8 0.1 collective-permute-start.8
  108.9 2.4 %collective-permute-start.9 = (bf16[16,512]{1,0:T(8,128)(2,1)S(1)}, bf16[16,512]{1,0:T(8,128)(2,1)S(1)}, u32[]{:S(2)}, u32[]{:S(2)}) collective-permute-start(bf16[16,512]{1,0:T(8,128)(2,1)S(1)} %collective-permute-done.7.own_t), channel_id=1, source_target_pairs={{0,3},{3,0},{1,2},{2,1},{4,7},{7,4},{5,6},{6,5},{8,11},{11,8},{9,1... | collective-permute-start | bytes 49160 | tf_op jit(solution)/shard_map/ppermute | solution.py:638
  111.3 0.9 collective-permute-start.3
  112.2 0.4 collective-permute-done.8.near_t
  112.5 0.3 collective-permute-start.5
  112.9 1.2 collective-permute-done.9.far_t
  114.1 0.8 collective-permute-start.10
  114.8 0.1 add_bitcast_fusion.2
  114.9 0.1 stack.61.place_ref
  115.0 4.3 %collective-permute-done.10.across_t = bf16[16,512]{1,0:T(8,128)(2,1)S(1)} collective-permute-done((bf16[16,512]{1,0:T(8,128)(2,1)S(1)}, bf16[16,512]{1,0:T(8,128)(2,1)S(1)}, u32[]{:S(2)}, u32[]{:S(2)}) %collective-permute-start.10) | collective-permute-done | bytes 16416 | tf_op jit(solution)/shard_map/ppermute | solution.py:644
  119.3 0.4 collective-permute-start.1
  119.7 3.1 %collective-permute-start.2 = (bf16[512,256]{1,0:T(8,128)(2,1)}, bf16[512,256]{1,0:T(8,128)(2,1)S(1)}, u32[]{:S(2)}, u32[]{:S(2)}) collective-permute-start(bf16[512,256]{1,0:T(8,128)(2,1)} %get-tuple-element.45.own_r), channel_id=1, source_target_pairs={{0,3},{3,0},{1,2},{2,1},{4,7},{7,4},{5,6},{6,5},{8,11},{11,8},{9,1... | collective-permute-start | bytes 786440 | tf_op jit(solution)/shard_map/ppermute | solution.py:638
  122.8 1.1 collective-permute-start.4
  123.9 0.7 collective-permute-start.6
  124.6 0.9 fusion
  125.5 2.8 %collective-permute-done.1.near_l = bf16[512,256]{1,0:T(8,128)(2,1)S(1)} collective-permute-done((bf16[512,256]{1,0:T(8,128)(2,1)S(1)}, bf16[512,256]{1,0:T(8,128)(2,1)S(1)}, u32[]{:S(2)}, u32[]{:S(2)}) %collective-permute-start.1) | collective-permute-done | bytes 262176 | tf_op jit(solution)/shard_map/ppermute | solution.py:634
  128.3 1.9 %collective-permute-start.16 = (bf16[16,2048]{1,0:T(8,128)(2,1)S(1)}, bf16[16,2048]{1,0:T(8,128)(2,1)S(1)}, u32[]{:S(2)}, u32[]{:S(2)}) collective-permute-start(bf16[16,2048]{1,0:T(8,128)(2,1)S(1)} %fusion), channel_id=1, source_target_pairs={{0,4},{4,8},{8,12},{12,16},{16,20},{20,24},{24,28},{28,32},{32,36}... | collective-permute-start | bytes 196616 | tf_op jit(solution)/shard_map/ppermute | solution.py:653
  130.2 0.9 collective-permute-done.4.across_l
  131.1 1.5 collective-permute-done.6.across_r
  132.6 3.3 %collective-permute-done.16.res_t = bf16[16,2048]{1,0:T(8,128)(2,1)S(1)} collective-permute-done((bf16[16,2048]{1,0:T(8,128)(2,1)S(1)}, bf16[16,2048]{1,0:T(8,128)(2,1)S(1)}, u32[]{:S(2)}, u32[]{:S(2)}) %collective-permute-start.16) | collective-permute-done | bytes 65568 | tf_op jit(solution)/shard_map/ppermute | solution.py:653
  136.0 0.5 copy-done.9
  136.6 10.7 %project_norm.1.rows.res_ref = bf16[528,2048]{1,0:T(8,128)(2,1)S(1)} custom-call(s32[5]{0:T(128)S(1)} %stack.61.place_ref, f32[1,2048]{1,0:T(1,128)} %bitcast.27, bf16[512,256]{1,0:T(8,128)(2,1)S(1)} %collective-permute-done.1.near_l, bf16[512,256]{1,0:T(8,128)(2,1)S(1)} %collective-permute-done.2.far_r, ...), custom_call_target="tpu_custom_call" | custom-call | tf_op jit(solution)/shard_map/project_norm/pallas_call | solution.py:410
  147.3 12.8 %widen.1 = (bf16[512,1408]{1,0:T(8,128)(2,1)S(1)}, bf16[2048,1408]{1,0:T(8,128)(2,1)S(1)}, bf16[256,512]{1,0:T(8,128)(2,1)S(1)}, bf16[256,512]{1,0:T(8,128)(2,1)S(1)}) custom-call(s32[2,2]{1,0:T(2,128)S(1)} %pad_add_fusion.1.sent_ref, bf16[3,1408]{1,0:T(4,128)(2,1)} %gate_t.1, bf16[3,1408]{1,0:T(4,128)(2,1)} %up_t.1, ...), custom_call_target="tpu_custom_call" | custom-call | tf_op jit(solution)/shard_map/widen/pallas_call | solution.py:525
  160.1 0.4 collective-permute-start.19
  160.5 2.0 %collective-permute-start.20 = (bf16[256,512]{1,0:T(8,128)(2,1)S(1)}, bf16[256,512]{1,0:T(8,128)(2,1)S(1)}, u32[]{:S(2)}, u32[]{:S(2)}) collective-permute-start(bf16[256,512]{1,0:T(8,128)(2,1)S(1)} %get-tuple-element.60), channel_id=1, source_target_pairs={{0,3},{3,0},{1,2},{2,1},{4,7},{7,4},{5,6},{6,5},{8,11},{11,8},{9,1... | collective-permute-start | bytes 786440 | tf_op jit(solution)/shard_map/ppermute | solution.py:638
  162.4 1.6 shrink_sent.1
  164.0 1.2 collective-permute-start.21
  165.2 1.3 collective-permute-start.22
  166.5 0.1 add_bitcast_fusion
  166.6 2.4 %shrink_held.1 = (f32[128,2048]{1,0:T(8,128)S(1)}, f32[128,1024]{1,0:T(8,128)S(1)}, f32[128,1024]{1,0:T(8,128)S(1)}) custom-call(s32[2,2]{1,0:T(2,128)S(1)} %pad_add_fusion.held_ref, bf16[512,1408]{1,0:T(8,128)(2,1)S(1)} %get-tuple-element.56.hid, bf16[2048,1408]{1,0:T(8,128)(2,1)S(1)} %get-tuple-element.57.down), custom_call_target="tpu_custom_call" | custom-call | tf_op jit(solution)/shard_map/shrink_held/pallas_call | solution.py:572
  168.9 1.9 collective-permute-done.20.once_r.r_1
  170.9 1.4 collective-permute-start.23
  172.4 0.6 collective-permute-done.21.once_l.l_2
  173.0 2.2 %collective-permute-done.22.once_r.r_2 = bf16[256,512]{1,0:T(8,128)(2,1)S(1)} collective-permute-done((bf16[256,512]{1,0:T(8,128)(2,1)S(1)}, bf16[256,512]{1,0:T(8,128)(2,1)S(1)}, u32[]{:S(2)}, u32[]{:S(2)}) %collective-permute-start.22) | collective-permute-done | bytes 262176 | tf_op jit(solution)/shard_map/ppermute | solution.py:638
  175.3 1.6 collective-permute-start.25
  176.9 0.3 collective-permute-done.23.ll_1
  177.2 0.1 collective-permute-done.24.rr_1
  177.3 4.2 %collective-permute-done.25.ll_2 = bf16[128,512]{1,0:T(8,128)(2,1)S(1)} collective-permute-done((bf16[128,512]{1,0:T(8,128)(2,1)S(1)}, bf16[128,512]{1,0:T(8,128)(2,1)S(1)}, u32[]{:S(2)}, u32[]{:S(2)}) %collective-permute-start.25) | collective-permute-done | bytes 131104 | tf_op jit(solution)/shard_map/ppermute | solution.py:638
  181.5 0.3 collective-permute-done.26.rr_2
  181.9 2.1 %last_norm.1 = bf16[128,2048]{1,0:T(8,128)(2,1)} custom-call(s32[5]{0:T(128)S(1)} %stack.61.place_ref, f32[128,2048]{1,0:T(8,128)S(1)} %get-tuple-element.58.own, bf16[256,512]{1,0:T(8,128)(2,1)S(1)} %collective-permute-done.19.once_l.l_1, bf16[256,512]{1,0:T(8,128)(2,1)S(1)} %collective-permute-done.20.once_r.r_1, ...), custom_call_target="tpu_custom_call" | custom-call | tf_op jit(solution)/shard_map/last_norm/pallas_call | solution.py:619
  (49 shorter events, 0.3 us)
Async XLA Ops:
  6.5 140.7 %all-gather.2.cloned.1.call-start = ((), (), s32[]{:S(2)}) async-start(), calls=%async_computation.2 | async-start | bytes 17571840 | tf_op jit(solution)/shard_map/all_gather | solution.py:689
  11.3 38.9 %collective-permute-start.13 = (bf16[512,1024]{1,0:T(8,128)(2,1)}, bf16[512,1024]{1,0:T(8,128)(2,1)S(1)}, u32[]{:S(2)}, u32[]{:S(2)}) collective-permute-start(bf16[512,1024]{1,0:T(8,128)(2,1)} %constant_dynamic-slice_fusion), channel_id=1, source_target_pairs={{0,1},{1,0},{2,3},{3,2},{4,5},{5,4},{6,7},{7,6},{8,9},{9,8},{10,11... | collective-permute-start | bytes 3145736 | tf_op jit(solution)/shard_map/ppermute | solution.py:634
  12.8 37.3 %collective-permute-start.14 = (bf16[512,1024]{1,0:T(8,128)(2,1)}, bf16[512,1024]{1,0:T(8,128)(2,1)S(1)}, u32[]{:S(2)}, u32[]{:S(2)}) collective-permute-start(bf16[512,1024]{1,0:T(8,128)(2,1)} %constant_dynamic-slice_fusion), channel_id=1, source_target_pairs={{0,3},{3,0},{1,2},{2,1},{4,7},{7,4},{5,6},{6,5},{8,11},{11,8},{9,1... | collective-permute-start | bytes 3145736 | tf_op jit(solution)/shard_map/ppermute | solution.py:638
  15.0 32.6 %collective-permute-start.11 = (bf16[128,2048]{1,0:T(8,128)(2,1)}, bf16[128,2048]{1,0:T(8,128)(2,1)S(1)}, u32[]{:S(2)}, u32[]{:S(2)}) collective-permute-start(bf16[128,2048]{1,0:T(8,128)(2,1)} %own_res), channel_id=1, source_target_pairs={{0,1},{1,0},{2,3},{3,2},{4,5},{5,4},{6,7},{7,6},{8,9},{9,8},{10,11... | collective-permute-start | bytes 1572872 | tf_op jit(solution)/shard_map/ppermute | solution.py:634
  15.7 34.4 %collective-permute-start.12 = (bf16[128,2048]{1,0:T(8,128)(2,1)}, bf16[128,2048]{1,0:T(8,128)(2,1)S(1)}, u32[]{:S(2)}, u32[]{:S(2)}) collective-permute-start(bf16[128,2048]{1,0:T(8,128)(2,1)} %own_res), channel_id=1, source_target_pairs={{0,3},{3,0},{1,2},{2,1},{4,7},{7,4},{5,6},{6,5},{8,11},{11,8},{9,1... | collective-permute-start | bytes 1572872 | tf_op jit(solution)/shard_map/ppermute | solution.py:638
  16.3 7.1 %collective-permute-start = (bf16[8,768]{1,0:T(8,128)(2,1)S(1)}, bf16[8,768]{1,0:T(8,128)(2,1)S(1)}, u32[]{:S(2)}, u32[]{:S(2)}) collective-permute-start(bf16[8,768]{1,0:T(8,128)(2,1)S(1)} %rim.1), channel_id=1, source_target_pairs={{0,4},{4,8},{8,12},{12,16},{16,20},{20,24},{24,28},{28,32},{32,36}... | collective-permute-start | bytes 36872 | tf_op jit(solution)/shard_map/ppermute | solution.py:653
  47.6 88.4 %copy-start.3 = (bf16[128,2048]{1,0:T(8,128)(2,1)}, bf16[128,2048]{1,0:T(8,128)(2,1)S(1)}, u32[]{:S(2)}) copy-start(bf16[128,2048]{1,0:T(8,128)(2,1)S(1)} %collective-permute-done.11.near_res) | copy-start | bytes 1572868
  50.1 74.5 %copy-start.4 = (bf16[128,2048]{1,0:T(8,128)(2,1)}, bf16[128,2048]{1,0:T(8,128)(2,1)S(1)}, u32[]{:S(2)}) copy-start(bf16[128,2048]{1,0:T(8,128)(2,1)S(1)} %collective-permute-done.12.far_res) | copy-start | bytes 1572868
  50.1 47.0 %copy-start = (bf16[512,1024]{1,0:T(8,128)(2,1)}, bf16[512,1024]{1,0:T(8,128)(2,1)S(1)}, u32[]{:S(2)}) copy-start(bf16[512,1024]{1,0:T(8,128)(2,1)S(1)} %collective-permute-done.13.near_w) | copy-start | bytes 3145732
  50.1 47.0 %copy-start.1 = (bf16[512,1024]{1,0:T(8,128)(2,1)}, bf16[512,1024]{1,0:T(8,128)(2,1)S(1)}, u32[]{:S(2)}) copy-start(bf16[512,1024]{1,0:T(8,128)(2,1)S(1)} %collective-permute-done.14.far_w) | copy-start | bytes 3145732
  50.3 46.8 %collective-permute-start.17 = (bf16[512,1024]{1,0:T(8,128)(2,1)S(1)}, bf16[512,1024]{1,0:T(8,128)(2,1)S(1)}, u32[]{:S(2)}, u32[]{:S(2)}) collective-permute-start(bf16[512,1024]{1,0:T(8,128)(2,1)S(1)} %broadcast_select_fusion), channel_id=1, source_target_pairs={{0,1},{1,0},{2,3},{3,2},{4,7},{7,4},{5,6},{6,5},{8,9},{9,8},{10,11... | collective-permute-start | bytes 3145736 | tf_op jit(solution)/shard_map/ppermute | solution.py:644
  97.1 2.1 %copy-start.2 = (bf16[512,1024]{1,0:T(8,128)(2,1)}, bf16[512,1024]{1,0:T(8,128)(2,1)S(1)}, u32[]{:S(2)}) copy-start(bf16[512,1024]{1,0:T(8,128)(2,1)S(1)} %collective-permute-done.17.across_w) | copy-start | bytes 3145732
  97.1 4.4 %copy-start.14 = (bf16[16,512]{1,0:T(8,128)(2,1)S(1)}, bf16[16,512]{1,0:T(8,128)(2,1)}, u32[]{:S(2)}) copy-start(bf16[16,512]{1,0:T(8,128)(2,1)} %get-tuple-element.46) | copy-start | bytes 49156
  97.1 14.2 %copy-start.6 = (bf16[512,256]{1,0:T(8,128)(2,1)S(1)}, bf16[512,256]{1,0:T(8,128)(2,1)}, u32[]{:S(2)}) copy-start(bf16[512,256]{1,0:T(8,128)(2,1)} %get-tuple-element.44.own_l) | copy-start | bytes 786436
  99.2 36.8 %collective-permute-start.18 = (bf16[1536,1024]{1,0:T(8,128)(2,1)}, bf16[1536,1024]{1,0:T(8,128)(2,1)}, u32[]{:S(2)}, u32[]{:S(2)}) collective-permute-start(bf16[1536,1024]{1,0:T(8,128)(2,1)} %pad_maximum_fusion), channel_id=1, source_target_pairs={{0,4},{4,0},{1,5},{5,1},{2,6},{6,2},{3,7},{7,3},{8,12},{12,8},{9,1... | collective-permute-start | bytes 9437192 | tf_op jit(solution)/shard_map/ppermute | solution.py:648
  99.5 24.4 %collective-permute-start.15 = (bf16[128,2048]{1,0:T(8,128)(2,1)S(1)}, bf16[128,2048]{1,0:T(8,128)(2,1)S(1)}, u32[]{:S(2)}, u32[]{:S(2)}) collective-permute-start(bf16[128,2048]{1,0:T(8,128)(2,1)S(1)} %broadcast_select_fusion.1), channel_id=1, source_target_pairs={{0,1},{1,0},{2,3},{3,2},{4,7},{7,4},{5,6},{6,5},{8,9},{9,8},{10,11... | collective-permute-start | bytes 1572872 | tf_op jit(solution)/shard_map/ppermute | solution.py:644
  101.5 7.3 %collective-permute-start.7 = (bf16[16,512]{1,0:T(8,128)(2,1)S(1)}, bf16[16,512]{1,0:T(8,128)(2,1)S(1)}, u32[]{:S(2)}, u32[]{:S(2)}) collective-permute-start(bf16[16,512]{1,0:T(8,128)(2,1)S(1)} %copy-done.14), channel_id=1, source_target_pairs={{0,4},{4,8},{8,12},{12,16},{16,20},{20,24},{24,28},{28,32},{32,36}... | collective-permute-start | bytes 49160 | tf_op jit(solution)/shard_map/ppermute | solution.py:653
  108.8 27.2 %copy-start.12 = (bf16[16,512]{1,0:T(8,128)(2,1)}, bf16[16,512]{1,0:T(8,128)(2,1)S(1)}, u32[]{:S(2)}) copy-start(bf16[16,512]{1,0:T(8,128)(2,1)S(1)} %collective-permute-done.7.own_t) | copy-start | bytes 49156
  108.8 3.7 %collective-permute-start.8 = (bf16[16,512]{1,0:T(8,128)(2,1)S(1)}, bf16[16,512]{1,0:T(8,128)(2,1)S(1)}, u32[]{:S(2)}, u32[]{:S(2)}) collective-permute-start(bf16[16,512]{1,0:T(8,128)(2,1)S(1)} %collective-permute-done.7.own_t), channel_id=1, source_target_pairs={{0,1},{1,0},{2,3},{3,2},{4,5},{5,4},{6,7},{7,6},{8,9},{9,8},{10,11... | collective-permute-start | bytes 49160 | tf_op jit(solution)/shard_map/ppermute | solution.py:634
  108.9 5.1 %collective-permute-start.9 = (bf16[16,512]{1,0:T(8,128)(2,1)S(1)}, bf16[16,512]{1,0:T(8,128)(2,1)S(1)}, u32[]{:S(2)}, u32[]{:S(2)}) collective-permute-start(bf16[16,512]{1,0:T(8,128)(2,1)S(1)} %collective-permute-done.7.own_t), channel_id=1, source_target_pairs={{0,3},{3,0},{1,2},{2,1},{4,7},{7,4},{5,6},{6,5},{8,11},{11,8},{9,1... | collective-permute-start | bytes 49160 | tf_op jit(solution)/shard_map/ppermute | solution.py:638
  111.3 8.4 %collective-permute-start.3 = (bf16[512,256]{1,0:T(8,128)(2,1)S(1)}, bf16[512,256]{1,0:T(8,128)(2,1)S(1)}, u32[]{:S(2)}, u32[]{:S(2)}) collective-permute-start(bf16[512,256]{1,0:T(8,128)(2,1)S(1)} %copy-done.6), channel_id=1, source_target_pairs={{0,3},{3,0},{1,2},{2,1},{4,7},{7,4},{5,6},{6,5},{8,11},{11,8},{9,1... | collective-permute-start | bytes 786440 | tf_op jit(solution)/shard_map/ppermute | solution.py:638
  112.5 23.5 %copy-start.10 = (bf16[16,512]{1,0:T(8,128)(2,1)}, bf16[16,512]{1,0:T(8,128)(2,1)S(1)}, u32[]{:S(2)}) copy-start(bf16[16,512]{1,0:T(8,128)(2,1)S(1)} %collective-permute-done.8.near_t) | copy-start | bytes 49156
  112.5 10.3 %collective-permute-start.5 = (bf16[512,256]{1,0:T(8,128)(2,1)}, bf16[512,256]{1,0:T(8,128)(2,1)S(1)}, u32[]{:S(2)}, u32[]{:S(2)}) collective-permute-start(bf16[512,256]{1,0:T(8,128)(2,1)} %get-tuple-element.45.own_r), channel_id=1, source_target_pairs={{0,1},{1,0},{2,3},{3,2},{4,5},{5,4},{6,7},{7,6},{8,9},{9,8},{10,11... | collective-permute-start | bytes 786440 | tf_op jit(solution)/shard_map/ppermute | solution.py:634
  114.1 22.0 %copy-start.11 = (bf16[16,512]{1,0:T(8,128)(2,1)}, bf16[16,512]{1,0:T(8,128)(2,1)S(1)}, u32[]{:S(2)}) copy-start(bf16[16,512]{1,0:T(8,128)(2,1)S(1)} %collective-permute-done.9.far_t) | copy-start | bytes 49156
  114.1 5.2 %collective-permute-start.10 = (bf16[16,512]{1,0:T(8,128)(2,1)S(1)}, bf16[16,512]{1,0:T(8,128)(2,1)S(1)}, u32[]{:S(2)}, u32[]{:S(2)}) collective-permute-start(bf16[16,512]{1,0:T(8,128)(2,1)S(1)} %broadcast_select_fusion.2), channel_id=1, source_target_pairs={{0,1},{1,0},{2,3},{3,2},{4,7},{7,4},{5,6},{6,5},{8,9},{9,8},{10,11... | collective-permute-start | bytes 49160 | tf_op jit(solution)/shard_map/ppermute | solution.py:644
  119.3 16.7 %copy-start.13 = (bf16[16,512]{1,0:T(8,128)(2,1)}, bf16[16,512]{1,0:T(8,128)(2,1)S(1)}, u32[]{:S(2)}) copy-start(bf16[16,512]{1,0:T(8,128)(2,1)S(1)} %collective-permute-done.10.across_t) | copy-start | bytes 49156
  119.3 9.0 %collective-permute-start.1 = (bf16[512,256]{1,0:T(8,128)(2,1)S(1)}, bf16[512,256]{1,0:T(8,128)(2,1)S(1)}, u32[]{:S(2)}, u32[]{:S(2)}) collective-permute-start(bf16[512,256]{1,0:T(8,128)(2,1)S(1)} %copy-done.6), channel_id=1, source_target_pairs={{0,1},{1,0},{2,3},{3,2},{4,5},{5,4},{6,7},{7,6},{8,9},{9,8},{10,11... | collective-permute-start | bytes 786440 | tf_op jit(solution)/shard_map/ppermute | solution.py:634
  119.7 16.3 %copy-start.7 = (bf16[512,256]{1,0:T(8,128)(2,1)}, bf16[512,256]{1,0:T(8,128)(2,1)S(1)}, u32[]{:S(2)}) copy-start(bf16[512,256]{1,0:T(8,128)(2,1)S(1)} %collective-permute-done.3.far_l) | copy-start | bytes 786436
  119.7 10.5 %collective-permute-start.2 = (bf16[512,256]{1,0:T(8,128)(2,1)}, bf16[512,256]{1,0:T(8,128)(2,1)S(1)}, u32[]{:S(2)}, u32[]{:S(2)}) collective-permute-start(bf16[512,256]{1,0:T(8,128)(2,1)} %get-tuple-element.45.own_r), channel_id=1, source_target_pairs={{0,3},{3,0},{1,2},{2,1},{4,7},{7,4},{5,6},{6,5},{8,11},{11,8},{9,1... | collective-permute-start | bytes 786440 | tf_op jit(solution)/shard_map/ppermute | solution.py:638
  122.8 13.2 %copy-start.8 = (bf16[512,256]{1,0:T(8,128)(2,1)}, bf16[512,256]{1,0:T(8,128)(2,1)S(1)}, u32[]{:S(2)}) copy-start(bf16[512,256]{1,0:T(8,128)(2,1)S(1)} %collective-permute-done.5.near_r) | copy-start | bytes 786436
  122.8 8.3 %collective-permute-start.4 = (bf16[512,256]{1,0:T(8,128)(2,1)S(1)}, bf16[512,256]{1,0:T(8,128)(2,1)S(1)}, u32[]{:S(2)}, u32[]{:S(2)}) collective-permute-start(bf16[512,256]{1,0:T(8,128)(2,1)S(1)} %collective-permute-done.3.far_l), channel_id=1, source_target_pairs={{0,1},{1,0},{2,3},{3,2},{4,5},{5,4},{6,7},{7,6},{8,9},{9,8},{10,11... | collective-permute-start | bytes 786440 | tf_op jit(solution)/shard_map/ppermute | solution.py:634
  123.9 12.1 %copy-start.5 = (bf16[128,2048]{1,0:T(8,128)(2,1)}, bf16[128,2048]{1,0:T(8,128)(2,1)S(1)}, u32[]{:S(2)}) copy-start(bf16[128,2048]{1,0:T(8,128)(2,1)S(1)} %collective-permute-done.15.across_res) | copy-start | bytes 1572868
  123.9 8.7 %collective-permute-start.6 = (bf16[512,256]{1,0:T(8,128)(2,1)S(1)}, bf16[512,256]{1,0:T(8,128)(2,1)S(1)}, u32[]{:S(2)}, u32[]{:S(2)}) collective-permute-start(bf16[512,256]{1,0:T(8,128)(2,1)S(1)} %collective-permute-done.5.near_r), channel_id=1, source_target_pairs={{0,3},{3,0},{1,2},{2,1},{4,7},{7,4},{5,6},{6,5},{8,11},{11,8},{9,1... | collective-permute-start | bytes 786440 | tf_op jit(solution)/shard_map/ppermute | solution.py:638
  128.3 7.7 %collective-permute-start.16 = (bf16[16,2048]{1,0:T(8,128)(2,1)S(1)}, bf16[16,2048]{1,0:T(8,128)(2,1)S(1)}, u32[]{:S(2)}, u32[]{:S(2)}) collective-permute-start(bf16[16,2048]{1,0:T(8,128)(2,1)S(1)} %fusion), channel_id=1, source_target_pairs={{0,4},{4,8},{8,12},{12,16},{16,20},{20,24},{24,28},{28,32},{32,36}... | collective-permute-start | bytes 196616 | tf_op jit(solution)/shard_map/ppermute | solution.py:653
  136.0 0.6 copy-start.9
  160.1 8.9 %collective-permute-start.19 = (bf16[256,512]{1,0:T(8,128)(2,1)S(1)}, bf16[256,512]{1,0:T(8,128)(2,1)S(1)}, u32[]{:S(2)}, u32[]{:S(2)}) collective-permute-start(bf16[256,512]{1,0:T(8,128)(2,1)S(1)} %get-tuple-element.59), channel_id=1, source_target_pairs={{0,1},{1,0},{2,3},{3,2},{4,5},{5,4},{6,7},{7,6},{8,9},{9,8},{10,11... | collective-permute-start | bytes 786440 | tf_op jit(solution)/shard_map/ppermute | solution.py:634
  160.5 10.4 %collective-permute-start.20 = (bf16[256,512]{1,0:T(8,128)(2,1)S(1)}, bf16[256,512]{1,0:T(8,128)(2,1)S(1)}, u32[]{:S(2)}, u32[]{:S(2)}) collective-permute-start(bf16[256,512]{1,0:T(8,128)(2,1)S(1)} %get-tuple-element.60), channel_id=1, source_target_pairs={{0,3},{3,0},{1,2},{2,1},{4,7},{7,4},{5,6},{6,5},{8,11},{11,8},{9,1... | collective-permute-start | bytes 786440 | tf_op jit(solution)/shard_map/ppermute | solution.py:638
  164.0 9.0 %collective-permute-start.21 = (bf16[256,512]{1,0:T(8,128)(2,1)S(1)}, bf16[256,512]{1,0:T(8,128)(2,1)S(1)}, u32[]{:S(2)}, u32[]{:S(2)}) collective-permute-start(bf16[256,512]{1,0:T(8,128)(2,1)S(1)} %get-tuple-element.61), channel_id=1, source_target_pairs={{0,1},{1,0},{2,3},{3,2},{4,5},{5,4},{6,7},{7,6},{8,9},{9,8},{10,11... | collective-permute-start | bytes 786440 | tf_op jit(solution)/shard_map/ppermute | solution.py:634
  165.2 10.0 %collective-permute-start.22 = (bf16[256,512]{1,0:T(8,128)(2,1)S(1)}, bf16[256,512]{1,0:T(8,128)(2,1)S(1)}, u32[]{:S(2)}, u32[]{:S(2)}) collective-permute-start(bf16[256,512]{1,0:T(8,128)(2,1)S(1)} %get-tuple-element.62), channel_id=1, source_target_pairs={{0,3},{3,0},{1,2},{2,1},{4,7},{7,4},{5,6},{6,5},{8,11},{11,8},{9,1... | collective-permute-start | bytes 786440 | tf_op jit(solution)/shard_map/ppermute | solution.py:638
  170.9 6.3 %collective-permute-start.23 = (bf16[128,512]{1,0:T(8,128)(2,1)S(1)}, bf16[128,512]{1,0:T(8,128)(2,1)S(1)}, u32[]{:S(2)}, u32[]{:S(2)}) collective-permute-start(bf16[128,512]{1,0:T(8,128)(2,1)S(1)} %get-tuple-element.64), channel_id=1, source_target_pairs={{0,3},{3,0},{1,2},{2,1},{4,7},{7,4},{5,6},{6,5},{8,11},{11,8},{9,1... | collective-permute-start | bytes 393224 | tf_op jit(solution)/shard_map/ppermute | solution.py:638
  172.4 5.0 %collective-permute-start.24 = (bf16[128,512]{1,0:T(8,128)(2,1)S(1)}, bf16[128,512]{1,0:T(8,128)(2,1)S(1)}, u32[]{:S(2)}, u32[]{:S(2)}) collective-permute-start(bf16[128,512]{1,0:T(8,128)(2,1)S(1)} %get-tuple-element.65), channel_id=1, source_target_pairs={{0,1},{1,0},{2,3},{3,2},{4,5},{5,4},{6,7},{7,6},{8,9},{9,8},{10,11... | collective-permute-start | bytes 393224 | tf_op jit(solution)/shard_map/ppermute | solution.py:634
  175.3 6.3 %collective-permute-start.25 = (bf16[128,512]{1,0:T(8,128)(2,1)S(1)}, bf16[128,512]{1,0:T(8,128)(2,1)S(1)}, u32[]{:S(2)}, u32[]{:S(2)}) collective-permute-start(bf16[128,512]{1,0:T(8,128)(2,1)S(1)} %get-tuple-element.67), channel_id=1, source_target_pairs={{0,3},{3,0},{1,2},{2,1},{4,7},{7,4},{5,6},{6,5},{8,11},{11,8},{9,1... | collective-permute-start | bytes 393224 | tf_op jit(solution)/shard_map/ppermute | solution.py:638
  176.9 5.0 %collective-permute-start.26 = (bf16[128,512]{1,0:T(8,128)(2,1)S(1)}, bf16[128,512]{1,0:T(8,128)(2,1)S(1)}, u32[]{:S(2)}, u32[]{:S(2)}) collective-permute-start(bf16[128,512]{1,0:T(8,128)(2,1)S(1)} %get-tuple-element.68), channel_id=1, source_target_pairs={{0,1},{1,0},{2,3},{3,2},{4,5},{5,4},{6,7},{7,6},{8,9},{9,8},{10,11... | collective-permute-start | bytes 393224 | tf_op jit(solution)/shard_map/ppermute | solution.py:634
Sparse Core Ops, SparseCore 0:
  10.1 106.6 all-gather.1
where the time goes:
time: 191 us
  waiting for transfers between devices  49.1 us (26%)
  Pallas kernels  46.3 us (24%)
  blocking collectives  43 us (23%)
  starting transfers between devices  30.8 us (16%)
  between operations  13.7 us (7%)
  other arithmetic  4.97 us (3%)
  local copies, waits for them, and re-layouts  2.96 us (2%)
    all_to_all x1, blocking collectives, shards(): received = lax.all_to_all(message, SP, 0, 0, tiled=True)  25.4 us
    all_to_all x1, blocking collectives, shards(): entering = lax.all_to_all(prefix, SP, 0, 0, tiled=True)  17.6 us
    ppermute x10, waiting for transfers between devices, with_near(): return lax.ppermute(part, 'tp', NEAR)  17.1 us
    ppermute x10, starting transfers between devices, with_far(): return lax.ppermute(part, 'tp', FAR)  16.2 us
    ppermute x3, waiting for transfers between devices, next_positions(): return lax.ppermute(shard, SP, [(i, i + 1) for i in range(count - 1)])  13.9 us
    ppermute x10, waiting for transfers between devices, with_far(): return lax.ppermute(part, 'tp', FAR)  13.8 us
    pallas_call x1, Pallas kernels, run_widen(): pl.pallas_call(widen_kernel, out_shape=(close_out((ROWS, FFL), BF16), clo...  12.8 us
    pallas_call x1, Pallas kernels, run_project(): pl.pallas_call(project_kernel, out_shape=close_out((RIM + ROWS, D), BF16)...  10.7 us
  transfers between devices with their start and end apart: 28, of which 18 were waited for; matrix products, arithmetic and copies ran while one was open for 3% of the time, Pallas kernels for 16%

commit v1 on v0

--- a/solution.py
+++ b/solution.py
@@ -290,7 +290,7 @@
     )(close(received))
 
 
-def gate_kernel(y_ref, cact_ref, grow_ref, in_ref, valve_ref, scale_ref, out_l, out_r, tail_ref):
+def gate_kernel(y_ref, cact_ref, grow_ref, in_ref, valve_ref, scale_ref, out_l, out_r):
     for i in range(ROWS // BLOCK):
         rows = pl.ds(i * BLOCK, BLOCK)
         grown = lane_pairs(grow_ref[rows, :], BLOCK)
@@ -308,10 +308,9 @@
         for q in range(NH // 2):
             cols = slice(q * 128, (q + 1) * 128)
             half = (out_l, out_r)[q // 2]
-            done = (gated[q] * factor * scale_ref[0:1, cols]).astype(BF16)
-            half[rows, (q % 2) * 128 : (q % 2 + 1) * 128] = done
-            if i == ROWS // BLOCK - 1:
-                tail_ref[:, cols] = done[BLOCK - RIM :, :]
+            half[rows, (q % 2) * 128 : (q % 2 + 1) * 128] = (
+                gated[q] * factor * scale_ref[0:1, cols]
+            ).astype(BF16)
 
 
 def run_gate(y, cact, grow, entering, valve, scale):
@@ -320,11 +319,10 @@
         out_shape=(
             away_out((ROWS, HALFCH), BF16),
             away_out((ROWS, HALFCH), BF16),
-            away_out((RIM, CH), BF16),
         ),
         compiler_params=limit(16),
         in_specs=[VMEM] * 6,
-        out_specs=(VMEM,) * 3,
+        out_specs=(VMEM,) * 2,
         name="gate_norm",
     )(*away(y, cact, grow), close(entering), *away(valve, scale))
 
@@ -335,18 +333,17 @@
 
 def project_kernel(
     place_ref, scale_ref, near_l, far_r, across_l, across_r,
-    own_l, own_r, near_r, far_l, own_t, near_t, far_t, across_t, res_t, own_w, near_w, far_w, across_w, other_w,
+    own_l, own_r, near_r, far_l, own_w, near_w, far_w, across_w, near_x, far_x, across_x,
     own_res, near_res, far_res, across_res,
-    out_ref,
-    weight, early, tails, tail_res, res, total, w_sems, e_sems, t_sems, r_sems,
+    out_ref, tail_ref,
+    weight, early, res, total, w_sems, e_sems, r_sems,
 ):
     core = place_ref[4]
     columns_of = (
         pl.ds(pl.multiple_of(core * HALF, HALF), HALF),
         pl.ds(pl.multiple_of((1 - core) * HALF, HALF), HALF),
     )
-    others = [other_w.at[k * CH : (k + 1) * CH, :] for k in range(3)]
-    arrived = ((near_w, far_w, across_w), others)
+    arrived = ((near_w, far_w, across_w), (near_x, far_x, across_x))
     copies = ([], [])
     for half in range(2):
         sources = (own_w.at[:, columns_of[half]], *arrived[half])
@@ -361,11 +358,6 @@
         pltpu.make_async_copy(source, early.at[k], e_sems.at[k])
         for k, source in enumerate((own_l, own_r, near_r, far_l))
     ]
-    early_copies += [
-        pltpu.make_async_copy(source, tails.at[k], t_sems.at[k])
-        for k, source in enumerate((own_t, near_t, far_t, across_t))
-    ]
-    early_copies.append(pltpu.make_async_copy(res_t, tail_res, t_sems.at[4]))
     acts = (early.at[0], early.at[1], near_l, early.at[2], early.at[3], far_r, across_l, across_r)
     for copy in early_copies + copies[0]:
         copy.start()
@@ -381,9 +373,7 @@
             cols = slice(n * CHUNK, (n + 1) * CHUNK)
             part = None
             for k, act in enumerate(acts):
-                side = slice((k % 2) * HALFCH, (k % 2 + 1) * HALFCH)
-                lhs = jnp.concatenate([tails[k // 2, :, side], act[...]], axis=0)
-                term = dot(lhs, weight[half, k * HALFCH : (k + 1) * HALFCH, cols])
+                term = dot(act[...], weight[half, k * HALFCH : (k + 1) * HALFCH, cols])
                 part = term if part is None else part + term
             start = pl.multiple_of((core if half == 0 else 1 - core) * HALF + n * CHUNK, CHUNK)
             total[:, pl.ds(start, CHUNK)] = part
@@ -395,33 +385,29 @@
         spread = jnp.sum(centred * centred, axis=-1, keepdims=True) * (1.0 / D)
         return (centred * lax.rsqrt(spread + EPSILON) * scale_ref[...]).astype(BF16)
 
-    out_ref[0:RIM, :] = norm(total[0:RIM, :] + ALPHA * tail_res[...].astype(F32))
 
     def norm_rows(i, carry):
         rows = pl.ds(pl.multiple_of(i * 64, 64), 64)
-        shifted = pl.ds(pl.multiple_of(RIM + i * 64, 16), 64)
-        out_ref[shifted, :] = norm(total[shifted, :] + ALPHA * res[rows, :].astype(F32))
+        out_ref[rows, :] = norm(total[rows, :] + ALPHA * res[rows, :].astype(F32))
         return carry
 
     lax.fori_loop(0, ROWS // 64, norm_rows, 0)
-
-
-def run_project(place, scale, weights, acts, tails, residuals):
+    tail_ref[...] = out_ref[ROWS - RIM : ROWS, :]
+
+
+def run_project(place, scale, weights, acts, residuals):
     return pl.pallas_call(
         project_kernel,
-        out_shape=close_out((RIM + ROWS, D), BF16),
-        in_specs=[SMEM] + [VMEM] * 5 + [ANY] * 18,
-        out_specs=VMEM,
+        out_shape=(close_out((ROWS, D), BF16), close_out((RIM, D), BF16)),
+        in_specs=[SMEM] + [VMEM] * 5 + [ANY] * 15,
+        out_specs=(VMEM, VMEM),
         scratch_shapes=[
             pltpu.VMEM((2, D, HALF), BF16),
             pltpu.VMEM((4, ROWS, HALFCH), BF16),
-            pltpu.VMEM((4, RIM, CH), BF16),
-            pltpu.VMEM((RIM, D), BF16),
             pltpu.VMEM((ROWS, D), BF16),
-            pltpu.VMEM((RIM + ROWS, D), F32),
+            pltpu.VMEM((ROWS, D), F32),
             pltpu.SemaphoreType.DMA((2, 4)),
             pltpu.SemaphoreType.DMA((4,)),
-            pltpu.SemaphoreType.DMA((5,)),
             pltpu.SemaphoreType.DMA((4,)),
         ],
         compiler_params=limit(30),
@@ -430,7 +416,7 @@
         place,
         *away(scale),
         *[close(acts[k]) for k in (2, 5, 6, 7)],
-        *away(*[acts[k] for k in (0, 1, 3, 4)], *tails, *weights, *residuals),
+        *away(*[acts[k] for k in (0, 1, 3, 4)], *weights, *residuals),
     )
 
 
@@ -461,7 +447,7 @@
 
 
 def widen_kernel(
-    sent_ref, gate_t, up_t, rows, w_ref,
+    sent_ref, gate_t, up_t, normed, rim, w_ref,
     hid, down, send_l, send_r,
     wide, gate_pad, up_pad, wide_sems, down_sems,
 ):
@@ -506,7 +492,8 @@
                 copy.start()
 
         at = pl.multiple_of(j * 128, 128)
-        both = dot(rows[...], wide[j]).astype(BF16).astype(F32)
+        rows = jnp.concatenate([rim[...], normed[...]], axis=0)
+        both = dot(rows, wide[j]).astype(BF16).astype(F32)
         gate_pad[...] = both[:, 0:128]
         up_pad[...] = both[:, 128:256]
         hid[:, pl.ds(at, 128)] = (
@@ -521,7 +508,7 @@
     send_r[...] = dot_nt(two_quarters(hid, sent_ref, 1), down[HALF : HALF + STRIP, :]).astype(BF16)
 
 
-def run_widen(sent, rows, weights, gate_t, up_t):
+def run_widen(sent, normed, rim, weights, gate_t, up_t):
     return pl.pallas_call(
         widen_kernel,
         out_shape=(
@@ -530,7 +517,7 @@
             close_out((2 * QUARTER, STRIP), BF16),
             close_out((2 * QUARTER, STRIP), BF16),
         ),
-        in_specs=[SMEM, VMEM, VMEM, VMEM, ANY],
+        in_specs=[SMEM, VMEM, VMEM, VMEM, VMEM, ANY],
         out_specs=(VMEM,) * 4,
         scratch_shapes=[
             pltpu.VMEM((TILES, D, 256), BF16),
@@ -541,7 +528,7 @@
         ],
         compiler_params=limit(24),
         name="widen",
-    )(sent, *away(gate_t, up_t), close(rows), *away(weights))
+    )(sent, *away(gate_t, up_t), close(normed), close(rim), *away(weights))
 
 
 def sent_kernel(sent_ref, hid, down, send_l, send_r):
@@ -599,10 +586,12 @@
     )(close(passed), close(once_l), close(once_r))
 
 
-def last_norm_kernel(place_ref, own, l_1, r_1, l_2, r_2, ll_1, rr_1, ll_2, rr_2, res_ref, scale_ref, out_ref):
+def last_norm_kernel(
+    place_ref, own, l_1, r_1, l_2, r_2, ll_1, rr_1, ll_2, rr_2, res_ref, scale_ref, out_ref
+):
     for i in range(2):
         rows = slice(i * 64, (i + 1) * 64)
-        kept = pl.ds(pl.multiple_of(RIM + place_ref[0] * QUARTER + i * 64, 16), 64)
+        kept = pl.ds(pl.multiple_of(place_ref[0] * QUARTER + i * 64, 64), 64)
         parts = []
         for k, (once, twice) in enumerate(((l_1, ll_1), (l_2, ll_2), (r_1, rr_1), (r_2, rr_2))):
             cols = slice(k * STRIP, (k + 1) * STRIP)
@@ -729,39 +718,34 @@
     )
     prefix = run_prefix(received)
     entering = lax.all_to_all(prefix, SP, 0, 0, tiled=True)
-    late = lax.optimization_barrier((y_local, w_near, w_far, res_near, res_far))
-    w_across = forwarded(late[2], late[1])
-    res_across = forwarded(late[4], late[3])
-    y_l, y_r, tail = run_gate(
+    _, late_near, late_far = lax.optimization_barrier((y_local, w_near, w_far))
+    w_across = forwarded(late_far, late_near)
+    _, late_near, late_far = lax.optimization_barrier((prefix, res_near, res_far))
+    res_across = forwarded(late_far, late_near)
+    y_l, y_r = run_gate(
         y_local, c_act, grow, entering, result_valve, cluster_scaling_vector.reshape(1, CH)
     )
-    swap = lax.optimization_barrier((w_near, w_far, w_across, y_l))[:3]
-    w_other = with_core(jnp.concatenate(swap, axis=0))
-    tail_own = next_positions(tail)
+    swap = lax.optimization_barrier((prefix, w_near, w_far))[1:]
+    w_other = (
+        with_core(swap[0]),
+        with_core(swap[1]),
+        with_core(lax.optimization_barrier((y_l, w_across))[1]),
+    )
     far_l = with_far(y_l)
     near_r = with_near(y_r)
     near_l = with_near(y_l)
     far_r = with_far(y_r)
-    tail_near = with_near(tail_own)
-    tail_far = with_far(tail_own)
-    tail_across = forwarded(tail_far, tail_near)
-    ends = [
-        jnp.where(at == 3, part[QUARTER - RIM :], jnp.zeros((RIM, D), BF16))
-        for at, part in ((own, residual), (near, res_near), (far, res_far), (across, res_across))
-    ]
-    res_tail = next_positions(ends[0] + ends[1] + ends[2] + ends[3])
     across_l = with_near(far_l)
     across_r = with_far(near_r)
-    rows = run_project(
+    normed, tail = run_project(
         place,
         initial_scaling_vector.reshape(1, D),
-        (mixer_result_matrix, w_near, w_far, w_across, w_other),
+        (mixer_result_matrix, w_near, w_far, w_across, *w_other),
         (y_l, y_r, near_l, near_r, far_l, far_r, across_l, across_r),
-        (tail_own, tail_near, tail_far, tail_across, res_tail),
         (residual, res_near, res_far, res_across),
     )
     hidden, down, send_l1, send_r1 = run_widen(
-        sent, rows, weights, valve_filter_kernel, widen_filter_kernel
+        sent, normed, next_positions(tail), weights, valve_filter_kernel, widen_filter_kernel
     )
     l_1 = with_near(send_l1)
     r_1 = with_far(send_r1)
@@ -780,7 +764,7 @@
         kept,
         (l_1, r_1, l_2, r_2),
         (ll_1, rr_1, ll_2, rr_2),
-        rows,
+        normed,
         latter_scaling_vector.reshape(1, D),
     )
 

time: 191 us -> 189 us (0.990)
  the two profiles are of different devices: /device:TPU:32 before, /device:TPU:1 now
where the time goes in v1:
time: 189 us; the launch traced here: 187 us
  waiting for transfers between devices  53.7 us (28%)
  starting transfers between devices  52.8 us (28%)
  Pallas kernels  45.8 us (24%)
  blocking collectives  16.9 us (9%)
  between operations  13.6 us (7%)
  other arithmetic  3.06 us (2%)
    ppermute x9, waiting for transfers between devices, with_near(): return lax.ppermute(part, 'tp', NEAR)  23 us
    ppermute x9, waiting for transfers between devices, with_far(): return lax.ppermute(part, 'tp', FAR)  19.2 us
    all_to_all x1, blocking collectives, shards(): entering = lax.all_to_all(prefix, SP, 0, 0, tiled=True)  16.9 us
    ppermute x2, starting transfers between devices, next_positions(): return lax.ppermute(shard, SP, [(i, i + 1) for i in range(count - 1)])  14.5 us
    pallas_call x1, Pallas kernels, run_widen(): pl.pallas_call(widen_kernel, out_shape=(close_out((ROWS, FFL), BF16), clo...  12.8 us
    all_to_all x1, starting transfers between devices, shards(): received = lax.all_to_all(message, SP, 0, 0, tiled=True)  12.6 us
    ppermute x9, starting transfers between devices, with_far(): return lax.ppermute(part, 'tp', FAR)  12.4 us
    pallas_call x1, Pallas kernels, run_project(): pl.pallas_call(project_kernel, out_shape=(close_out((ROWS, D), BF16), clo...  10.2 us
  transfers between devices with their start and end apart: 27, of which 16 were waited for; matrix products, arithmetic and copies ran while one was open for 1% of the time, Pallas kernels for 17%

profile of v1, /device:TPU:1, one launch (start us, length us, event | category | flops | bytes accessed | tf_op | source)
XLA Modules:
  0.0 187.3 jit_solution(5966636500147838635)
XLA Ops:
  6.5 1.7 pad_maximum_fusion
  8.3 0.0 all-gather.2.cloned.1.call-update
  8.3 0.7 rim.1
  9.0 1.3 constant_dynamic-slice_fusion
  10.3 2.2 %collective-permute-start.7 = (bf16[512,1024]{1,0:T(8,128)(2,1)S(1)}, bf16[512,1024]{1,0:T(8,128)(2,1)S(1)}, u32[]{:S(2)}, u32[]{:S(2)}) collective-permute-start(bf16[512,1024]{1,0:T(8,128)(2,1)S(1)} %constant_dynamic-slice_fusion), channel_id=1, source_target_pairs={{0,1},{1,0},{2,3},{3,2},{4,5},{5,4},{6,7},{7,6},{8,9},{9,8},{10,11... | collective-permute-start | bytes 3145736 | tf_op jit(solution)/shard_map/ppermute | solution.py:623
  12.5 1.9 %collective-permute-start.8 = (bf16[512,1024]{1,0:T(8,128)(2,1)S(1)}, bf16[512,1024]{1,0:T(8,128)(2,1)}, u32[]{:S(2)}, u32[]{:S(2)}) collective-permute-start(bf16[512,1024]{1,0:T(8,128)(2,1)S(1)} %constant_dynamic-slice_fusion), channel_id=1, source_target_pairs={{0,3},{3,0},{1,2},{2,1},{4,7},{7,4},{5,6},{6,5},{8,11},{11,8},{9,1... | collective-permute-start | bytes 3145736 | tf_op jit(solution)/shard_map/ppermute | solution.py:627
  14.4 4.2 %collective-permute-start = (bf16[8,768]{1,0:T(8,128)(2,1)S(1)}, bf16[8,768]{1,0:T(8,128)(2,1)S(1)}, u32[]{:S(2)}, u32[]{:S(2)}) collective-permute-start(bf16[8,768]{1,0:T(8,128)(2,1)S(1)} %rim.1), channel_id=1, source_target_pairs={{0,4},{4,8},{8,12},{12,16},{16,20},{20,24},{24,28},{28,32},{32,36}... | collective-permute-start | bytes 36872 | tf_op jit(solution)/shard_map/ppermute | solution.py:642
  18.6 0.8 collective-permute-done.rim_ref
  19.5 5.7 %local_state.1 = (bf16[512,512]{1,0:T(8,128)(2,1)}, bf16[512,128]{1,0:T(8,128)(2,1)}, bf16[3,128,512]{2,1,0:T(8,128)(2,1)}, bf16[64,16,128]{2,1,0:T(8,128)(2,1)}) custom-call(bf16[512,512]{1,0:T(8,128)(2,1)} %x_ref.3, bf16[512,128]{1,0:T(8,128)(2,1)} %b_ref.3, bf16[8,768]{1,0:T(8,128)(2,1)S(1)} %collective-permute-done.rim_ref, bf16[4,512]{1,0:T(4,128)(2,1)} %xt_ref.1, ...), custom_call_target="tpu_custom_call" | custom-call | tf_op jit(solution)/shard_map/local_state/pallas_call | solution.py:197
  25.1 6.7 %local_mixer.1 = (f32[512,512]{1,0:T(8,128)}, bf16[512,128]{1,0:T(8,128)(2,1)}, f32[512,8]{1,0:T(8,128)}) custom-call(bf16[512,512]{1,0:T(8,128)(2,1)} %get-tuple-element.38.x_ref, bf16[512,128]{1,0:T(8,128)(2,1)} %get-tuple-element.39.b_ref, bf16[3,128,512]{2,1,0:T(8,128)(2,1)} %get-tuple-element.40.state_ref, bf16[512,128]{1,0:T(8,128)(2,1)} %c_ref.3, ...), custom_call_target="tpu_custom_call" | custom-call | tf_op jit(solution)/shard_map/local_mixer/pallas_call | solution.py:258
  31.8 2.4 %collective-permute-done.7.near_w = bf16[512,1024]{1,0:T(8,128)(2,1)S(1)} collective-permute-done((bf16[512,1024]{1,0:T(8,128)(2,1)S(1)}, bf16[512,1024]{1,0:T(8,128)(2,1)S(1)}, u32[]{:S(2)}, u32[]{:S(2)}) %collective-permute-start.7) | collective-permute-done | bytes 1048608 | tf_op jit(solution)/shard_map/ppermute | solution.py:623
  34.2 3.1 %collective-permute-done.8.far_w = bf16[512,1024]{1,0:T(8,128)(2,1)} collective-permute-done((bf16[512,1024]{1,0:T(8,128)(2,1)S(1)}, bf16[512,1024]{1,0:T(8,128)(2,1)}, u32[]{:S(2)}, u32[]{:S(2)}) %collective-permute-start.8) | collective-permute-done | bytes 1048608 | tf_op jit(solution)/shard_map/ppermute | solution.py:627
  37.3 1.1 broadcast_select_fusion
  38.5 2.1 %collective-permute-start.9 = (bf16[512,1024]{1,0:T(8,128)(2,1)}, bf16[512,1024]{1,0:T(8,128)(2,1)}, u32[]{:S(2)}, u32[]{:S(2)}) collective-permute-start(bf16[512,1024]{1,0:T(8,128)(2,1)} %broadcast_select_fusion), channel_id=1, source_target_pairs={{0,1},{1,0},{2,3},{3,2},{4,7},{7,4},{5,6},{6,5},{8,9},{9,8},{10,11... | collective-permute-start | bytes 3145736 | tf_op jit(solution)/shard_map/ppermute | solution.py:633
  40.6 12.6 %all-to-all-start = ((bf16[64,16,128]{2,1,0:T(8,128)(2,1)}), bf16[64,16,128]{2,1,0:T(8,128)(2,1)S(1)}, u32[]{:S(2)}, u32[]{:S(2)}) async-start(bf16[64,16,128]{2,1,0:T(8,128)(2,1)} %get-tuple-element.44), calls=%async_computation | async-start | bytes 524288 | tf_op jit(solution)/shard_map/all_to_all | solution.py:701
  53.2 1.8 collective-permute-start.13
  55.1 1.9 %collective-permute-start.14 = (bf16[128,2048]{1,0:T(8,128)(2,1)}, bf16[128,2048]{1,0:T(8,128)(2,1)S(1)}, u32[]{:S(2)}, u32[]{:S(2)}) collective-permute-start(bf16[128,2048]{1,0:T(8,128)(2,1)} %own_res), channel_id=1, source_target_pairs={{0,3},{3,0},{1,2},{2,1},{4,7},{7,4},{5,6},{6,5},{8,11},{11,8},{9,1... | collective-permute-start | bytes 1572872 | tf_op jit(solution)/shard_map/ppermute | solution.py:627
  57.0 9.4 %all-to-all-done.in_ref = bf16[64,16,128]{2,1,0:T(8,128)(2,1)S(1)} async-done(((bf16[64,16,128]{2,1,0:T(8,128)(2,1)}), bf16[64,16,128]{2,1,0:T(8,128)(2,1)S(1)}, u32[]{:S(2)}, u32[]{:S(2)}) %all-to-all-start) | async-done | bytes 262176 | tf_op jit(solution)/shard_map/all_to_all | solution.py:701
  66.3 0.1 state_prefix.1
  66.5 16.9 %all_to_all.10.in_ref = bf16[64,8,128]{2,1,0:T(8,128)(2,1)S(1)} all-to-all(bf16[64,8,128]{2,1,0:T(8,128)(2,1)S(1)} %state_prefix.1), channel_id=1, replica_groups=mesh['sp_0'=8,'sp_1'=4,'sp_2'=2,'tp'=4] {'sp_0','sp_1','sp_2'}, dimensions={0} | all-to-all | bytes 262144 | tf_op jit(solution)/shard_map/all_to_all | solution.py:720
  83.3 3.6 %gate_norm.1 = (bf16[512,256]{1,0:T(8,128)(2,1)}, bf16[512,256]{1,0:T(8,128)(2,1)}) custom-call(f32[512,512]{1,0:T(8,128)} %get-tuple-element.41.y_ref, bf16[512,128]{1,0:T(8,128)(2,1)} %get-tuple-element.42.cact_ref, f32[512,8]{1,0:T(8,128)} %get-tuple-element.43.grow_ref, bf16[64,8,128]{2,1,0:T(8,128)(2,1)S(1)} %all_to_all.10.in_ref, ...), custom_call_target="tpu_custom_call" | custom-call | tf_op jit(solution)/shard_map/gate_norm/pallas_call | solution.py:317
  86.9 1.7 collective-permute-start.1
  88.6 2.0 %collective-permute-start.3 = (bf16[512,256]{1,0:T(8,128)(2,1)}, bf16[512,256]{1,0:T(8,128)(2,1)S(1)}, u32[]{:S(2)}, u32[]{:S(2)}) collective-permute-start(bf16[512,256]{1,0:T(8,128)(2,1)} %get-tuple-element.45.own_l), channel_id=1, source_target_pairs={{0,3},{3,0},{1,2},{2,1},{4,7},{7,4},{5,6},{6,5},{8,11},{11,8},{9,1... | collective-permute-start | bytes 786440 | tf_op jit(solution)/shard_map/ppermute | solution.py:627
  90.6 0.8 collective-permute-start.2
  91.4 1.3 collective-permute-start.10
  92.7 0.0 collective-permute-done.9.across_w
  92.7 0.1 collective-permute-start.11
  92.8 2.4 %collective-permute-done.1.near_l = bf16[512,256]{1,0:T(8,128)(2,1)S(1)} collective-permute-done((bf16[512,256]{1,0:T(8,128)(2,1)}, bf16[512,256]{1,0:T(8,128)(2,1)S(1)}, u32[]{:S(2)}, u32[]{:S(2)}) %collective-permute-start.1) | collective-permute-done | bytes 262176 | tf_op jit(solution)/shard_map/ppermute | solution.py:623
  95.1 1.0 collective-permute-start.12
  96.1 0.1 broadcast_select_fusion.1
  96.2 6.9 %collective-permute-done.2.far_r = bf16[512,256]{1,0:T(8,128)(2,1)S(1)} collective-permute-done((bf16[512,256]{1,0:T(8,128)(2,1)}, bf16[512,256]{1,0:T(8,128)(2,1)S(1)}, u32[]{:S(2)}, u32[]{:S(2)}) %collective-permute-start.2) | collective-permute-done | bytes 262176 | tf_op jit(solution)/shard_map/ppermute | solution.py:627
  103.0 1.9 %collective-permute-start.15 = (bf16[128,2048]{1,0:T(8,128)(2,1)S(1)}, bf16[128,2048]{1,0:T(8,128)(2,1)}, u32[]{:S(2)}, u32[]{:S(2)}) collective-permute-start(bf16[128,2048]{1,0:T(8,128)(2,1)S(1)} %broadcast_select_fusion.1), channel_id=1, source_target_pairs={{0,1},{1,0},{2,3},{3,2},{4,7},{7,4},{5,6},{6,5},{8,9},{9,8},{10,11... | collective-permute-start | bytes 1572872 | tf_op jit(solution)/shard_map/ppermute | solution.py:633
  104.9 0.0 collective-permute-done.3.far_l
  105.0 0.0 collective-permute-start.5
  105.0 8.6 %collective-permute-done.5.near_r = bf16[512,256]{1,0:T(8,128)(2,1)S(1)} collective-permute-done((bf16[512,256]{1,0:T(8,128)(2,1)}, bf16[512,256]{1,0:T(8,128)(2,1)S(1)}, u32[]{:S(2)}, u32[]{:S(2)}) %collective-permute-start.5) | collective-permute-done | bytes 262176 | tf_op jit(solution)/shard_map/ppermute | solution.py:623
  113.6 0.0 collective-permute-start.4
  113.6 0.0 collective-permute-done.15.across_res
  113.6 1.0 collective-permute-start.6
  114.6 0.1 stack.61.place_ref
  114.7 0.1 add_bitcast_fusion.2
  114.7 6.7 %collective-permute-done.4.across_l = bf16[512,256]{1,0:T(8,128)(2,1)S(1)} collective-permute-done((bf16[512,256]{1,0:T(8,128)(2,1)S(1)}, bf16[512,256]{1,0:T(8,128)(2,1)S(1)}, u32[]{:S(2)}, u32[]{:S(2)}) %collective-permute-start.4) | collective-permute-done | bytes 262176 | tf_op jit(solution)/shard_map/ppermute | solution.py:623
  121.5 10.2 %project_norm.1 = (bf16[512,2048]{1,0:T(8,128)(2,1)S(1)}, bf16[16,2048]{1,0:T(8,128)(2,1)S(1)}) custom-call(s32[5]{0:T(128)S(1)} %stack.61.place_ref, f32[1,2048]{1,0:T(1,128)} %bitcast.28, bf16[512,256]{1,0:T(8,128)(2,1)S(1)} %collective-permute-done.1.near_l, bf16[512,256]{1,0:T(8,128)(2,1)S(1)} %collective-permute-done.2.far_r, ...), custom_call_target="tpu_custom_call" | custom-call | tf_op jit(solution)/shard_map/project_norm/pallas_call | solution.py:399
  131.8 10.3 %collective-permute-start.16 = (bf16[16,2048]{1,0:T(8,128)(2,1)S(1)}, bf16[16,2048]{1,0:T(8,128)(2,1)S(1)}, u32[]{:S(2)}, u32[]{:S(2)}) collective-permute-start(bf16[16,2048]{1,0:T(8,128)(2,1)S(1)} %get-tuple-element.57), channel_id=1, source_target_pairs={{0,4},{4,8},{8,12},{12,16},{16,20},{20,24},{24,28},{28,32},{32,36}... | collective-permute-start | bytes 196616 | tf_op jit(solution)/shard_map/ppermute | solution.py:642
  142.1 1.3 collective-permute-done.16.rim
  143.4 12.8 %widen.1 = (bf16[512,1408]{1,0:T(8,128)(2,1)S(1)}, bf16[2048,1408]{1,0:T(8,128)(2,1)S(1)}, bf16[256,512]{1,0:T(8,128)(2,1)S(1)}, bf16[256,512]{1,0:T(8,128)(2,1)S(1)}) custom-call(s32[2,2]{1,0:T(2,128)S(1)} %pad_add_fusion.1.sent_ref, bf16[3,1408]{1,0:T(4,128)(2,1)} %gate_t.1, bf16[3,1408]{1,0:T(4,128)(2,1)} %up_t.1, ...), custom_call_target="tpu_custom_call" | custom-call | tf_op jit(solution)/shard_map/widen/pallas_call | solution.py:512
  156.1 0.5 collective-permute-start.17
  156.6 1.1 collective-permute-start.18
  157.7 1.6 shrink_sent.1
  159.3 0.7 collective-permute-start.19
  160.0 1.4 collective-permute-start.20
  161.4 0.1 add_bitcast_fusion
  161.5 2.4 %shrink_held.1 = (f32[128,2048]{1,0:T(8,128)S(1)}, f32[128,1024]{1,0:T(8,128)S(1)}, f32[128,1024]{1,0:T(8,128)S(1)}) custom-call(s32[2,2]{1,0:T(2,128)S(1)} %pad_add_fusion.held_ref, bf16[512,1408]{1,0:T(8,128)(2,1)S(1)} %get-tuple-element.58.hid, bf16[2048,1408]{1,0:T(8,128)(2,1)S(1)} %get-tuple-element.59.down), custom_call_target="tpu_custom_call" | custom-call | tf_op jit(solution)/shard_map/shrink_held/pallas_call | solution.py:559
  163.8 0.7 collective-permute-done.17.once_l.l_1
  164.5 1.7 collective-permute-done.18.once_r.r_1
  166.2 0.1 round_sum.2
  166.2 1.2 collective-permute-start.21
  167.4 1.8 collective-permute-done.19.once_l.l_2
  169.3 2.5 %collective-permute-done.20.once_r.r_2 = bf16[256,512]{1,0:T(8,128)(2,1)S(1)} collective-permute-done((bf16[256,512]{1,0:T(8,128)(2,1)S(1)}, bf16[256,512]{1,0:T(8,128)(2,1)S(1)}, u32[]{:S(2)}, u32[]{:S(2)}) %collective-permute-start.20) | collective-permute-done | bytes 262176 | tf_op jit(solution)/shard_map/ppermute | solution.py:627
  171.8 0.1 round_sum.3
  171.9 1.2 collective-permute-start.23
  173.0 0.7 collective-permute-done.21.ll_1
  173.7 4.3 %collective-permute-done.23.ll_2 = bf16[128,512]{1,0:T(8,128)(2,1)S(1)} collective-permute-done((bf16[128,512]{1,0:T(8,128)(2,1)S(1)}, bf16[128,512]{1,0:T(8,128)(2,1)S(1)}, u32[]{:S(2)}, u32[]{:S(2)}) %collective-permute-start.23) | collective-permute-done | bytes 131104 | tf_op jit(solution)/shard_map/ppermute | solution.py:627
  178.0 0.4 collective-permute-done.24.rr_2
  178.4 2.1 %last_norm.1 = bf16[128,2048]{1,0:T(8,128)(2,1)} custom-call(s32[5]{0:T(128)S(1)} %stack.61.place_ref, f32[128,2048]{1,0:T(8,128)S(1)} %get-tuple-element.60.own, bf16[256,512]{1,0:T(8,128)(2,1)S(1)} %collective-permute-done.17.once_l.l_1, bf16[256,512]{1,0:T(8,128)(2,1)S(1)} %collective-permute-done.18.once_r.r_1, ...), custom_call_target="tpu_custom_call" | custom-call | tf_op jit(solution)/shard_map/last_norm/pallas_call | solution.py:608
  (23 shorter events, 0.1 us)
Async XLA Ops:
  6.5 136.8 %all-gather.2.cloned.1.call-start = ((), (), s32[]{:S(2)}) async-start(), calls=%async_computation.2 | async-start | bytes 17571840 | tf_op jit(solution)/shard_map/all_gather | solution.py:678
  10.3 23.9 %collective-permute-start.7 = (bf16[512,1024]{1,0:T(8,128)(2,1)S(1)}, bf16[512,1024]{1,0:T(8,128)(2,1)S(1)}, u32[]{:S(2)}, u32[]{:S(2)}) collective-permute-start(bf16[512,1024]{1,0:T(8,128)(2,1)S(1)} %constant_dynamic-slice_fusion), channel_id=1, source_target_pairs={{0,1},{1,0},{2,3},{3,2},{4,5},{5,4},{6,7},{7,6},{8,9},{9,8},{10,11... | collective-permute-start | bytes 3145736 | tf_op jit(solution)/shard_map/ppermute | solution.py:623
  12.5 24.8 %collective-permute-start.8 = (bf16[512,1024]{1,0:T(8,128)(2,1)S(1)}, bf16[512,1024]{1,0:T(8,128)(2,1)}, u32[]{:S(2)}, u32[]{:S(2)}) collective-permute-start(bf16[512,1024]{1,0:T(8,128)(2,1)S(1)} %constant_dynamic-slice_fusion), channel_id=1, source_target_pairs={{0,3},{3,0},{1,2},{2,1},{4,7},{7,4},{5,6},{6,5},{8,11},{11,8},{9,1... | collective-permute-start | bytes 3145736 | tf_op jit(solution)/shard_map/ppermute | solution.py:627
  14.4 5.0 %collective-permute-start = (bf16[8,768]{1,0:T(8,128)(2,1)S(1)}, bf16[8,768]{1,0:T(8,128)(2,1)S(1)}, u32[]{:S(2)}, u32[]{:S(2)}) collective-permute-start(bf16[8,768]{1,0:T(8,128)(2,1)S(1)} %rim.1), channel_id=1, source_target_pairs={{0,4},{4,8},{8,12},{12,16},{16,20},{20,24},{24,28},{28,32},{32,36}... | collective-permute-start | bytes 36872 | tf_op jit(solution)/shard_map/ppermute | solution.py:642
  34.2 57.2 %copy-start = (bf16[512,1024]{1,0:T(8,128)(2,1)}, bf16[512,1024]{1,0:T(8,128)(2,1)S(1)}, u32[]{:S(2)}) copy-start(bf16[512,1024]{1,0:T(8,128)(2,1)S(1)} %collective-permute-done.7.near_w) | copy-start | bytes 3145732
  38.5 54.2 %collective-permute-start.9 = (bf16[512,1024]{1,0:T(8,128)(2,1)}, bf16[512,1024]{1,0:T(8,128)(2,1)}, u32[]{:S(2)}, u32[]{:S(2)}) collective-permute-start(bf16[512,1024]{1,0:T(8,128)(2,1)} %broadcast_select_fusion), channel_id=1, source_target_pairs={{0,1},{1,0},{2,3},{3,2},{4,7},{7,4},{5,6},{6,5},{8,9},{9,8},{10,11... | collective-permute-start | bytes 3145736 | tf_op jit(solution)/shard_map/ppermute | solution.py:633
  40.6 25.7 %all-to-all-start = ((bf16[64,16,128]{2,1,0:T(8,128)(2,1)}), bf16[64,16,128]{2,1,0:T(8,128)(2,1)S(1)}, u32[]{:S(2)}, u32[]{:S(2)}) async-start(bf16[64,16,128]{2,1,0:T(8,128)(2,1)} %get-tuple-element.44), calls=%async_computation | async-start | bytes 524288 | tf_op jit(solution)/shard_map/all_to_all | solution.py:701
  53.2 35.4 %collective-permute-start.13 = (bf16[128,2048]{1,0:T(8,128)(2,1)}, bf16[128,2048]{1,0:T(8,128)(2,1)S(1)}, u32[]{:S(2)}, u32[]{:S(2)}) collective-permute-start(bf16[128,2048]{1,0:T(8,128)(2,1)} %own_res), channel_id=1, source_target_pairs={{0,1},{1,0},{2,3},{3,2},{4,5},{5,4},{6,7},{7,6},{8,9},{9,8},{10,11... | collective-permute-start | bytes 1572872 | tf_op jit(solution)/shard_map/ppermute | solution.py:623
  55.1 33.6 %collective-permute-start.14 = (bf16[128,2048]{1,0:T(8,128)(2,1)}, bf16[128,2048]{1,0:T(8,128)(2,1)S(1)}, u32[]{:S(2)}, u32[]{:S(2)}) collective-permute-start(bf16[128,2048]{1,0:T(8,128)(2,1)} %own_res), channel_id=1, source_target_pairs={{0,3},{3,0},{1,2},{2,1},{4,7},{7,4},{5,6},{6,5},{8,11},{11,8},{9,1... | collective-permute-start | bytes 1572872 | tf_op jit(solution)/shard_map/ppermute | solution.py:627
  86.9 8.2 %collective-permute-start.1 = (bf16[512,256]{1,0:T(8,128)(2,1)}, bf16[512,256]{1,0:T(8,128)(2,1)S(1)}, u32[]{:S(2)}, u32[]{:S(2)}) collective-permute-start(bf16[512,256]{1,0:T(8,128)(2,1)} %get-tuple-element.45.own_l), channel_id=1, source_target_pairs={{0,1},{1,0},{2,3},{3,2},{4,5},{5,4},{6,7},{7,6},{8,9},{9,8},{10,11... | collective-permute-start | bytes 786440 | tf_op jit(solution)/shard_map/ppermute | solution.py:623
  88.6 32.9 %copy-start.1 = (bf16[128,2048]{1,0:T(8,128)(2,1)}, bf16[128,2048]{1,0:T(8,128)(2,1)S(1)}, u32[]{:S(2)}) copy-start(bf16[128,2048]{1,0:T(8,128)(2,1)S(1)} %collective-permute-done.13.near_res) | copy-start | bytes 1572868
  88.6 16.3 %copy-start.2 = (bf16[128,2048]{1,0:T(8,128)(2,1)}, bf16[128,2048]{1,0:T(8,128)(2,1)S(1)}, u32[]{:S(2)}) copy-start(bf16[128,2048]{1,0:T(8,128)(2,1)S(1)} %collective-permute-done.14.far_res) | copy-start | bytes 1572868
  88.6 16.3 %collective-permute-start.3 = (bf16[512,256]{1,0:T(8,128)(2,1)}, bf16[512,256]{1,0:T(8,128)(2,1)S(1)}, u32[]{:S(2)}, u32[]{:S(2)}) collective-permute-start(bf16[512,256]{1,0:T(8,128)(2,1)} %get-tuple-element.45.own_l), channel_id=1, source_target_pairs={{0,3},{3,0},{1,2},{2,1},{4,7},{7,4},{5,6},{6,5},{8,11},{11,8},{9,1... | collective-permute-start | bytes 786440 | tf_op jit(solution)/shard_map/ppermute | solution.py:627
  90.6 12.4 %collective-permute-start.2 = (bf16[512,256]{1,0:T(8,128)(2,1)}, bf16[512,256]{1,0:T(8,128)(2,1)S(1)}, u32[]{:S(2)}, u32[]{:S(2)}) collective-permute-start(bf16[512,256]{1,0:T(8,128)(2,1)} %get-tuple-element.46.own_r), channel_id=1, source_target_pairs={{0,3},{3,0},{1,2},{2,1},{4,7},{7,4},{5,6},{6,5},{8,11},{11,8},{9,1... | collective-permute-start | bytes 786440 | tf_op jit(solution)/shard_map/ppermute | solution.py:627
  91.4 30.1 %collective-permute-start.10 = (bf16[512,1024]{1,0:T(8,128)(2,1)S(1)}, bf16[512,1024]{1,0:T(8,128)(2,1)}, u32[]{:S(2)}, u32[]{:S(2)}) collective-permute-start(bf16[512,1024]{1,0:T(8,128)(2,1)S(1)} %collective-permute-done.7.near_w), channel_id=1, source_target_pairs={{0,4},{4,0},{1,5},{5,1},{2,6},{6,2},{3,7},{7,3},{8,12},{12,8},{9,1... | collective-permute-start | bytes 3145736 | tf_op jit(solution)/shard_map/ppermute | solution.py:637
  92.7 28.8 %collective-permute-start.11 = (bf16[512,1024]{1,0:T(8,128)(2,1)}, bf16[512,1024]{1,0:T(8,128)(2,1)}, u32[]{:S(2)}, u32[]{:S(2)}) collective-permute-start(bf16[512,1024]{1,0:T(8,128)(2,1)} %collective-permute-done.8.far_w), channel_id=1, source_target_pairs={{0,4},{4,0},{1,5},{5,1},{2,6},{6,2},{3,7},{7,3},{8,12},{12,8},{9,1... | collective-permute-start | bytes 3145736 | tf_op jit(solution)/shard_map/ppermute | solution.py:637
  95.1 26.4 %collective-permute-start.12 = (bf16[512,1024]{1,0:T(8,128)(2,1)}, bf16[512,1024]{1,0:T(8,128)(2,1)}, u32[]{:S(2)}, u32[]{:S(2)}) collective-permute-start(bf16[512,1024]{1,0:T(8,128)(2,1)} %collective-permute-done.9.across_w), channel_id=1, source_target_pairs={{0,4},{4,0},{1,5},{5,1},{2,6},{6,2},{3,7},{7,3},{8,12},{12,8},{9,1... | collective-permute-start | bytes 3145736 | tf_op jit(solution)/shard_map/ppermute | solution.py:637
  103.0 10.6 %collective-permute-start.15 = (bf16[128,2048]{1,0:T(8,128)(2,1)S(1)}, bf16[128,2048]{1,0:T(8,128)(2,1)}, u32[]{:S(2)}, u32[]{:S(2)}) collective-permute-start(bf16[128,2048]{1,0:T(8,128)(2,1)S(1)} %broadcast_select_fusion.1), channel_id=1, source_target_pairs={{0,1},{1,0},{2,3},{3,2},{4,7},{7,4},{5,6},{6,5},{8,9},{9,8},{10,11... | collective-permute-start | bytes 1572872 | tf_op jit(solution)/shard_map/ppermute | solution.py:633
  104.9 16.6 %copy-start.3 = (bf16[512,256]{1,0:T(8,128)(2,1)}, bf16[512,256]{1,0:T(8,128)(2,1)S(1)}, u32[]{:S(2)}) copy-start(bf16[512,256]{1,0:T(8,128)(2,1)S(1)} %collective-permute-done.3.far_l) | copy-start | bytes 786436
  105.0 8.6 %collective-permute-start.5 = (bf16[512,256]{1,0:T(8,128)(2,1)}, bf16[512,256]{1,0:T(8,128)(2,1)S(1)}, u32[]{:S(2)}, u32[]{:S(2)}) collective-permute-start(bf16[512,256]{1,0:T(8,128)(2,1)} %get-tuple-element.46.own_r), channel_id=1, source_target_pairs={{0,1},{1,0},{2,3},{3,2},{4,5},{5,4},{6,7},{7,6},{8,9},{9,8},{10,11... | collective-permute-start | bytes 786440 | tf_op jit(solution)/shard_map/ppermute | solution.py:623
  113.6 7.9 %copy-start.4 = (bf16[512,256]{1,0:T(8,128)(2,1)}, bf16[512,256]{1,0:T(8,128)(2,1)S(1)}, u32[]{:S(2)}) copy-start(bf16[512,256]{1,0:T(8,128)(2,1)S(1)} %collective-permute-done.5.near_r) | copy-start | bytes 786436
  113.6 7.9 %collective-permute-start.4 = (bf16[512,256]{1,0:T(8,128)(2,1)S(1)}, bf16[512,256]{1,0:T(8,128)(2,1)S(1)}, u32[]{:S(2)}, u32[]{:S(2)}) collective-permute-start(bf16[512,256]{1,0:T(8,128)(2,1)S(1)} %collective-permute-done.3.far_l), channel_id=1, source_target_pairs={{0,1},{1,0},{2,3},{3,2},{4,5},{5,4},{6,7},{7,6},{8,9},{9,8},{10,11... | collective-permute-start | bytes 786440 | tf_op jit(solution)/shard_map/ppermute | solution.py:623
  113.6 7.9 %collective-permute-start.6 = (bf16[512,256]{1,0:T(8,128)(2,1)S(1)}, bf16[512,256]{1,0:T(8,128)(2,1)S(1)}, u32[]{:S(2)}, u32[]{:S(2)}) collective-permute-start(bf16[512,256]{1,0:T(8,128)(2,1)S(1)} %collective-permute-done.5.near_r), channel_id=1, source_target_pairs={{0,3},{3,0},{1,2},{2,1},{4,7},{7,4},{5,6},{6,5},{8,11},{11,8},{9,1... | collective-permute-start | bytes 786440 | tf_op jit(solution)/shard_map/ppermute | solution.py:627
  131.8 11.6 %collective-permute-start.16 = (bf16[16,2048]{1,0:T(8,128)(2,1)S(1)}, bf16[16,2048]{1,0:T(8,128)(2,1)S(1)}, u32[]{:S(2)}, u32[]{:S(2)}) collective-permute-start(bf16[16,2048]{1,0:T(8,128)(2,1)S(1)} %get-tuple-element.57), channel_id=1, source_target_pairs={{0,4},{4,8},{8,12},{12,16},{16,20},{20,24},{24,28},{28,32},{32,36}... | collective-permute-start | bytes 196616 | tf_op jit(solution)/shard_map/ppermute | solution.py:642
  156.1 8.4 %collective-permute-start.17 = (bf16[256,512]{1,0:T(8,128)(2,1)S(1)}, bf16[256,512]{1,0:T(8,128)(2,1)S(1)}, u32[]{:S(2)}, u32[]{:S(2)}) collective-permute-start(bf16[256,512]{1,0:T(8,128)(2,1)S(1)} %get-tuple-element.61), channel_id=1, source_target_pairs={{0,1},{1,0},{2,3},{3,2},{4,5},{5,4},{6,7},{7,6},{8,9},{9,8},{10,11... | collective-permute-start | bytes 786440 | tf_op jit(solution)/shard_map/ppermute | solution.py:623
  156.6 9.5 %collective-permute-start.18 = (bf16[256,512]{1,0:T(8,128)(2,1)S(1)}, bf16[256,512]{1,0:T(8,128)(2,1)S(1)}, u32[]{:S(2)}, u32[]{:S(2)}) collective-permute-start(bf16[256,512]{1,0:T(8,128)(2,1)S(1)} %get-tuple-element.62), channel_id=1, source_target_pairs={{0,3},{3,0},{1,2},{2,1},{4,7},{7,4},{5,6},{6,5},{8,11},{11,8},{9,1... | collective-permute-start | bytes 786440 | tf_op jit(solution)/shard_map/ppermute | solution.py:627
  159.3 10.0 %collective-permute-start.19 = (bf16[256,512]{1,0:T(8,128)(2,1)S(1)}, bf16[256,512]{1,0:T(8,128)(2,1)S(1)}, u32[]{:S(2)}, u32[]{:S(2)}) collective-permute-start(bf16[256,512]{1,0:T(8,128)(2,1)S(1)} %get-tuple-element.63), channel_id=1, source_target_pairs={{0,1},{1,0},{2,3},{3,2},{4,5},{5,4},{6,7},{7,6},{8,9},{9,8},{10,11... | collective-permute-start | bytes 786440 | tf_op jit(solution)/shard_map/ppermute | solution.py:623
  160.0 11.8 %collective-permute-start.20 = (bf16[256,512]{1,0:T(8,128)(2,1)S(1)}, bf16[256,512]{1,0:T(8,128)(2,1)S(1)}, u32[]{:S(2)}, u32[]{:S(2)}) collective-permute-start(bf16[256,512]{1,0:T(8,128)(2,1)S(1)} %get-tuple-element.64), channel_id=1, source_target_pairs={{0,3},{3,0},{1,2},{2,1},{4,7},{7,4},{5,6},{6,5},{8,11},{11,8},{9,1... | collective-permute-start | bytes 786440 | tf_op jit(solution)/shard_map/ppermute | solution.py:627
  166.2 7.5 %collective-permute-start.21 = (bf16[128,512]{1,0:T(8,128)(2,1)S(1)}, bf16[128,512]{1,0:T(8,128)(2,1)S(1)}, u32[]{:S(2)}, u32[]{:S(2)}) collective-permute-start(bf16[128,512]{1,0:T(8,128)(2,1)S(1)} %get-tuple-element.66), channel_id=1, source_target_pairs={{0,3},{3,0},{1,2},{2,1},{4,7},{7,4},{5,6},{6,5},{8,11},{11,8},{9,1... | collective-permute-start | bytes 393224 | tf_op jit(solution)/shard_map/ppermute | solution.py:627
  167.4 6.3 %collective-permute-start.22 = (bf16[128,512]{1,0:T(8,128)(2,1)S(1)}, bf16[128,512]{1,0:T(8,128)(2,1)S(1)}, u32[]{:S(2)}, u32[]{:S(2)}) collective-permute-start(bf16[128,512]{1,0:T(8,128)(2,1)S(1)} %get-tuple-element.67), channel_id=1, source_target_pairs={{0,1},{1,0},{2,3},{3,2},{4,5},{5,4},{6,7},{7,6},{8,9},{9,8},{10,11... | collective-permute-start | bytes 393224 | tf_op jit(solution)/shard_map/ppermute | solution.py:623
  171.9 6.2 %collective-permute-start.23 = (bf16[128,512]{1,0:T(8,128)(2,1)S(1)}, bf16[128,512]{1,0:T(8,128)(2,1)S(1)}, u32[]{:S(2)}, u32[]{:S(2)}) collective-permute-start(bf16[128,512]{1,0:T(8,128)(2,1)S(1)} %get-tuple-element.69), channel_id=1, source_target_pairs={{0,3},{3,0},{1,2},{2,1},{4,7},{7,4},{5,6},{6,5},{8,11},{11,8},{9,1... | collective-permute-start | bytes 393224 | tf_op jit(solution)/shard_map/ppermute | solution.py:627
  173.0 5.4 %collective-permute-start.24 = (bf16[128,512]{1,0:T(8,128)(2,1)S(1)}, bf16[128,512]{1,0:T(8,128)(2,1)S(1)}, u32[]{:S(2)}, u32[]{:S(2)}) collective-permute-start(bf16[128,512]{1,0:T(8,128)(2,1)S(1)} %get-tuple-element.70), channel_id=1, source_target_pairs={{0,1},{1,0},{2,3},{3,2},{4,5},{5,4},{6,7},{7,6},{8,9},{9,8},{10,11... | collective-permute-start | bytes 393224 | tf_op jit(solution)/shard_map/ppermute | solution.py:623
Sparse Core Ops, SparseCore 0:
  10.1 106.0 all-gather.1

commit v2 on v1

--- a/solution.py
+++ b/solution.py
@@ -123,6 +123,28 @@
         total = term if total is None else total + term
     pad[0:8, :] = pad[BLOCK : BLOCK + 8, :]
     return silu(total)
+
+
+def pack_kernel(gate_ref, up_ref, down_ref, out_ref, sems):
+    copies = [
+        pltpu.make_async_copy(part, out_ref.at[:, k * FFL : (k + 1) * FFL], sems.at[k])
+        for k, part in enumerate((gate_ref, up_ref, down_ref))
+    ]
+    for copy in copies:
+        copy.start()
+    for copy in copies:
+        copy.wait()
+
+
+def run_pack(gate, up, down):
+    return pl.pallas_call(
+        pack_kernel,
+        out_shape=away_out((gate.shape[0], 3 * FFL), BF16),
+        in_specs=[ANY] * 3,
+        out_specs=ANY,
+        scratch_shapes=[pltpu.SemaphoreType.DMA((3,))],
+        name="pack",
+    )(*away(gate, up, down))
 
 
 def rim_kernel(x_ref, b_ref, c_ref, out_ref):
@@ -477,6 +499,14 @@
             total = term if total is None else total + term
         return total
 
+    def finish(j):
+        at = j * 128
+        if not isinstance(j, int):
+            at = pl.multiple_of(at, 128)
+        hid[:, pl.ds(at, 128)] = (
+            silu(conv(gate_pad, gate_t, at)) * conv(up_pad, up_t, at)
+        ).astype(BF16)
+
     def tile(j, carry):
         for copy in wide_copies(j):
             copy.wait()
@@ -491,17 +521,15 @@
             for copy in downs:
                 copy.start()
 
-        at = pl.multiple_of(j * 128, 128)
+        finish(jnp.maximum(j - 1, 0))
         rows = jnp.concatenate([rim[...], normed[...]], axis=0)
         both = dot(rows, wide[j]).astype(BF16).astype(F32)
         gate_pad[...] = both[:, 0:128]
         up_pad[...] = both[:, 128:256]
-        hid[:, pl.ds(at, 128)] = (
-            silu(conv(gate_pad, gate_t, at)) * conv(up_pad, up_t, at)
-        ).astype(BF16)
         return carry
 
     lax.fori_loop(0, TILES, tile, 0)
+    finish(TILES - 1)
     for copy in downs:
         copy.wait()
     send_l[...] = dot_nt(two_quarters(hid, sent_ref, 0), down[0:STRIP, :]).astype(BF16)
@@ -676,7 +704,7 @@
     held = jnp.stack([jnp.stack([own, far]), jnp.stack([own, near])])
 
     weights = lax.all_gather(
-        jnp.concatenate([valve_matrix, widen_matrix, shrink_matrix.T], axis=1), SP, tiled=True
+        run_pack(valve_matrix, widen_matrix, shrink_matrix.T), SP, tiled=True
     )
 
     rim = run_rim(channel_feed_matrix, memory_feed_matrix, memory_query_matrix)

time: 189 us -> 196 us (1.037)
  Pallas kernels: 45.8 us -> 54.2 us
    pallas_call x0 -> x1, Pallas kernels: none -> 9.32 us  [run_pack(): pl.pallas_call(pack_kernel, out_shape=away_out((gate.shape[0], 3 * FFL),...]
  transfers between devices with their start and end apart: 27 -> 27, of which waited for: 16 -> 15; matrix products, arithmetic and copies ran while one was open for 1% -> 1% of each run, Pallas kernels for 17% -> 16%
where the time goes in v2:
time: 196 us; the launch traced here: 194 us
  Pallas kernels  54.2 us (28%)
  starting transfers between devices  54.1 us (28%)
  waiting for transfers between devices  52.1 us (27%)
  blocking collectives  16.9 us (9%)
  between operations  13.6 us (7%)
    ppermute x9, waiting for transfers between devices, with_near(): return lax.ppermute(part, 'tp', NEAR)  21.9 us
    ppermute x9, waiting for transfers between devices, with_far(): return lax.ppermute(part, 'tp', FAR)  18.8 us
    all_to_all x1, blocking collectives, shards(): entering = lax.all_to_all(prefix, SP, 0, 0, tiled=True)  16.9 us
    ppermute x2, starting transfers between devices, next_positions(): return lax.ppermute(shard, SP, [(i, i + 1) for i in range(count - 1)])  14.3 us
    ppermute x9, starting transfers between devices, with_far(): return lax.ppermute(part, 'tp', FAR)  14.2 us
    all_to_all x1, starting transfers between devices, shards(): received = lax.all_to_all(message, SP, 0, 0, tiled=True)  12.6 us
    pallas_call x1, Pallas kernels, run_widen(): pl.pallas_call(widen_kernel, out_shape=(close_out((ROWS, FFL), BF16), clo...  11.7 us
    pallas_call x1, Pallas kernels, run_project(): pl.pallas_call(project_kernel, out_shape=(close_out((ROWS, D), BF16), clo...  10.2 us
  transfers between devices with their start and end apart: 27, of which 15 were waited for; matrix products, arithmetic and copies ran while one was open for 1% of the time, Pallas kernels for 16%

profile of v2, /device:TPU:1, one launch (start us, length us, event | category | flops | bytes accessed | tf_op | source)
XLA Modules:
  0.0 193.7 jit_solution(798727141055836070)
XLA Ops:
  6.5 9.3 %pack.1 = bf16[32,4224]{1,0:T(8,128)(2,1)} custom-call(bf16[32,1408]{1,0:T(8,128)(2,1)} %gate_ref.1, bf16[32,1408]{1,0:T(8,128)(2,1)} %up_ref.1, bf16[32,1408]{1,0:T(8,128)(2,1)} %bitcast.22), custom_call_target="tpu_custom_call" | custom-call | tf_op jit(solution)/shard_map/pack/pallas_call | solution.py:140
  15.9 0.0 all-gather.2.cloned.1.call-update
  15.9 0.7 rim.1
  16.6 1.3 constant_dynamic-slice_fusion
  17.9 2.2 %collective-permute-start.7 = (bf16[512,1024]{1,0:T(8,128)(2,1)S(1)}, bf16[512,1024]{1,0:T(8,128)(2,1)S(1)}, u32[]{:S(2)}, u32[]{:S(2)}) collective-permute-start(bf16[512,1024]{1,0:T(8,128)(2,1)S(1)} %constant_dynamic-slice_fusion), channel_id=1, source_target_pairs={{0,1},{1,0},{2,3},{3,2},{4,5},{5,4},{6,7},{7,6},{8,9},{9,8},{10,11... | collective-permute-start | bytes 3145736 | tf_op jit(solution)/shard_map/ppermute | solution.py:651
  20.1 1.9 collective-permute-start.8
  22.0 4.2 %collective-permute-start = (bf16[8,768]{1,0:T(8,128)(2,1)S(1)}, bf16[8,768]{1,0:T(8,128)(2,1)S(1)}, u32[]{:S(2)}, u32[]{:S(2)}) collective-permute-start(bf16[8,768]{1,0:T(8,128)(2,1)S(1)} %rim.1), channel_id=1, source_target_pairs={{0,4},{4,8},{8,12},{12,16},{16,20},{20,24},{24,28},{28,32},{32,36}... | collective-permute-start | bytes 36872 | tf_op jit(solution)/shard_map/ppermute | solution.py:670
  26.3 0.8 collective-permute-done.rim_ref
  27.1 5.7 %local_state.1 = (bf16[512,512]{1,0:T(8,128)(2,1)}, bf16[512,128]{1,0:T(8,128)(2,1)}, bf16[3,128,512]{2,1,0:T(8,128)(2,1)}, bf16[64,16,128]{2,1,0:T(8,128)(2,1)}) custom-call(bf16[512,512]{1,0:T(8,128)(2,1)} %x_ref.3, bf16[512,128]{1,0:T(8,128)(2,1)} %b_ref.3, bf16[8,768]{1,0:T(8,128)(2,1)S(1)} %collective-permute-done.rim_ref, bf16[4,512]{1,0:T(4,128)(2,1)} %xt_ref.1, ...), custom_call_target="tpu_custom_call" | custom-call | tf_op jit(solution)/shard_map/local_state/pallas_call | solution.py:219
  32.7 6.7 %local_mixer.1 = (f32[512,512]{1,0:T(8,128)}, bf16[512,128]{1,0:T(8,128)(2,1)}, f32[512,8]{1,0:T(8,128)}) custom-call(bf16[512,512]{1,0:T(8,128)(2,1)} %get-tuple-element.38.x_ref, bf16[512,128]{1,0:T(8,128)(2,1)} %get-tuple-element.39.b_ref, bf16[3,128,512]{2,1,0:T(8,128)(2,1)} %get-tuple-element.40.state_ref, bf16[512,128]{1,0:T(8,128)(2,1)} %c_ref.3, ...), custom_call_target="tpu_custom_call" | custom-call | tf_op jit(solution)/shard_map/local_mixer/pallas_call | solution.py:280
  39.5 2.4 %collective-permute-done.7.near_w = bf16[512,1024]{1,0:T(8,128)(2,1)S(1)} collective-permute-done((bf16[512,1024]{1,0:T(8,128)(2,1)S(1)}, bf16[512,1024]{1,0:T(8,128)(2,1)S(1)}, u32[]{:S(2)}, u32[]{:S(2)}) %collective-permute-start.7) | collective-permute-done | bytes 1048608 | tf_op jit(solution)/shard_map/ppermute | solution.py:651
  41.8 3.1 %collective-permute-done.8.far_w = bf16[512,1024]{1,0:T(8,128)(2,1)} collective-permute-done((bf16[512,1024]{1,0:T(8,128)(2,1)S(1)}, bf16[512,1024]{1,0:T(8,128)(2,1)}, u32[]{:S(2)}, u32[]{:S(2)}) %collective-permute-start.8) | collective-permute-done | bytes 1048608 | tf_op jit(solution)/shard_map/ppermute | solution.py:655
  45.0 1.1 broadcast_select_fusion
  46.1 2.1 %collective-permute-start.9 = (bf16[512,1024]{1,0:T(8,128)(2,1)}, bf16[512,1024]{1,0:T(8,128)(2,1)}, u32[]{:S(2)}, u32[]{:S(2)}) collective-permute-start(bf16[512,1024]{1,0:T(8,128)(2,1)} %broadcast_select_fusion), channel_id=1, source_target_pairs={{0,1},{1,0},{2,3},{3,2},{4,7},{7,4},{5,6},{6,5},{8,9},{9,8},{10,11... | collective-permute-start | bytes 3145736 | tf_op jit(solution)/shard_map/ppermute | solution.py:661
  48.2 12.6 %all-to-all-start = ((bf16[64,16,128]{2,1,0:T(8,128)(2,1)}), bf16[64,16,128]{2,1,0:T(8,128)(2,1)S(1)}, u32[]{:S(2)}, u32[]{:S(2)}) async-start(bf16[64,16,128]{2,1,0:T(8,128)(2,1)} %get-tuple-element.44), calls=%async_computation | async-start | bytes 524288 | tf_op jit(solution)/shard_map/all_to_all | solution.py:729
  60.8 1.8 collective-permute-start.13
  62.7 1.9 collective-permute-start.14
  64.6 9.4 %all-to-all-done.in_ref = bf16[64,16,128]{2,1,0:T(8,128)(2,1)S(1)} async-done(((bf16[64,16,128]{2,1,0:T(8,128)(2,1)}), bf16[64,16,128]{2,1,0:T(8,128)(2,1)S(1)}, u32[]{:S(2)}, u32[]{:S(2)}) %all-to-all-start) | async-done | bytes 262176 | tf_op jit(solution)/shard_map/all_to_all | solution.py:729
  73.9 0.1 state_prefix.1
  74.1 16.9 %all_to_all.10.in_ref = bf16[64,8,128]{2,1,0:T(8,128)(2,1)S(1)} all-to-all(bf16[64,8,128]{2,1,0:T(8,128)(2,1)S(1)} %state_prefix.1), channel_id=1, replica_groups=mesh['sp_0'=8,'sp_1'=4,'sp_2'=2,'tp'=4] {'sp_0','sp_1','sp_2'}, dimensions={0} | all-to-all | bytes 262144 | tf_op jit(solution)/shard_map/all_to_all | solution.py:748
  91.0 3.6 %gate_norm.1 = (bf16[512,256]{1,0:T(8,128)(2,1)}, bf16[512,256]{1,0:T(8,128)(2,1)}) custom-call(f32[512,512]{1,0:T(8,128)} %get-tuple-element.41.y_ref, bf16[512,128]{1,0:T(8,128)(2,1)} %get-tuple-element.42.cact_ref, f32[512,8]{1,0:T(8,128)} %get-tuple-element.43.grow_ref, bf16[64,8,128]{2,1,0:T(8,128)(2,1)S(1)} %all_to_all.10.in_ref, ...), custom_call_target="tpu_custom_call" | custom-call | tf_op jit(solution)/shard_map/gate_norm/pallas_call | solution.py:339
  94.6 1.5 collective-permute-start.1
  96.2 0.0 collective-permute-done.13.near_res
  96.2 0.0 collective-permute-done.14.far_res
  96.2 1.9 collective-permute-start.3
  98.1 0.8 collective-permute-start.2
  99.0 1.0 collective-permute-start.10
  100.0 0.0 collective-permute-done.9.across_w
  100.0 0.1 collective-permute-start.11
  100.1 2.5 %collective-permute-done.1.near_l = bf16[512,256]{1,0:T(8,128)(2,1)S(1)} collective-permute-done((bf16[512,256]{1,0:T(8,128)(2,1)}, bf16[512,256]{1,0:T(8,128)(2,1)S(1)}, u32[]{:S(2)}, u32[]{:S(2)}) %collective-permute-start.1) | collective-permute-done | bytes 262176 | tf_op jit(solution)/shard_map/ppermute | solution.py:651
  102.6 1.0 collective-permute-start.12
  103.6 0.1 broadcast_select_fusion.1
  103.7 7.1 %collective-permute-done.2.far_r = bf16[512,256]{1,0:T(8,128)(2,1)S(1)} collective-permute-done((bf16[512,256]{1,0:T(8,128)(2,1)}, bf16[512,256]{1,0:T(8,128)(2,1)S(1)}, u32[]{:S(2)}, u32[]{:S(2)}) %collective-permute-start.2) | collective-permute-done | bytes 262176 | tf_op jit(solution)/shard_map/ppermute | solution.py:655
  110.8 1.8 collective-permute-start.15
  112.6 0.0 collective-permute-start.5
  112.7 8.6 %collective-permute-done.5.near_r = bf16[512,256]{1,0:T(8,128)(2,1)S(1)} collective-permute-done((bf16[512,256]{1,0:T(8,128)(2,1)}, bf16[512,256]{1,0:T(8,128)(2,1)S(1)}, u32[]{:S(2)}, u32[]{:S(2)}) %collective-permute-start.5) | collective-permute-done | bytes 262176 | tf_op jit(solution)/shard_map/ppermute | solution.py:651
  121.3 0.0 collective-permute-start.4
  121.3 1.0 collective-permute-start.6
  122.3 0.1 stack.61.place_ref
  122.4 0.1 add_bitcast_fusion.2
  122.4 6.5 %collective-permute-done.4.across_l = bf16[512,256]{1,0:T(8,128)(2,1)S(1)} collective-permute-done((bf16[512,256]{1,0:T(8,128)(2,1)S(1)}, bf16[512,256]{1,0:T(8,128)(2,1)S(1)}, u32[]{:S(2)}, u32[]{:S(2)}) %collective-permute-start.4) | collective-permute-done | bytes 262176 | tf_op jit(solution)/shard_map/ppermute | solution.py:651
  129.0 0.0 collective-permute-done.10.near_x
  129.0 10.2 %project_norm.1 = (bf16[512,2048]{1,0:T(8,128)(2,1)S(1)}, bf16[16,2048]{1,0:T(8,128)(2,1)S(1)}) custom-call(s32[5]{0:T(128)S(1)} %stack.61.place_ref, f32[1,2048]{1,0:T(1,128)} %bitcast.28, bf16[512,256]{1,0:T(8,128)(2,1)S(1)} %collective-permute-done.1.near_l, bf16[512,256]{1,0:T(8,128)(2,1)S(1)} %collective-permute-done.2.far_r, ...), custom_call_target="tpu_custom_call" | custom-call | tf_op jit(solution)/shard_map/project_norm/pallas_call | solution.py:421
  139.2 10.1 %collective-permute-start.16 = (bf16[16,2048]{1,0:T(8,128)(2,1)S(1)}, bf16[16,2048]{1,0:T(8,128)(2,1)S(1)}, u32[]{:S(2)}, u32[]{:S(2)}) collective-permute-start(bf16[16,2048]{1,0:T(8,128)(2,1)S(1)} %get-tuple-element.57), channel_id=1, source_target_pairs={{0,4},{4,8},{8,12},{12,16},{16,20},{20,24},{24,28},{28,32},{32,36}... | collective-permute-start | bytes 196616 | tf_op jit(solution)/shard_map/ppermute | solution.py:670
  149.4 1.3 collective-permute-done.16.rim
  150.7 11.7 %widen.1 = (bf16[512,1408]{1,0:T(8,128)(2,1)S(1)}, bf16[2048,1408]{1,0:T(8,128)(2,1)S(1)}, bf16[256,512]{1,0:T(8,128)(2,1)S(1)}, bf16[256,512]{1,0:T(8,128)(2,1)S(1)}) custom-call(s32[2,2]{1,0:T(2,128)S(1)} %pad_add_fusion.1.sent_ref, bf16[3,1408]{1,0:T(4,128)(2,1)} %gate_t.1, bf16[3,1408]{1,0:T(4,128)(2,1)} %up_t.1, ...), custom_call_target="tpu_custom_call" | custom-call | tf_op jit(solution)/shard_map/widen/pallas_call | solution.py:540
  162.4 0.5 collective-permute-start.17
  162.9 1.9 collective-permute-start.18
  164.8 1.6 shrink_sent.1
  166.3 0.7 collective-permute-start.19
  167.0 0.6 collective-permute-start.20
  167.6 0.1 add_bitcast_fusion
  167.7 2.4 %shrink_held.1 = (f32[128,2048]{1,0:T(8,128)S(1)}, f32[128,1024]{1,0:T(8,128)S(1)}, f32[128,1024]{1,0:T(8,128)S(1)}) custom-call(s32[2,2]{1,0:T(2,128)S(1)} %pad_add_fusion.held_ref, bf16[512,1408]{1,0:T(8,128)(2,1)S(1)} %get-tuple-element.58.hid, bf16[2048,1408]{1,0:T(8,128)(2,1)S(1)} %get-tuple-element.59.down), custom_call_target="tpu_custom_call" | custom-call | tf_op jit(solution)/shard_map/shrink_held/pallas_call | solution.py:587
  170.1 0.7 collective-permute-done.17.once_l.l_1
  170.8 1.7 collective-permute-done.18.once_r.r_1
  172.4 0.1 round_sum.2
  172.5 2.2 %collective-permute-start.21 = (bf16[128,512]{1,0:T(8,128)(2,1)S(1)}, bf16[128,512]{1,0:T(8,128)(2,1)S(1)}, u32[]{:S(2)}, u32[]{:S(2)}) collective-permute-start(bf16[128,512]{1,0:T(8,128)(2,1)S(1)} %get-tuple-element.66), channel_id=1, source_target_pairs={{0,3},{3,0},{1,2},{2,1},{4,7},{7,4},{5,6},{6,5},{8,11},{11,8},{9,1... | collective-permute-start | bytes 393224 | tf_op jit(solution)/shard_map/ppermute | solution.py:655
  174.7 0.9 collective-permute-done.19.once_l.l_2
  175.6 2.5 %collective-permute-done.20.once_r.r_2 = bf16[256,512]{1,0:T(8,128)(2,1)S(1)} collective-permute-done((bf16[256,512]{1,0:T(8,128)(2,1)S(1)}, bf16[256,512]{1,0:T(8,128)(2,1)S(1)}, u32[]{:S(2)}, u32[]{:S(2)}) %collective-permute-start.20) | collective-permute-done | bytes 262176 | tf_op jit(solution)/shard_map/ppermute | solution.py:655
  178.0 0.1 round_sum.3
  178.1 2.0 %collective-permute-start.23 = (bf16[128,512]{1,0:T(8,128)(2,1)S(1)}, bf16[128,512]{1,0:T(8,128)(2,1)S(1)}, u32[]{:S(2)}, u32[]{:S(2)}) collective-permute-start(bf16[128,512]{1,0:T(8,128)(2,1)S(1)} %get-tuple-element.69), channel_id=1, source_target_pairs={{0,3},{3,0},{1,2},{2,1},{4,7},{7,4},{5,6},{6,5},{8,11},{11,8},{9,1... | collective-permute-start | bytes 393224 | tf_op jit(solution)/shard_map/ppermute | solution.py:655
  180.1 4.4 %collective-permute-done.23.ll_2 = bf16[128,512]{1,0:T(8,128)(2,1)S(1)} collective-permute-done((bf16[128,512]{1,0:T(8,128)(2,1)S(1)}, bf16[128,512]{1,0:T(8,128)(2,1)S(1)}, u32[]{:S(2)}, u32[]{:S(2)}) %collective-permute-start.23) | collective-permute-done | bytes 131104 | tf_op jit(solution)/shard_map/ppermute | solution.py:655
  184.5 0.3 collective-permute-done.24.rr_2
  184.8 2.1 %last_norm.1 = bf16[128,2048]{1,0:T(8,128)(2,1)} custom-call(s32[5]{0:T(128)S(1)} %stack.61.place_ref, f32[128,2048]{1,0:T(8,128)S(1)} %get-tuple-element.60.own, bf16[256,512]{1,0:T(8,128)(2,1)S(1)} %collective-permute-done.17.once_l.l_1, bf16[256,512]{1,0:T(8,128)(2,1)S(1)} %collective-permute-done.18.once_r.r_1, ...), custom_call_target="tpu_custom_call" | custom-call | tf_op jit(solution)/shard_map/last_norm/pallas_call | solution.py:636
  (23 shorter events, 0.1 us)
Async XLA Ops:
  6.5 144.1 %all-gather.2.cloned.1.call-start = ((), (), s32[]{:S(2)}) async-start(), calls=%async_computation.2 | async-start | bytes 17571840 | tf_op jit(solution)/shard_map/all_gather | solution.py:706
  17.9 23.9 %collective-permute-start.7 = (bf16[512,1024]{1,0:T(8,128)(2,1)S(1)}, bf16[512,1024]{1,0:T(8,128)(2,1)S(1)}, u32[]{:S(2)}, u32[]{:S(2)}) collective-permute-start(bf16[512,1024]{1,0:T(8,128)(2,1)S(1)} %constant_dynamic-slice_fusion), channel_id=1, source_target_pairs={{0,1},{1,0},{2,3},{3,2},{4,5},{5,4},{6,7},{7,6},{8,9},{9,8},{10,11... | collective-permute-start | bytes 3145736 | tf_op jit(solution)/shard_map/ppermute | solution.py:651
  20.1 24.8 %collective-permute-start.8 = (bf16[512,1024]{1,0:T(8,128)(2,1)S(1)}, bf16[512,1024]{1,0:T(8,128)(2,1)}, u32[]{:S(2)}, u32[]{:S(2)}) collective-permute-start(bf16[512,1024]{1,0:T(8,128)(2,1)S(1)} %constant_dynamic-slice_fusion), channel_id=1, source_target_pairs={{0,3},{3,0},{1,2},{2,1},{4,7},{7,4},{5,6},{6,5},{8,11},{11,8},{9,1... | collective-permute-start | bytes 3145736 | tf_op jit(solution)/shard_map/ppermute | solution.py:655
  22.0 5.0 %collective-permute-start = (bf16[8,768]{1,0:T(8,128)(2,1)S(1)}, bf16[8,768]{1,0:T(8,128)(2,1)S(1)}, u32[]{:S(2)}, u32[]{:S(2)}) collective-permute-start(bf16[8,768]{1,0:T(8,128)(2,1)S(1)} %rim.1), channel_id=1, source_target_pairs={{0,4},{4,8},{8,12},{12,16},{16,20},{20,24},{24,28},{28,32},{32,36}... | collective-permute-start | bytes 36872 | tf_op jit(solution)/shard_map/ppermute | solution.py:670
  41.8 57.1 %copy-start = (bf16[512,1024]{1,0:T(8,128)(2,1)}, bf16[512,1024]{1,0:T(8,128)(2,1)S(1)}, u32[]{:S(2)}) copy-start(bf16[512,1024]{1,0:T(8,128)(2,1)S(1)} %collective-permute-done.7.near_w) | copy-start | bytes 3145732
  46.1 53.9 %collective-permute-start.9 = (bf16[512,1024]{1,0:T(8,128)(2,1)}, bf16[512,1024]{1,0:T(8,128)(2,1)}, u32[]{:S(2)}, u32[]{:S(2)}) collective-permute-start(bf16[512,1024]{1,0:T(8,128)(2,1)} %broadcast_select_fusion), channel_id=1, source_target_pairs={{0,1},{1,0},{2,3},{3,2},{4,7},{7,4},{5,6},{6,5},{8,9},{9,8},{10,11... | collective-permute-start | bytes 3145736 | tf_op jit(solution)/shard_map/ppermute | solution.py:661
  48.2 25.7 %all-to-all-start = ((bf16[64,16,128]{2,1,0:T(8,128)(2,1)}), bf16[64,16,128]{2,1,0:T(8,128)(2,1)S(1)}, u32[]{:S(2)}, u32[]{:S(2)}) async-start(bf16[64,16,128]{2,1,0:T(8,128)(2,1)} %get-tuple-element.44), calls=%async_computation | async-start | bytes 524288 | tf_op jit(solution)/shard_map/all_to_all | solution.py:729
  60.8 35.3 %collective-permute-start.13 = (bf16[128,2048]{1,0:T(8,128)(2,1)}, bf16[128,2048]{1,0:T(8,128)(2,1)S(1)}, u32[]{:S(2)}, u32[]{:S(2)}) collective-permute-start(bf16[128,2048]{1,0:T(8,128)(2,1)} %own_res), channel_id=1, source_target_pairs={{0,1},{1,0},{2,3},{3,2},{4,5},{5,4},{6,7},{7,6},{8,9},{9,8},{10,11... | collective-permute-start | bytes 1572872 | tf_op jit(solution)/shard_map/ppermute | solution.py:651
  62.7 33.5 %collective-permute-start.14 = (bf16[128,2048]{1,0:T(8,128)(2,1)}, bf16[128,2048]{1,0:T(8,128)(2,1)S(1)}, u32[]{:S(2)}, u32[]{:S(2)}) collective-permute-start(bf16[128,2048]{1,0:T(8,128)(2,1)} %own_res), channel_id=1, source_target_pairs={{0,3},{3,0},{1,2},{2,1},{4,7},{7,4},{5,6},{6,5},{8,11},{11,8},{9,1... | collective-permute-start | bytes 1572872 | tf_op jit(solution)/shard_map/ppermute | solution.py:655
  94.6 8.0 %collective-permute-start.1 = (bf16[512,256]{1,0:T(8,128)(2,1)}, bf16[512,256]{1,0:T(8,128)(2,1)S(1)}, u32[]{:S(2)}, u32[]{:S(2)}) collective-permute-start(bf16[512,256]{1,0:T(8,128)(2,1)} %get-tuple-element.45.own_l), channel_id=1, source_target_pairs={{0,1},{1,0},{2,3},{3,2},{4,5},{5,4},{6,7},{7,6},{8,9},{9,8},{10,11... | collective-permute-start | bytes 786440 | tf_op jit(solution)/shard_map/ppermute | solution.py:651
  96.2 32.8 %copy-start.1 = (bf16[128,2048]{1,0:T(8,128)(2,1)}, bf16[128,2048]{1,0:T(8,128)(2,1)S(1)}, u32[]{:S(2)}) copy-start(bf16[128,2048]{1,0:T(8,128)(2,1)S(1)} %collective-permute-done.13.near_res) | copy-start | bytes 1572868
  96.2 16.5 %copy-start.2 = (bf16[128,2048]{1,0:T(8,128)(2,1)}, bf16[128,2048]{1,0:T(8,128)(2,1)S(1)}, u32[]{:S(2)}) copy-start(bf16[128,2048]{1,0:T(8,128)(2,1)S(1)} %collective-permute-done.14.far_res) | copy-start | bytes 1572868
  96.2 16.5 %collective-permute-start.3 = (bf16[512,256]{1,0:T(8,128)(2,1)}, bf16[512,256]{1,0:T(8,128)(2,1)S(1)}, u32[]{:S(2)}, u32[]{:S(2)}) collective-permute-start(bf16[512,256]{1,0:T(8,128)(2,1)} %get-tuple-element.45.own_l), channel_id=1, source_target_pairs={{0,3},{3,0},{1,2},{2,1},{4,7},{7,4},{5,6},{6,5},{8,11},{11,8},{9,1... | collective-permute-start | bytes 786440 | tf_op jit(solution)/shard_map/ppermute | solution.py:655
  98.1 12.7 %collective-permute-start.2 = (bf16[512,256]{1,0:T(8,128)(2,1)}, bf16[512,256]{1,0:T(8,128)(2,1)S(1)}, u32[]{:S(2)}, u32[]{:S(2)}) collective-permute-start(bf16[512,256]{1,0:T(8,128)(2,1)} %get-tuple-element.46.own_r), channel_id=1, source_target_pairs={{0,3},{3,0},{1,2},{2,1},{4,7},{7,4},{5,6},{6,5},{8,11},{11,8},{9,1... | collective-permute-start | bytes 786440 | tf_op jit(solution)/shard_map/ppermute | solution.py:655
  99.0 30.0 %collective-permute-start.10 = (bf16[512,1024]{1,0:T(8,128)(2,1)S(1)}, bf16[512,1024]{1,0:T(8,128)(2,1)}, u32[]{:S(2)}, u32[]{:S(2)}) collective-permute-start(bf16[512,1024]{1,0:T(8,128)(2,1)S(1)} %collective-permute-done.7.near_w), channel_id=1, source_target_pairs={{0,4},{4,0},{1,5},{5,1},{2,6},{6,2},{3,7},{7,3},{8,12},{12,8},{9,1... | collective-permute-start | bytes 3145736 | tf_op jit(solution)/shard_map/ppermute | solution.py:665
  100.0 29.0 %collective-permute-start.11 = (bf16[512,1024]{1,0:T(8,128)(2,1)}, bf16[512,1024]{1,0:T(8,128)(2,1)}, u32[]{:S(2)}, u32[]{:S(2)}) collective-permute-start(bf16[512,1024]{1,0:T(8,128)(2,1)} %collective-permute-done.8.far_w), channel_id=1, source_target_pairs={{0,4},{4,0},{1,5},{5,1},{2,6},{6,2},{3,7},{7,3},{8,12},{12,8},{9,1... | collective-permute-start | bytes 3145736 | tf_op jit(solution)/shard_map/ppermute | solution.py:665
  102.6 26.3 %collective-permute-start.12 = (bf16[512,1024]{1,0:T(8,128)(2,1)}, bf16[512,1024]{1,0:T(8,128)(2,1)}, u32[]{:S(2)}, u32[]{:S(2)}) collective-permute-start(bf16[512,1024]{1,0:T(8,128)(2,1)} %collective-permute-done.9.across_w), channel_id=1, source_target_pairs={{0,4},{4,0},{1,5},{5,1},{2,6},{6,2},{3,7},{7,3},{8,12},{12,8},{9,1... | collective-permute-start | bytes 3145736 | tf_op jit(solution)/shard_map/ppermute | solution.py:665
  110.8 10.5 %collective-permute-start.15 = (bf16[128,2048]{1,0:T(8,128)(2,1)S(1)}, bf16[128,2048]{1,0:T(8,128)(2,1)}, u32[]{:S(2)}, u32[]{:S(2)}) collective-permute-start(bf16[128,2048]{1,0:T(8,128)(2,1)S(1)} %broadcast_select_fusion.1), channel_id=1, source_target_pairs={{0,1},{1,0},{2,3},{3,2},{4,7},{7,4},{5,6},{6,5},{8,9},{9,8},{10,11... | collective-permute-start | bytes 1572872 | tf_op jit(solution)/shard_map/ppermute | solution.py:661
  112.6 16.4 %copy-start.3 = (bf16[512,256]{1,0:T(8,128)(2,1)}, bf16[512,256]{1,0:T(8,128)(2,1)S(1)}, u32[]{:S(2)}) copy-start(bf16[512,256]{1,0:T(8,128)(2,1)S(1)} %collective-permute-done.3.far_l) | copy-start | bytes 786436
  112.6 8.6 %collective-permute-start.5 = (bf16[512,256]{1,0:T(8,128)(2,1)}, bf16[512,256]{1,0:T(8,128)(2,1)S(1)}, u32[]{:S(2)}, u32[]{:S(2)}) collective-permute-start(bf16[512,256]{1,0:T(8,128)(2,1)} %get-tuple-element.46.own_r), channel_id=1, source_target_pairs={{0,1},{1,0},{2,3},{3,2},{4,5},{5,4},{6,7},{7,6},{8,9},{9,8},{10,11... | collective-permute-start | bytes 786440 | tf_op jit(solution)/shard_map/ppermute | solution.py:651
  121.3 7.7 %copy-start.4 = (bf16[512,256]{1,0:T(8,128)(2,1)}, bf16[512,256]{1,0:T(8,128)(2,1)S(1)}, u32[]{:S(2)}) copy-start(bf16[512,256]{1,0:T(8,128)(2,1)S(1)} %collective-permute-done.5.near_r) | copy-start | bytes 786436
  121.3 7.7 %collective-permute-start.4 = (bf16[512,256]{1,0:T(8,128)(2,1)S(1)}, bf16[512,256]{1,0:T(8,128)(2,1)S(1)}, u32[]{:S(2)}, u32[]{:S(2)}) collective-permute-start(bf16[512,256]{1,0:T(8,128)(2,1)S(1)} %collective-permute-done.3.far_l), channel_id=1, source_target_pairs={{0,1},{1,0},{2,3},{3,2},{4,5},{5,4},{6,7},{7,6},{8,9},{9,8},{10,11... | collective-permute-start | bytes 786440 | tf_op jit(solution)/shard_map/ppermute | solution.py:651
  121.3 7.7 %collective-permute-start.6 = (bf16[512,256]{1,0:T(8,128)(2,1)S(1)}, bf16[512,256]{1,0:T(8,128)(2,1)S(1)}, u32[]{:S(2)}, u32[]{:S(2)}) collective-permute-start(bf16[512,256]{1,0:T(8,128)(2,1)S(1)} %collective-permute-done.5.near_r), channel_id=1, source_target_pairs={{0,3},{3,0},{1,2},{2,1},{4,7},{7,4},{5,6},{6,5},{8,11},{11,8},{9,1... | collective-permute-start | bytes 786440 | tf_op jit(solution)/shard_map/ppermute | solution.py:655
  139.2 11.4 %collective-permute-start.16 = (bf16[16,2048]{1,0:T(8,128)(2,1)S(1)}, bf16[16,2048]{1,0:T(8,128)(2,1)S(1)}, u32[]{:S(2)}, u32[]{:S(2)}) collective-permute-start(bf16[16,2048]{1,0:T(8,128)(2,1)S(1)} %get-tuple-element.57), channel_id=1, source_target_pairs={{0,4},{4,8},{8,12},{12,16},{16,20},{20,24},{24,28},{28,32},{32,36}... | collective-permute-start | bytes 196616 | tf_op jit(solution)/shard_map/ppermute | solution.py:670
  162.4 8.4 %collective-permute-start.17 = (bf16[256,512]{1,0:T(8,128)(2,1)S(1)}, bf16[256,512]{1,0:T(8,128)(2,1)S(1)}, u32[]{:S(2)}, u32[]{:S(2)}) collective-permute-start(bf16[256,512]{1,0:T(8,128)(2,1)S(1)} %get-tuple-element.61), channel_id=1, source_target_pairs={{0,1},{1,0},{2,3},{3,2},{4,5},{5,4},{6,7},{7,6},{8,9},{9,8},{10,11... | collective-permute-start | bytes 786440 | tf_op jit(solution)/shard_map/ppermute | solution.py:651
  162.9 9.5 %collective-permute-start.18 = (bf16[256,512]{1,0:T(8,128)(2,1)S(1)}, bf16[256,512]{1,0:T(8,128)(2,1)S(1)}, u32[]{:S(2)}, u32[]{:S(2)}) collective-permute-start(bf16[256,512]{1,0:T(8,128)(2,1)S(1)} %get-tuple-element.62), channel_id=1, source_target_pairs={{0,3},{3,0},{1,2},{2,1},{4,7},{7,4},{5,6},{6,5},{8,11},{11,8},{9,1... | collective-permute-start | bytes 786440 | tf_op jit(solution)/shard_map/ppermute | solution.py:655
  166.3 9.2 %collective-permute-start.19 = (bf16[256,512]{1,0:T(8,128)(2,1)S(1)}, bf16[256,512]{1,0:T(8,128)(2,1)S(1)}, u32[]{:S(2)}, u32[]{:S(2)}) collective-permute-start(bf16[256,512]{1,0:T(8,128)(2,1)S(1)} %get-tuple-element.63), channel_id=1, source_target_pairs={{0,1},{1,0},{2,3},{3,2},{4,5},{5,4},{6,7},{7,6},{8,9},{9,8},{10,11... | collective-permute-start | bytes 786440 | tf_op jit(solution)/shard_map/ppermute | solution.py:651
  167.0 11.0 %collective-permute-start.20 = (bf16[256,512]{1,0:T(8,128)(2,1)S(1)}, bf16[256,512]{1,0:T(8,128)(2,1)S(1)}, u32[]{:S(2)}, u32[]{:S(2)}) collective-permute-start(bf16[256,512]{1,0:T(8,128)(2,1)S(1)} %get-tuple-element.64), channel_id=1, source_target_pairs={{0,3},{3,0},{1,2},{2,1},{4,7},{7,4},{5,6},{6,5},{8,11},{11,8},{9,1... | collective-permute-start | bytes 786440 | tf_op jit(solution)/shard_map/ppermute | solution.py:655
  172.5 7.6 %collective-permute-start.21 = (bf16[128,512]{1,0:T(8,128)(2,1)S(1)}, bf16[128,512]{1,0:T(8,128)(2,1)S(1)}, u32[]{:S(2)}, u32[]{:S(2)}) collective-permute-start(bf16[128,512]{1,0:T(8,128)(2,1)S(1)} %get-tuple-element.66), channel_id=1, source_target_pairs={{0,3},{3,0},{1,2},{2,1},{4,7},{7,4},{5,6},{6,5},{8,11},{11,8},{9,1... | collective-permute-start | bytes 393224 | tf_op jit(solution)/shard_map/ppermute | solution.py:655
  174.7 5.4 %collective-permute-start.22 = (bf16[128,512]{1,0:T(8,128)(2,1)S(1)}, bf16[128,512]{1,0:T(8,128)(2,1)S(1)}, u32[]{:S(2)}, u32[]{:S(2)}) collective-permute-start(bf16[128,512]{1,0:T(8,128)(2,1)S(1)} %get-tuple-element.67), channel_id=1, source_target_pairs={{0,1},{1,0},{2,3},{3,2},{4,5},{5,4},{6,7},{7,6},{8,9},{9,8},{10,11... | collective-permute-start | bytes 393224 | tf_op jit(solution)/shard_map/ppermute | solution.py:651
  178.1 6.4 %collective-permute-start.23 = (bf16[128,512]{1,0:T(8,128)(2,1)S(1)}, bf16[128,512]{1,0:T(8,128)(2,1)S(1)}, u32[]{:S(2)}, u32[]{:S(2)}) collective-permute-start(bf16[128,512]{1,0:T(8,128)(2,1)S(1)} %get-tuple-element.69), channel_id=1, source_target_pairs={{0,3},{3,0},{1,2},{2,1},{4,7},{7,4},{5,6},{6,5},{8,11},{11,8},{9,1... | collective-permute-start | bytes 393224 | tf_op jit(solution)/shard_map/ppermute | solution.py:655
  180.1 4.7 %collective-permute-start.24 = (bf16[128,512]{1,0:T(8,128)(2,1)S(1)}, bf16[128,512]{1,0:T(8,128)(2,1)S(1)}, u32[]{:S(2)}, u32[]{:S(2)}) collective-permute-start(bf16[128,512]{1,0:T(8,128)(2,1)S(1)} %get-tuple-element.70), channel_id=1, source_target_pairs={{0,1},{1,0},{2,3},{3,2},{4,5},{5,4},{6,7},{7,6},{8,9},{9,8},{10,11... | collective-permute-start | bytes 393224 | tf_op jit(solution)/shard_map/ppermute | solution.py:651
Sparse Core Ops, SparseCore 0:
  16.0 106.1 all-gather.1

commit v3 on v1

--- a/solution.py
+++ b/solution.py
@@ -477,6 +477,14 @@
             total = term if total is None else total + term
         return total
 
+    def finish(j):
+        at = j * 128
+        if not isinstance(j, int):
+            at = pl.multiple_of(at, 128)
+        hid[:, pl.ds(at, 128)] = (
+            silu(conv(gate_pad, gate_t, at)) * conv(up_pad, up_t, at)
+        ).astype(BF16)
+
     def tile(j, carry):
         for copy in wide_copies(j):
             copy.wait()
@@ -491,17 +499,15 @@
             for copy in downs:
                 copy.start()
 
-        at = pl.multiple_of(j * 128, 128)
+        finish(jnp.maximum(j - 1, 0))
         rows = jnp.concatenate([rim[...], normed[...]], axis=0)
         both = dot(rows, wide[j]).astype(BF16).astype(F32)
         gate_pad[...] = both[:, 0:128]
         up_pad[...] = both[:, 128:256]
-        hid[:, pl.ds(at, 128)] = (
-            silu(conv(gate_pad, gate_t, at)) * conv(up_pad, up_t, at)
-        ).astype(BF16)
         return carry
 
     lax.fori_loop(0, TILES, tile, 0)
+    finish(TILES - 1)
     for copy in downs:
         copy.wait()
     send_l[...] = dot_nt(two_quarters(hid, sent_ref, 0), down[0:STRIP, :]).astype(BF16)

time: 189 us -> 188 us (level)
  no operation moved by 1% of the time
where the time goes in v3:
time: 188 us; the launch traced here: 186 us
  waiting for transfers between devices  53.5 us (28%)
  starting transfers between devices  53.1 us (28%)
  Pallas kernels  44.8 us (24%)
  blocking collectives  16.9 us (9%)
  between operations  13.6 us (7%)
  other arithmetic  3.06 us (2%)
    ppermute x9, waiting for transfers between devices, with_near(): return lax.ppermute(part, 'tp', NEAR)  22.8 us
    ppermute x9, waiting for transfers between devices, with_far(): return lax.ppermute(part, 'tp', FAR)  19.2 us
    all_to_all x1, blocking collectives, shards(): entering = lax.all_to_all(prefix, SP, 0, 0, tiled=True)  16.9 us
    ppermute x2, starting transfers between devices, next_positions(): return lax.ppermute(shard, SP, [(i, i + 1) for i in range(count - 1)])  14.5 us
    all_to_all x1, starting transfers between devices, shards(): received = lax.all_to_all(message, SP, 0, 0, tiled=True)  12.6 us
    ppermute x9, starting transfers between devices, with_far(): return lax.ppermute(part, 'tp', FAR)  12.6 us
    pallas_call x1, Pallas kernels, run_widen(): pl.pallas_call(widen_kernel, out_shape=(close_out((ROWS, FFL), BF16), clo...  11.7 us
    pallas_call x1, Pallas kernels, run_project(): pl.pallas_call(project_kernel, out_shape=(close_out((ROWS, D), BF16), clo...  10.2 us
  transfers between devices with their start and end apart: 27, of which 16 were waited for; matrix products, arithmetic and copies ran while one was open for 1% of the time, Pallas kernels for 17%

profile of v3, /device:TPU:1, one launch (start us, length us, event | category | flops | bytes accessed | tf_op | source)
XLA Modules:
  0.0 186.3 jit_solution(8845563665357016002)
XLA Ops:
  6.5 1.7 pad_maximum_fusion
  8.3 0.0 all-gather.2.cloned.1.call-update
  8.3 0.7 rim.1
  9.0 1.3 constant_dynamic-slice_fusion
  10.3 2.2 %collective-permute-start.7 = (bf16[512,1024]{1,0:T(8,128)(2,1)S(1)}, bf16[512,1024]{1,0:T(8,128)(2,1)S(1)}, u32[]{:S(2)}, u32[]{:S(2)}) collective-permute-start(bf16[512,1024]{1,0:T(8,128)(2,1)S(1)} %constant_dynamic-slice_fusion), channel_id=1, source_target_pairs={{0,1},{1,0},{2,3},{3,2},{4,5},{5,4},{6,7},{7,6},{8,9},{9,8},{10,11... | collective-permute-start | bytes 3145736 | tf_op jit(solution)/shard_map/ppermute | solution.py:629
  12.5 1.9 %collective-permute-start.8 = (bf16[512,1024]{1,0:T(8,128)(2,1)S(1)}, bf16[512,1024]{1,0:T(8,128)(2,1)}, u32[]{:S(2)}, u32[]{:S(2)}) collective-permute-start(bf16[512,1024]{1,0:T(8,128)(2,1)S(1)} %constant_dynamic-slice_fusion), channel_id=1, source_target_pairs={{0,3},{3,0},{1,2},{2,1},{4,7},{7,4},{5,6},{6,5},{8,11},{11,8},{9,1... | collective-permute-start | bytes 3145736 | tf_op jit(solution)/shard_map/ppermute | solution.py:633
  14.4 4.2 %collective-permute-start = (bf16[8,768]{1,0:T(8,128)(2,1)S(1)}, bf16[8,768]{1,0:T(8,128)(2,1)S(1)}, u32[]{:S(2)}, u32[]{:S(2)}) collective-permute-start(bf16[8,768]{1,0:T(8,128)(2,1)S(1)} %rim.1), channel_id=1, source_target_pairs={{0,4},{4,8},{8,12},{12,16},{16,20},{20,24},{24,28},{28,32},{32,36}... | collective-permute-start | bytes 36872 | tf_op jit(solution)/shard_map/ppermute | solution.py:648
  18.6 0.8 collective-permute-done.rim_ref
  19.5 5.7 %local_state.1 = (bf16[512,512]{1,0:T(8,128)(2,1)}, bf16[512,128]{1,0:T(8,128)(2,1)}, bf16[3,128,512]{2,1,0:T(8,128)(2,1)}, bf16[64,16,128]{2,1,0:T(8,128)(2,1)}) custom-call(bf16[512,512]{1,0:T(8,128)(2,1)} %x_ref.3, bf16[512,128]{1,0:T(8,128)(2,1)} %b_ref.3, bf16[8,768]{1,0:T(8,128)(2,1)S(1)} %collective-permute-done.rim_ref, bf16[4,512]{1,0:T(4,128)(2,1)} %xt_ref.1, ...), custom_call_target="tpu_custom_call" | custom-call | tf_op jit(solution)/shard_map/local_state/pallas_call | solution.py:197
  25.1 6.7 %local_mixer.1 = (f32[512,512]{1,0:T(8,128)}, bf16[512,128]{1,0:T(8,128)(2,1)}, f32[512,8]{1,0:T(8,128)}) custom-call(bf16[512,512]{1,0:T(8,128)(2,1)} %get-tuple-element.38.x_ref, bf16[512,128]{1,0:T(8,128)(2,1)} %get-tuple-element.39.b_ref, bf16[3,128,512]{2,1,0:T(8,128)(2,1)} %get-tuple-element.40.state_ref, bf16[512,128]{1,0:T(8,128)(2,1)} %c_ref.3, ...), custom_call_target="tpu_custom_call" | custom-call | tf_op jit(solution)/shard_map/local_mixer/pallas_call | solution.py:258
  31.8 2.4 %collective-permute-done.7.near_w = bf16[512,1024]{1,0:T(8,128)(2,1)S(1)} collective-permute-done((bf16[512,1024]{1,0:T(8,128)(2,1)S(1)}, bf16[512,1024]{1,0:T(8,128)(2,1)S(1)}, u32[]{:S(2)}, u32[]{:S(2)}) %collective-permute-start.7) | collective-permute-done | bytes 1048608 | tf_op jit(solution)/shard_map/ppermute | solution.py:629
  34.2 3.1 %collective-permute-done.8.far_w = bf16[512,1024]{1,0:T(8,128)(2,1)} collective-permute-done((bf16[512,1024]{1,0:T(8,128)(2,1)S(1)}, bf16[512,1024]{1,0:T(8,128)(2,1)}, u32[]{:S(2)}, u32[]{:S(2)}) %collective-permute-start.8) | collective-permute-done | bytes 1048608 | tf_op jit(solution)/shard_map/ppermute | solution.py:633
  37.3 1.1 broadcast_select_fusion
  38.5 2.1 %collective-permute-start.9 = (bf16[512,1024]{1,0:T(8,128)(2,1)}, bf16[512,1024]{1,0:T(8,128)(2,1)}, u32[]{:S(2)}, u32[]{:S(2)}) collective-permute-start(bf16[512,1024]{1,0:T(8,128)(2,1)} %broadcast_select_fusion), channel_id=1, source_target_pairs={{0,1},{1,0},{2,3},{3,2},{4,7},{7,4},{5,6},{6,5},{8,9},{9,8},{10,11... | collective-permute-start | bytes 3145736 | tf_op jit(solution)/shard_map/ppermute | solution.py:639
  40.6 12.6 %all-to-all-start = ((bf16[64,16,128]{2,1,0:T(8,128)(2,1)}), bf16[64,16,128]{2,1,0:T(8,128)(2,1)S(1)}, u32[]{:S(2)}, u32[]{:S(2)}) async-start(bf16[64,16,128]{2,1,0:T(8,128)(2,1)} %get-tuple-element.44), calls=%async_computation | async-start | bytes 524288 | tf_op jit(solution)/shard_map/all_to_all | solution.py:707
  53.2 1.8 collective-permute-start.13
  55.1 1.9 %collective-permute-start.14 = (bf16[128,2048]{1,0:T(8,128)(2,1)}, bf16[128,2048]{1,0:T(8,128)(2,1)S(1)}, u32[]{:S(2)}, u32[]{:S(2)}) collective-permute-start(bf16[128,2048]{1,0:T(8,128)(2,1)} %own_res), channel_id=1, source_target_pairs={{0,3},{3,0},{1,2},{2,1},{4,7},{7,4},{5,6},{6,5},{8,11},{11,8},{9,1... | collective-permute-start | bytes 1572872 | tf_op jit(solution)/shard_map/ppermute | solution.py:633
  57.0 9.4 %all-to-all-done.in_ref = bf16[64,16,128]{2,1,0:T(8,128)(2,1)S(1)} async-done(((bf16[64,16,128]{2,1,0:T(8,128)(2,1)}), bf16[64,16,128]{2,1,0:T(8,128)(2,1)S(1)}, u32[]{:S(2)}, u32[]{:S(2)}) %all-to-all-start) | async-done | bytes 262176 | tf_op jit(solution)/shard_map/all_to_all | solution.py:707
  66.3 0.1 state_prefix.1
  66.5 16.9 %all_to_all.10.in_ref = bf16[64,8,128]{2,1,0:T(8,128)(2,1)S(1)} all-to-all(bf16[64,8,128]{2,1,0:T(8,128)(2,1)S(1)} %state_prefix.1), channel_id=1, replica_groups=mesh['sp_0'=8,'sp_1'=4,'sp_2'=2,'tp'=4] {'sp_0','sp_1','sp_2'}, dimensions={0} | all-to-all | bytes 262144 | tf_op jit(solution)/shard_map/all_to_all | solution.py:726
  83.3 3.6 %gate_norm.1 = (bf16[512,256]{1,0:T(8,128)(2,1)}, bf16[512,256]{1,0:T(8,128)(2,1)}) custom-call(f32[512,512]{1,0:T(8,128)} %get-tuple-element.41.y_ref, bf16[512,128]{1,0:T(8,128)(2,1)} %get-tuple-element.42.cact_ref, f32[512,8]{1,0:T(8,128)} %get-tuple-element.43.grow_ref, bf16[64,8,128]{2,1,0:T(8,128)(2,1)S(1)} %all_to_all.10.in_ref, ...), custom_call_target="tpu_custom_call" | custom-call | tf_op jit(solution)/shard_map/gate_norm/pallas_call | solution.py:317
  86.9 1.7 collective-permute-start.1
  88.6 2.0 %collective-permute-start.3 = (bf16[512,256]{1,0:T(8,128)(2,1)}, bf16[512,256]{1,0:T(8,128)(2,1)S(1)}, u32[]{:S(2)}, u32[]{:S(2)}) collective-permute-start(bf16[512,256]{1,0:T(8,128)(2,1)} %get-tuple-element.45.own_l), channel_id=1, source_target_pairs={{0,3},{3,0},{1,2},{2,1},{4,7},{7,4},{5,6},{6,5},{8,11},{11,8},{9,1... | collective-permute-start | bytes 786440 | tf_op jit(solution)/shard_map/ppermute | solution.py:633
  90.6 0.8 collective-permute-start.2
  91.4 1.3 collective-permute-start.10
  92.7 0.0 collective-permute-done.9.across_w
  92.7 0.1 collective-permute-start.11
  92.8 2.4 %collective-permute-done.1.near_l = bf16[512,256]{1,0:T(8,128)(2,1)S(1)} collective-permute-done((bf16[512,256]{1,0:T(8,128)(2,1)}, bf16[512,256]{1,0:T(8,128)(2,1)S(1)}, u32[]{:S(2)}, u32[]{:S(2)}) %collective-permute-start.1) | collective-permute-done | bytes 262176 | tf_op jit(solution)/shard_map/ppermute | solution.py:629
  95.1 1.0 collective-permute-start.12
  96.1 0.1 broadcast_select_fusion.1
  96.2 6.9 %collective-permute-done.2.far_r = bf16[512,256]{1,0:T(8,128)(2,1)S(1)} collective-permute-done((bf16[512,256]{1,0:T(8,128)(2,1)}, bf16[512,256]{1,0:T(8,128)(2,1)S(1)}, u32[]{:S(2)}, u32[]{:S(2)}) %collective-permute-start.2) | collective-permute-done | bytes 262176 | tf_op jit(solution)/shard_map/ppermute | solution.py:633
  103.0 1.9 %collective-permute-start.15 = (bf16[128,2048]{1,0:T(8,128)(2,1)S(1)}, bf16[128,2048]{1,0:T(8,128)(2,1)}, u32[]{:S(2)}, u32[]{:S(2)}) collective-permute-start(bf16[128,2048]{1,0:T(8,128)(2,1)S(1)} %broadcast_select_fusion.1), channel_id=1, source_target_pairs={{0,1},{1,0},{2,3},{3,2},{4,7},{7,4},{5,6},{6,5},{8,9},{9,8},{10,11... | collective-permute-start | bytes 1572872 | tf_op jit(solution)/shard_map/ppermute | solution.py:639
  104.9 0.0 collective-permute-done.3.far_l
  105.0 0.0 collective-permute-start.5
  105.0 8.6 %collective-permute-done.5.near_r = bf16[512,256]{1,0:T(8,128)(2,1)S(1)} collective-permute-done((bf16[512,256]{1,0:T(8,128)(2,1)}, bf16[512,256]{1,0:T(8,128)(2,1)S(1)}, u32[]{:S(2)}, u32[]{:S(2)}) %collective-permute-start.5) | collective-permute-done | bytes 262176 | tf_op jit(solution)/shard_map/ppermute | solution.py:629
  113.6 0.0 collective-permute-start.4
  113.6 0.0 collective-permute-done.15.across_res
  113.6 1.0 collective-permute-start.6
  114.6 0.1 stack.61.place_ref
  114.7 0.1 add_bitcast_fusion.2
  114.7 6.7 %collective-permute-done.4.across_l = bf16[512,256]{1,0:T(8,128)(2,1)S(1)} collective-permute-done((bf16[512,256]{1,0:T(8,128)(2,1)S(1)}, bf16[512,256]{1,0:T(8,128)(2,1)S(1)}, u32[]{:S(2)}, u32[]{:S(2)}) %collective-permute-start.4) | collective-permute-done | bytes 262176 | tf_op jit(solution)/shard_map/ppermute | solution.py:629
  121.5 10.2 %project_norm.1 = (bf16[512,2048]{1,0:T(8,128)(2,1)S(1)}, bf16[16,2048]{1,0:T(8,128)(2,1)S(1)}) custom-call(s32[5]{0:T(128)S(1)} %stack.61.place_ref, f32[1,2048]{1,0:T(1,128)} %bitcast.28, bf16[512,256]{1,0:T(8,128)(2,1)S(1)} %collective-permute-done.1.near_l, bf16[512,256]{1,0:T(8,128)(2,1)S(1)} %collective-permute-done.2.far_r, ...), custom_call_target="tpu_custom_call" | custom-call | tf_op jit(solution)/shard_map/project_norm/pallas_call | solution.py:399
  131.8 10.3 %collective-permute-start.16 = (bf16[16,2048]{1,0:T(8,128)(2,1)S(1)}, bf16[16,2048]{1,0:T(8,128)(2,1)S(1)}, u32[]{:S(2)}, u32[]{:S(2)}) collective-permute-start(bf16[16,2048]{1,0:T(8,128)(2,1)S(1)} %get-tuple-element.57), channel_id=1, source_target_pairs={{0,4},{4,8},{8,12},{12,16},{16,20},{20,24},{24,28},{28,32},{32,36}... | collective-permute-start | bytes 196616 | tf_op jit(solution)/shard_map/ppermute | solution.py:648
  142.1 1.3 collective-permute-done.16.rim
  143.4 11.7 %widen.1 = (bf16[512,1408]{1,0:T(8,128)(2,1)S(1)}, bf16[2048,1408]{1,0:T(8,128)(2,1)S(1)}, bf16[256,512]{1,0:T(8,128)(2,1)S(1)}, bf16[256,512]{1,0:T(8,128)(2,1)S(1)}) custom-call(s32[2,2]{1,0:T(2,128)S(1)} %pad_add_fusion.1.sent_ref, bf16[3,1408]{1,0:T(4,128)(2,1)} %gate_t.1, bf16[3,1408]{1,0:T(4,128)(2,1)} %up_t.1, ...), custom_call_target="tpu_custom_call" | custom-call | tf_op jit(solution)/shard_map/widen/pallas_call | solution.py:518
  155.0 0.5 collective-permute-start.17
  155.6 1.1 collective-permute-start.18
  156.7 1.6 shrink_sent.1
  158.2 0.7 collective-permute-start.19
  158.9 1.4 collective-permute-start.20
  160.3 0.1 add_bitcast_fusion
  160.4 2.4 %shrink_held.1 = (f32[128,2048]{1,0:T(8,128)S(1)}, f32[128,1024]{1,0:T(8,128)S(1)}, f32[128,1024]{1,0:T(8,128)S(1)}) custom-call(s32[2,2]{1,0:T(2,128)S(1)} %pad_add_fusion.held_ref, bf16[512,1408]{1,0:T(8,128)(2,1)S(1)} %get-tuple-element.58.hid, bf16[2048,1408]{1,0:T(8,128)(2,1)S(1)} %get-tuple-element.59.down), custom_call_target="tpu_custom_call" | custom-call | tf_op jit(solution)/shard_map/shrink_held/pallas_call | solution.py:565
  162.8 0.7 collective-permute-done.17.once_l.l_1
  163.5 1.7 collective-permute-done.18.once_r.r_1
  165.1 0.1 round_sum.2
  165.2 1.4 collective-permute-start.21
  166.6 1.6 collective-permute-done.19.once_l.l_2
  168.2 2.5 %collective-permute-done.20.once_r.r_2 = bf16[256,512]{1,0:T(8,128)(2,1)S(1)} collective-permute-done((bf16[256,512]{1,0:T(8,128)(2,1)S(1)}, bf16[256,512]{1,0:T(8,128)(2,1)S(1)}, u32[]{:S(2)}, u32[]{:S(2)}) %collective-permute-start.20) | collective-permute-done | bytes 262176 | tf_op jit(solution)/shard_map/ppermute | solution.py:633
  170.7 0.1 round_sum.3
  170.8 1.2 collective-permute-start.23
  172.0 0.7 collective-permute-done.21.ll_1
  172.7 4.3 %collective-permute-done.23.ll_2 = bf16[128,512]{1,0:T(8,128)(2,1)S(1)} collective-permute-done((bf16[128,512]{1,0:T(8,128)(2,1)S(1)}, bf16[128,512]{1,0:T(8,128)(2,1)S(1)}, u32[]{:S(2)}, u32[]{:S(2)}) %collective-permute-start.23) | collective-permute-done | bytes 131104 | tf_op jit(solution)/shard_map/ppermute | solution.py:633
  177.0 0.4 collective-permute-done.24.rr_2
  177.4 2.1 %last_norm.1 = bf16[128,2048]{1,0:T(8,128)(2,1)} custom-call(s32[5]{0:T(128)S(1)} %stack.61.place_ref, f32[128,2048]{1,0:T(8,128)S(1)} %get-tuple-element.60.own, bf16[256,512]{1,0:T(8,128)(2,1)S(1)} %collective-permute-done.17.once_l.l_1, bf16[256,512]{1,0:T(8,128)(2,1)S(1)} %collective-permute-done.18.once_r.r_1, ...), custom_call_target="tpu_custom_call" | custom-call | tf_op jit(solution)/shard_map/last_norm/pallas_call | solution.py:614
  (23 shorter events, 0.1 us)
Async XLA Ops:
  6.5 136.8 %all-gather.2.cloned.1.call-start = ((), (), s32[]{:S(2)}) async-start(), calls=%async_computation.2 | async-start | bytes 17571840 | tf_op jit(solution)/shard_map/all_gather | solution.py:684
  10.3 23.9 %collective-permute-start.7 = (bf16[512,1024]{1,0:T(8,128)(2,1)S(1)}, bf16[512,1024]{1,0:T(8,128)(2,1)S(1)}, u32[]{:S(2)}, u32[]{:S(2)}) collective-permute-start(bf16[512,1024]{1,0:T(8,128)(2,1)S(1)} %constant_dynamic-slice_fusion), channel_id=1, source_target_pairs={{0,1},{1,0},{2,3},{3,2},{4,5},{5,4},{6,7},{7,6},{8,9},{9,8},{10,11... | collective-permute-start | bytes 3145736 | tf_op jit(solution)/shard_map/ppermute | solution.py:629
  12.5 24.8 %collective-permute-start.8 = (bf16[512,1024]{1,0:T(8,128)(2,1)S(1)}, bf16[512,1024]{1,0:T(8,128)(2,1)}, u32[]{:S(2)}, u32[]{:S(2)}) collective-permute-start(bf16[512,1024]{1,0:T(8,128)(2,1)S(1)} %constant_dynamic-slice_fusion), channel_id=1, source_target_pairs={{0,3},{3,0},{1,2},{2,1},{4,7},{7,4},{5,6},{6,5},{8,11},{11,8},{9,1... | collective-permute-start | bytes 3145736 | tf_op jit(solution)/shard_map/ppermute | solution.py:633
  14.4 5.0 %collective-permute-start = (bf16[8,768]{1,0:T(8,128)(2,1)S(1)}, bf16[8,768]{1,0:T(8,128)(2,1)S(1)}, u32[]{:S(2)}, u32[]{:S(2)}) collective-permute-start(bf16[8,768]{1,0:T(8,128)(2,1)S(1)} %rim.1), channel_id=1, source_target_pairs={{0,4},{4,8},{8,12},{12,16},{16,20},{20,24},{24,28},{28,32},{32,36}... | collective-permute-start | bytes 36872 | tf_op jit(solution)/shard_map/ppermute | solution.py:648
  34.2 57.2 %copy-start = (bf16[512,1024]{1,0:T(8,128)(2,1)}, bf16[512,1024]{1,0:T(8,128)(2,1)S(1)}, u32[]{:S(2)}) copy-start(bf16[512,1024]{1,0:T(8,128)(2,1)S(1)} %collective-permute-done.7.near_w) | copy-start | bytes 3145732
  38.5 54.2 %collective-permute-start.9 = (bf16[512,1024]{1,0:T(8,128)(2,1)}, bf16[512,1024]{1,0:T(8,128)(2,1)}, u32[]{:S(2)}, u32[]{:S(2)}) collective-permute-start(bf16[512,1024]{1,0:T(8,128)(2,1)} %broadcast_select_fusion), channel_id=1, source_target_pairs={{0,1},{1,0},{2,3},{3,2},{4,7},{7,4},{5,6},{6,5},{8,9},{9,8},{10,11... | collective-permute-start | bytes 3145736 | tf_op jit(solution)/shard_map/ppermute | solution.py:639
  40.6 25.7 %all-to-all-start = ((bf16[64,16,128]{2,1,0:T(8,128)(2,1)}), bf16[64,16,128]{2,1,0:T(8,128)(2,1)S(1)}, u32[]{:S(2)}, u32[]{:S(2)}) async-start(bf16[64,16,128]{2,1,0:T(8,128)(2,1)} %get-tuple-element.44), calls=%async_computation | async-start | bytes 524288 | tf_op jit(solution)/shard_map/all_to_all | solution.py:707
  53.2 35.4 %collective-permute-start.13 = (bf16[128,2048]{1,0:T(8,128)(2,1)}, bf16[128,2048]{1,0:T(8,128)(2,1)S(1)}, u32[]{:S(2)}, u32[]{:S(2)}) collective-permute-start(bf16[128,2048]{1,0:T(8,128)(2,1)} %own_res), channel_id=1, source_target_pairs={{0,1},{1,0},{2,3},{3,2},{4,5},{5,4},{6,7},{7,6},{8,9},{9,8},{10,11... | collective-permute-start | bytes 1572872 | tf_op jit(solution)/shard_map/ppermute | solution.py:629
  55.1 33.6 %collective-permute-start.14 = (bf16[128,2048]{1,0:T(8,128)(2,1)}, bf16[128,2048]{1,0:T(8,128)(2,1)S(1)}, u32[]{:S(2)}, u32[]{:S(2)}) collective-permute-start(bf16[128,2048]{1,0:T(8,128)(2,1)} %own_res), channel_id=1, source_target_pairs={{0,3},{3,0},{1,2},{2,1},{4,7},{7,4},{5,6},{6,5},{8,11},{11,8},{9,1... | collective-permute-start | bytes 1572872 | tf_op jit(solution)/shard_map/ppermute | solution.py:633
  86.9 8.2 %collective-permute-start.1 = (bf16[512,256]{1,0:T(8,128)(2,1)}, bf16[512,256]{1,0:T(8,128)(2,1)S(1)}, u32[]{:S(2)}, u32[]{:S(2)}) collective-permute-start(bf16[512,256]{1,0:T(8,128)(2,1)} %get-tuple-element.45.own_l), channel_id=1, source_target_pairs={{0,1},{1,0},{2,3},{3,2},{4,5},{5,4},{6,7},{7,6},{8,9},{9,8},{10,11... | collective-permute-start | bytes 786440 | tf_op jit(solution)/shard_map/ppermute | solution.py:629
  88.6 32.9 %copy-start.1 = (bf16[128,2048]{1,0:T(8,128)(2,1)}, bf16[128,2048]{1,0:T(8,128)(2,1)S(1)}, u32[]{:S(2)}) copy-start(bf16[128,2048]{1,0:T(8,128)(2,1)S(1)} %collective-permute-done.13.near_res) | copy-start | bytes 1572868
  88.6 16.3 %copy-start.2 = (bf16[128,2048]{1,0:T(8,128)(2,1)}, bf16[128,2048]{1,0:T(8,128)(2,1)S(1)}, u32[]{:S(2)}) copy-start(bf16[128,2048]{1,0:T(8,128)(2,1)S(1)} %collective-permute-done.14.far_res) | copy-start | bytes 1572868
  88.6 16.3 %collective-permute-start.3 = (bf16[512,256]{1,0:T(8,128)(2,1)}, bf16[512,256]{1,0:T(8,128)(2,1)S(1)}, u32[]{:S(2)}, u32[]{:S(2)}) collective-permute-start(bf16[512,256]{1,0:T(8,128)(2,1)} %get-tuple-element.45.own_l), channel_id=1, source_target_pairs={{0,3},{3,0},{1,2},{2,1},{4,7},{7,4},{5,6},{6,5},{8,11},{11,8},{9,1... | collective-permute-start | bytes 786440 | tf_op jit(solution)/shard_map/ppermute | solution.py:633
  90.6 12.4 %collective-permute-start.2 = (bf16[512,256]{1,0:T(8,128)(2,1)}, bf16[512,256]{1,0:T(8,128)(2,1)S(1)}, u32[]{:S(2)}, u32[]{:S(2)}) collective-permute-start(bf16[512,256]{1,0:T(8,128)(2,1)} %get-tuple-element.46.own_r), channel_id=1, source_target_pairs={{0,3},{3,0},{1,2},{2,1},{4,7},{7,4},{5,6},{6,5},{8,11},{11,8},{9,1... | collective-permute-start | bytes 786440 | tf_op jit(solution)/shard_map/ppermute | solution.py:633
  91.4 30.1 %collective-permute-start.10 = (bf16[512,1024]{1,0:T(8,128)(2,1)S(1)}, bf16[512,1024]{1,0:T(8,128)(2,1)}, u32[]{:S(2)}, u32[]{:S(2)}) collective-permute-start(bf16[512,1024]{1,0:T(8,128)(2,1)S(1)} %collective-permute-done.7.near_w), channel_id=1, source_target_pairs={{0,4},{4,0},{1,5},{5,1},{2,6},{6,2},{3,7},{7,3},{8,12},{12,8},{9,1... | collective-permute-start | bytes 3145736 | tf_op jit(solution)/shard_map/ppermute | solution.py:643
  92.7 28.8 %collective-permute-start.11 = (bf16[512,1024]{1,0:T(8,128)(2,1)}, bf16[512,1024]{1,0:T(8,128)(2,1)}, u32[]{:S(2)}, u32[]{:S(2)}) collective-permute-start(bf16[512,1024]{1,0:T(8,128)(2,1)} %collective-permute-done.8.far_w), channel_id=1, source_target_pairs={{0,4},{4,0},{1,5},{5,1},{2,6},{6,2},{3,7},{7,3},{8,12},{12,8},{9,1... | collective-permute-start | bytes 3145736 | tf_op jit(solution)/shard_map/ppermute | solution.py:643
  95.1 26.4 %collective-permute-start.12 = (bf16[512,1024]{1,0:T(8,128)(2,1)}, bf16[512,1024]{1,0:T(8,128)(2,1)}, u32[]{:S(2)}, u32[]{:S(2)}) collective-permute-start(bf16[512,1024]{1,0:T(8,128)(2,1)} %collective-permute-done.9.across_w), channel_id=1, source_target_pairs={{0,4},{4,0},{1,5},{5,1},{2,6},{6,2},{3,7},{7,3},{8,12},{12,8},{9,1... | collective-permute-start | bytes 3145736 | tf_op jit(solution)/shard_map/ppermute | solution.py:643
  103.0 10.6 %collective-permute-start.15 = (bf16[128,2048]{1,0:T(8,128)(2,1)S(1)}, bf16[128,2048]{1,0:T(8,128)(2,1)}, u32[]{:S(2)}, u32[]{:S(2)}) collective-permute-start(bf16[128,2048]{1,0:T(8,128)(2,1)S(1)} %broadcast_select_fusion.1), channel_id=1, source_target_pairs={{0,1},{1,0},{2,3},{3,2},{4,7},{7,4},{5,6},{6,5},{8,9},{9,8},{10,11... | collective-permute-start | bytes 1572872 | tf_op jit(solution)/shard_map/ppermute | solution.py:639
  104.9 16.6 %copy-start.3 = (bf16[512,256]{1,0:T(8,128)(2,1)}, bf16[512,256]{1,0:T(8,128)(2,1)S(1)}, u32[]{:S(2)}) copy-start(bf16[512,256]{1,0:T(8,128)(2,1)S(1)} %collective-permute-done.3.far_l) | copy-start | bytes 786436
  105.0 8.6 %collective-permute-start.5 = (bf16[512,256]{1,0:T(8,128)(2,1)}, bf16[512,256]{1,0:T(8,128)(2,1)S(1)}, u32[]{:S(2)}, u32[]{:S(2)}) collective-permute-start(bf16[512,256]{1,0:T(8,128)(2,1)} %get-tuple-element.46.own_r), channel_id=1, source_target_pairs={{0,1},{1,0},{2,3},{3,2},{4,5},{5,4},{6,7},{7,6},{8,9},{9,8},{10,11... | collective-permute-start | bytes 786440 | tf_op jit(solution)/shard_map/ppermute | solution.py:629
  113.6 7.9 %copy-start.4 = (bf16[512,256]{1,0:T(8,128)(2,1)}, bf16[512,256]{1,0:T(8,128)(2,1)S(1)}, u32[]{:S(2)}) copy-start(bf16[512,256]{1,0:T(8,128)(2,1)S(1)} %collective-permute-done.5.near_r) | copy-start | bytes 786436
  113.6 7.9 %collective-permute-start.4 = (bf16[512,256]{1,0:T(8,128)(2,1)S(1)}, bf16[512,256]{1,0:T(8,128)(2,1)S(1)}, u32[]{:S(2)}, u32[]{:S(2)}) collective-permute-start(bf16[512,256]{1,0:T(8,128)(2,1)S(1)} %collective-permute-done.3.far_l), channel_id=1, source_target_pairs={{0,1},{1,0},{2,3},{3,2},{4,5},{5,4},{6,7},{7,6},{8,9},{9,8},{10,11... | collective-permute-start | bytes 786440 | tf_op jit(solution)/shard_map/ppermute | solution.py:629
  113.6 7.9 %collective-permute-start.6 = (bf16[512,256]{1,0:T(8,128)(2,1)S(1)}, bf16[512,256]{1,0:T(8,128)(2,1)S(1)}, u32[]{:S(2)}, u32[]{:S(2)}) collective-permute-start(bf16[512,256]{1,0:T(8,128)(2,1)S(1)} %collective-permute-done.5.near_r), channel_id=1, source_target_pairs={{0,3},{3,0},{1,2},{2,1},{4,7},{7,4},{5,6},{6,5},{8,11},{11,8},{9,1... | collective-permute-start | bytes 786440 | tf_op jit(solution)/shard_map/ppermute | solution.py:633
  131.8 11.6 %collective-permute-start.16 = (bf16[16,2048]{1,0:T(8,128)(2,1)S(1)}, bf16[16,2048]{1,0:T(8,128)(2,1)S(1)}, u32[]{:S(2)}, u32[]{:S(2)}) collective-permute-start(bf16[16,2048]{1,0:T(8,128)(2,1)S(1)} %get-tuple-element.57), channel_id=1, source_target_pairs={{0,4},{4,8},{8,12},{12,16},{16,20},{20,24},{24,28},{28,32},{32,36}... | collective-permute-start | bytes 196616 | tf_op jit(solution)/shard_map/ppermute | solution.py:648
  155.0 8.4 %collective-permute-start.17 = (bf16[256,512]{1,0:T(8,128)(2,1)S(1)}, bf16[256,512]{1,0:T(8,128)(2,1)S(1)}, u32[]{:S(2)}, u32[]{:S(2)}) collective-permute-start(bf16[256,512]{1,0:T(8,128)(2,1)S(1)} %get-tuple-element.61), channel_id=1, source_target_pairs={{0,1},{1,0},{2,3},{3,2},{4,5},{5,4},{6,7},{7,6},{8,9},{9,8},{10,11... | collective-permute-start | bytes 786440 | tf_op jit(solution)/shard_map/ppermute | solution.py:629
  155.6 9.5 %collective-permute-start.18 = (bf16[256,512]{1,0:T(8,128)(2,1)S(1)}, bf16[256,512]{1,0:T(8,128)(2,1)S(1)}, u32[]{:S(2)}, u32[]{:S(2)}) collective-permute-start(bf16[256,512]{1,0:T(8,128)(2,1)S(1)} %get-tuple-element.62), channel_id=1, source_target_pairs={{0,3},{3,0},{1,2},{2,1},{4,7},{7,4},{5,6},{6,5},{8,11},{11,8},{9,1... | collective-permute-start | bytes 786440 | tf_op jit(solution)/shard_map/ppermute | solution.py:633
  158.2 10.0 %collective-permute-start.19 = (bf16[256,512]{1,0:T(8,128)(2,1)S(1)}, bf16[256,512]{1,0:T(8,128)(2,1)S(1)}, u32[]{:S(2)}, u32[]{:S(2)}) collective-permute-start(bf16[256,512]{1,0:T(8,128)(2,1)S(1)} %get-tuple-element.63), channel_id=1, source_target_pairs={{0,1},{1,0},{2,3},{3,2},{4,5},{5,4},{6,7},{7,6},{8,9},{9,8},{10,11... | collective-permute-start | bytes 786440 | tf_op jit(solution)/shard_map/ppermute | solution.py:629
  158.9 11.8 %collective-permute-start.20 = (bf16[256,512]{1,0:T(8,128)(2,1)S(1)}, bf16[256,512]{1,0:T(8,128)(2,1)S(1)}, u32[]{:S(2)}, u32[]{:S(2)}) collective-permute-start(bf16[256,512]{1,0:T(8,128)(2,1)S(1)} %get-tuple-element.64), channel_id=1, source_target_pairs={{0,3},{3,0},{1,2},{2,1},{4,7},{7,4},{5,6},{6,5},{8,11},{11,8},{9,1... | collective-permute-start | bytes 786440 | tf_op jit(solution)/shard_map/ppermute | solution.py:633
  165.2 7.5 %collective-permute-start.21 = (bf16[128,512]{1,0:T(8,128)(2,1)S(1)}, bf16[128,512]{1,0:T(8,128)(2,1)S(1)}, u32[]{:S(2)}, u32[]{:S(2)}) collective-permute-start(bf16[128,512]{1,0:T(8,128)(2,1)S(1)} %get-tuple-element.66), channel_id=1, source_target_pairs={{0,3},{3,0},{1,2},{2,1},{4,7},{7,4},{5,6},{6,5},{8,11},{11,8},{9,1... | collective-permute-start | bytes 393224 | tf_op jit(solution)/shard_map/ppermute | solution.py:633
  166.6 6.1 %collective-permute-start.22 = (bf16[128,512]{1,0:T(8,128)(2,1)S(1)}, bf16[128,512]{1,0:T(8,128)(2,1)S(1)}, u32[]{:S(2)}, u32[]{:S(2)}) collective-permute-start(bf16[128,512]{1,0:T(8,128)(2,1)S(1)} %get-tuple-element.67), channel_id=1, source_target_pairs={{0,1},{1,0},{2,3},{3,2},{4,5},{5,4},{6,7},{7,6},{8,9},{9,8},{10,11... | collective-permute-start | bytes 393224 | tf_op jit(solution)/shard_map/ppermute | solution.py:629
  170.8 6.2 %collective-permute-start.23 = (bf16[128,512]{1,0:T(8,128)(2,1)S(1)}, bf16[128,512]{1,0:T(8,128)(2,1)S(1)}, u32[]{:S(2)}, u32[]{:S(2)}) collective-permute-start(bf16[128,512]{1,0:T(8,128)(2,1)S(1)} %get-tuple-element.69), channel_id=1, source_target_pairs={{0,3},{3,0},{1,2},{2,1},{4,7},{7,4},{5,6},{6,5},{8,11},{11,8},{9,1... | collective-permute-start | bytes 393224 | tf_op jit(solution)/shard_map/ppermute | solution.py:633
  172.0 5.4 %collective-permute-start.24 = (bf16[128,512]{1,0:T(8,128)(2,1)S(1)}, bf16[128,512]{1,0:T(8,128)(2,1)S(1)}, u32[]{:S(2)}, u32[]{:S(2)}) collective-permute-start(bf16[128,512]{1,0:T(8,128)(2,1)S(1)} %get-tuple-element.70), channel_id=1, source_target_pairs={{0,1},{1,0},{2,3},{3,2},{4,5},{5,4},{6,7},{7,6},{8,9},{9,8},{10,11... | collective-permute-start | bytes 393224 | tf_op jit(solution)/shard_map/ppermute | solution.py:629
Sparse Core Ops, SparseCore 0:
  10.1 106.0 all-gather.1

commit v4 on v3

--- a/solution.py
+++ b/solution.py
@@ -443,6 +443,7 @@
 
 
 AHEAD = 4
+FIRST = 2
 STRIP = 512
 
 
@@ -465,7 +466,7 @@
         )
 
     downs = down_copies(w_ref, down, down_sems)
-    for j in range(AHEAD):
+    for j in range(FIRST):
         for copy in wide_copies(j):
             copy.start()
 
@@ -488,6 +489,12 @@
     def tile(j, carry):
         for copy in wide_copies(j):
             copy.wait()
+
+        @pl.when(j == 0)
+        def _():
+            for later in range(FIRST, AHEAD):
+                for copy in wide_copies(later):
+                    copy.start()
 
         @pl.when(j + AHEAD < TILES)
         def _():

time: 188 us -> 188 us (level)
  no operation moved by 1% of the time
where the time goes in v4:
time: 188 us; the launch traced here: 186 us
  waiting for transfers between devices  53.5 us (28%)
  starting transfers between devices  53.1 us (28%)
  Pallas kernels  44.8 us (24%)
  blocking collectives  16.9 us (9%)
  between operations  13.6 us (7%)
  other arithmetic  3.06 us (2%)
    ppermute x9, waiting for transfers between devices, with_near(): return lax.ppermute(part, 'tp', NEAR)  22.8 us
    ppermute x9, waiting for transfers between devices, with_far(): return lax.ppermute(part, 'tp', FAR)  19.2 us
    all_to_all x1, blocking collectives, shards(): entering = lax.all_to_all(prefix, SP, 0, 0, tiled=True)  16.9 us
    ppermute x2, starting transfers between devices, next_positions(): return lax.ppermute(shard, SP, [(i, i + 1) for i in range(count - 1)])  14.5 us
    all_to_all x1, starting transfers between devices, shards(): received = lax.all_to_all(message, SP, 0, 0, tiled=True)  12.6 us
    ppermute x9, starting transfers between devices, with_far(): return lax.ppermute(part, 'tp', FAR)  12.6 us
    pallas_call x1, Pallas kernels, run_widen(): pl.pallas_call(widen_kernel, out_shape=(close_out((ROWS, FFL), BF16), clo...  11.7 us
    pallas_call x1, Pallas kernels, run_project(): pl.pallas_call(project_kernel, out_shape=(close_out((ROWS, D), BF16), clo...  10.2 us
  transfers between devices with their start and end apart: 27, of which 16 were waited for; matrix products, arithmetic and copies ran while one was open for 1% of the time, Pallas kernels for 17%

profile of v4, /device:TPU:1, one launch (start us, length us, event | category | flops | bytes accessed | tf_op | source)
XLA Modules:
  0.0 186.3 jit_solution(2568571087681716308)
XLA Ops:
  6.5 1.7 pad_maximum_fusion
  8.3 0.0 all-gather.2.cloned.1.call-update
  8.3 0.7 rim.1
  9.0 1.3 constant_dynamic-slice_fusion
  10.3 2.2 %collective-permute-start.7 = (bf16[512,1024]{1,0:T(8,128)(2,1)S(1)}, bf16[512,1024]{1,0:T(8,128)(2,1)S(1)}, u32[]{:S(2)}, u32[]{:S(2)}) collective-permute-start(bf16[512,1024]{1,0:T(8,128)(2,1)S(1)} %constant_dynamic-slice_fusion), channel_id=1, source_target_pairs={{0,1},{1,0},{2,3},{3,2},{4,5},{5,4},{6,7},{7,6},{8,9},{9,8},{10,11... | collective-permute-start | bytes 3145736 | tf_op jit(solution)/shard_map/ppermute | solution.py:636
  12.5 1.9 %collective-permute-start.8 = (bf16[512,1024]{1,0:T(8,128)(2,1)S(1)}, bf16[512,1024]{1,0:T(8,128)(2,1)}, u32[]{:S(2)}, u32[]{:S(2)}) collective-permute-start(bf16[512,1024]{1,0:T(8,128)(2,1)S(1)} %constant_dynamic-slice_fusion), channel_id=1, source_target_pairs={{0,3},{3,0},{1,2},{2,1},{4,7},{7,4},{5,6},{6,5},{8,11},{11,8},{9,1... | collective-permute-start | bytes 3145736 | tf_op jit(solution)/shard_map/ppermute | solution.py:640
  14.4 4.2 %collective-permute-start = (bf16[8,768]{1,0:T(8,128)(2,1)S(1)}, bf16[8,768]{1,0:T(8,128)(2,1)S(1)}, u32[]{:S(2)}, u32[]{:S(2)}) collective-permute-start(bf16[8,768]{1,0:T(8,128)(2,1)S(1)} %rim.1), channel_id=1, source_target_pairs={{0,4},{4,8},{8,12},{12,16},{16,20},{20,24},{24,28},{28,32},{32,36}... | collective-permute-start | bytes 36872 | tf_op jit(solution)/shard_map/ppermute | solution.py:655
  18.6 0.8 collective-permute-done.rim_ref
  19.5 5.7 %local_state.1 = (bf16[512,512]{1,0:T(8,128)(2,1)}, bf16[512,128]{1,0:T(8,128)(2,1)}, bf16[3,128,512]{2,1,0:T(8,128)(2,1)}, bf16[64,16,128]{2,1,0:T(8,128)(2,1)}) custom-call(bf16[512,512]{1,0:T(8,128)(2,1)} %x_ref.3, bf16[512,128]{1,0:T(8,128)(2,1)} %b_ref.3, bf16[8,768]{1,0:T(8,128)(2,1)S(1)} %collective-permute-done.rim_ref, bf16[4,512]{1,0:T(4,128)(2,1)} %xt_ref.1, ...), custom_call_target="tpu_custom_call" | custom-call | tf_op jit(solution)/shard_map/local_state/pallas_call | solution.py:197
  25.1 6.7 %local_mixer.1 = (f32[512,512]{1,0:T(8,128)}, bf16[512,128]{1,0:T(8,128)(2,1)}, f32[512,8]{1,0:T(8,128)}) custom-call(bf16[512,512]{1,0:T(8,128)(2,1)} %get-tuple-element.38.x_ref, bf16[512,128]{1,0:T(8,128)(2,1)} %get-tuple-element.39.b_ref, bf16[3,128,512]{2,1,0:T(8,128)(2,1)} %get-tuple-element.40.state_ref, bf16[512,128]{1,0:T(8,128)(2,1)} %c_ref.3, ...), custom_call_target="tpu_custom_call" | custom-call | tf_op jit(solution)/shard_map/local_mixer/pallas_call | solution.py:258
  31.8 2.4 %collective-permute-done.7.near_w = bf16[512,1024]{1,0:T(8,128)(2,1)S(1)} collective-permute-done((bf16[512,1024]{1,0:T(8,128)(2,1)S(1)}, bf16[512,1024]{1,0:T(8,128)(2,1)S(1)}, u32[]{:S(2)}, u32[]{:S(2)}) %collective-permute-start.7) | collective-permute-done | bytes 1048608 | tf_op jit(solution)/shard_map/ppermute | solution.py:636
  34.2 3.1 %collective-permute-done.8.far_w = bf16[512,1024]{1,0:T(8,128)(2,1)} collective-permute-done((bf16[512,1024]{1,0:T(8,128)(2,1)S(1)}, bf16[512,1024]{1,0:T(8,128)(2,1)}, u32[]{:S(2)}, u32[]{:S(2)}) %collective-permute-start.8) | collective-permute-done | bytes 1048608 | tf_op jit(solution)/shard_map/ppermute | solution.py:640
  37.3 1.1 broadcast_select_fusion
  38.5 2.1 %collective-permute-start.9 = (bf16[512,1024]{1,0:T(8,128)(2,1)}, bf16[512,1024]{1,0:T(8,128)(2,1)}, u32[]{:S(2)}, u32[]{:S(2)}) collective-permute-start(bf16[512,1024]{1,0:T(8,128)(2,1)} %broadcast_select_fusion), channel_id=1, source_target_pairs={{0,1},{1,0},{2,3},{3,2},{4,7},{7,4},{5,6},{6,5},{8,9},{9,8},{10,11... | collective-permute-start | bytes 3145736 | tf_op jit(solution)/shard_map/ppermute | solution.py:646
  40.6 12.6 %all-to-all-start = ((bf16[64,16,128]{2,1,0:T(8,128)(2,1)}), bf16[64,16,128]{2,1,0:T(8,128)(2,1)S(1)}, u32[]{:S(2)}, u32[]{:S(2)}) async-start(bf16[64,16,128]{2,1,0:T(8,128)(2,1)} %get-tuple-element.44), calls=%async_computation | async-start | bytes 524288 | tf_op jit(solution)/shard_map/all_to_all | solution.py:714
  53.2 1.8 collective-permute-start.13
  55.1 1.9 %collective-permute-start.14 = (bf16[128,2048]{1,0:T(8,128)(2,1)}, bf16[128,2048]{1,0:T(8,128)(2,1)S(1)}, u32[]{:S(2)}, u32[]{:S(2)}) collective-permute-start(bf16[128,2048]{1,0:T(8,128)(2,1)} %own_res), channel_id=1, source_target_pairs={{0,3},{3,0},{1,2},{2,1},{4,7},{7,4},{5,6},{6,5},{8,11},{11,8},{9,1... | collective-permute-start | bytes 1572872 | tf_op jit(solution)/shard_map/ppermute | solution.py:640
  57.0 9.4 %all-to-all-done.in_ref = bf16[64,16,128]{2,1,0:T(8,128)(2,1)S(1)} async-done(((bf16[64,16,128]{2,1,0:T(8,128)(2,1)}), bf16[64,16,128]{2,1,0:T(8,128)(2,1)S(1)}, u32[]{:S(2)}, u32[]{:S(2)}) %all-to-all-start) | async-done | bytes 262176 | tf_op jit(solution)/shard_map/all_to_all | solution.py:714
  66.3 0.1 state_prefix.1
  66.5 16.9 %all_to_all.10.in_ref = bf16[64,8,128]{2,1,0:T(8,128)(2,1)S(1)} all-to-all(bf16[64,8,128]{2,1,0:T(8,128)(2,1)S(1)} %state_prefix.1), channel_id=1, replica_groups=mesh['sp_0'=8,'sp_1'=4,'sp_2'=2,'tp'=4] {'sp_0','sp_1','sp_2'}, dimensions={0} | all-to-all | bytes 262144 | tf_op jit(solution)/shard_map/all_to_all | solution.py:733
  83.3 3.6 %gate_norm.1 = (bf16[512,256]{1,0:T(8,128)(2,1)}, bf16[512,256]{1,0:T(8,128)(2,1)}) custom-call(f32[512,512]{1,0:T(8,128)} %get-tuple-element.41.y_ref, bf16[512,128]{1,0:T(8,128)(2,1)} %get-tuple-element.42.cact_ref, f32[512,8]{1,0:T(8,128)} %get-tuple-element.43.grow_ref, bf16[64,8,128]{2,1,0:T(8,128)(2,1)S(1)} %all_to_all.10.in_ref, ...), custom_call_target="tpu_custom_call" | custom-call | tf_op jit(solution)/shard_map/gate_norm/pallas_call | solution.py:317
  86.9 1.7 collective-permute-start.1
  88.6 2.0 %collective-permute-start.3 = (bf16[512,256]{1,0:T(8,128)(2,1)}, bf16[512,256]{1,0:T(8,128)(2,1)S(1)}, u32[]{:S(2)}, u32[]{:S(2)}) collective-permute-start(bf16[512,256]{1,0:T(8,128)(2,1)} %get-tuple-element.45.own_l), channel_id=1, source_target_pairs={{0,3},{3,0},{1,2},{2,1},{4,7},{7,4},{5,6},{6,5},{8,11},{11,8},{9,1... | collective-permute-start | bytes 786440 | tf_op jit(solution)/shard_map/ppermute | solution.py:640
  90.6 0.8 collective-permute-start.2
  91.4 1.3 collective-permute-start.10
  92.7 0.0 collective-permute-done.9.across_w
  92.7 0.1 collective-permute-start.11
  92.8 2.4 %collective-permute-done.1.near_l = bf16[512,256]{1,0:T(8,128)(2,1)S(1)} collective-permute-done((bf16[512,256]{1,0:T(8,128)(2,1)}, bf16[512,256]{1,0:T(8,128)(2,1)S(1)}, u32[]{:S(2)}, u32[]{:S(2)}) %collective-permute-start.1) | collective-permute-done | bytes 262176 | tf_op jit(solution)/shard_map/ppermute | solution.py:636
  95.1 1.0 collective-permute-start.12
  96.1 0.1 broadcast_select_fusion.1
  96.2 6.9 %collective-permute-done.2.far_r = bf16[512,256]{1,0:T(8,128)(2,1)S(1)} collective-permute-done((bf16[512,256]{1,0:T(8,128)(2,1)}, bf16[512,256]{1,0:T(8,128)(2,1)S(1)}, u32[]{:S(2)}, u32[]{:S(2)}) %collective-permute-start.2) | collective-permute-done | bytes 262176 | tf_op jit(solution)/shard_map/ppermute | solution.py:640
  103.0 1.9 %collective-permute-start.15 = (bf16[128,2048]{1,0:T(8,128)(2,1)S(1)}, bf16[128,2048]{1,0:T(8,128)(2,1)}, u32[]{:S(2)}, u32[]{:S(2)}) collective-permute-start(bf16[128,2048]{1,0:T(8,128)(2,1)S(1)} %broadcast_select_fusion.1), channel_id=1, source_target_pairs={{0,1},{1,0},{2,3},{3,2},{4,7},{7,4},{5,6},{6,5},{8,9},{9,8},{10,11... | collective-permute-start | bytes 1572872 | tf_op jit(solution)/shard_map/ppermute | solution.py:646
  104.9 0.0 collective-permute-done.3.far_l
  105.0 0.0 collective-permute-start.5
  105.0 8.6 %collective-permute-done.5.near_r = bf16[512,256]{1,0:T(8,128)(2,1)S(1)} collective-permute-done((bf16[512,256]{1,0:T(8,128)(2,1)}, bf16[512,256]{1,0:T(8,128)(2,1)S(1)}, u32[]{:S(2)}, u32[]{:S(2)}) %collective-permute-start.5) | collective-permute-done | bytes 262176 | tf_op jit(solution)/shard_map/ppermute | solution.py:636
  113.6 0.0 collective-permute-start.4
  113.6 0.0 collective-permute-done.15.across_res
  113.6 1.0 collective-permute-start.6
  114.6 0.1 stack.61.place_ref
  114.7 0.1 add_bitcast_fusion.2
  114.7 6.7 %collective-permute-done.4.across_l = bf16[512,256]{1,0:T(8,128)(2,1)S(1)} collective-permute-done((bf16[512,256]{1,0:T(8,128)(2,1)S(1)}, bf16[512,256]{1,0:T(8,128)(2,1)S(1)}, u32[]{:S(2)}, u32[]{:S(2)}) %collective-permute-start.4) | collective-permute-done | bytes 262176 | tf_op jit(solution)/shard_map/ppermute | solution.py:636
  121.5 10.2 %project_norm.1 = (bf16[512,2048]{1,0:T(8,128)(2,1)S(1)}, bf16[16,2048]{1,0:T(8,128)(2,1)S(1)}) custom-call(s32[5]{0:T(128)S(1)} %stack.61.place_ref, f32[1,2048]{1,0:T(1,128)} %bitcast.28, bf16[512,256]{1,0:T(8,128)(2,1)S(1)} %collective-permute-done.1.near_l, bf16[512,256]{1,0:T(8,128)(2,1)S(1)} %collective-permute-done.2.far_r, ...), custom_call_target="tpu_custom_call" | custom-call | tf_op jit(solution)/shard_map/project_norm/pallas_call | solution.py:399
  131.8 10.3 %collective-permute-start.16 = (bf16[16,2048]{1,0:T(8,128)(2,1)S(1)}, bf16[16,2048]{1,0:T(8,128)(2,1)S(1)}, u32[]{:S(2)}, u32[]{:S(2)}) collective-permute-start(bf16[16,2048]{1,0:T(8,128)(2,1)S(1)} %get-tuple-element.57), channel_id=1, source_target_pairs={{0,4},{4,8},{8,12},{12,16},{16,20},{20,24},{24,28},{28,32},{32,36}... | collective-permute-start | bytes 196616 | tf_op jit(solution)/shard_map/ppermute | solution.py:655
  142.1 1.3 collective-permute-done.16.rim
  143.4 11.7 %widen.1 = (bf16[512,1408]{1,0:T(8,128)(2,1)S(1)}, bf16[2048,1408]{1,0:T(8,128)(2,1)S(1)}, bf16[256,512]{1,0:T(8,128)(2,1)S(1)}, bf16[256,512]{1,0:T(8,128)(2,1)S(1)}) custom-call(s32[2,2]{1,0:T(2,128)S(1)} %pad_add_fusion.1.sent_ref, bf16[3,1408]{1,0:T(4,128)(2,1)} %gate_t.1, bf16[3,1408]{1,0:T(4,128)(2,1)} %up_t.1, ...), custom_call_target="tpu_custom_call" | custom-call | tf_op jit(solution)/shard_map/widen/pallas_call | solution.py:525
  155.1 0.5 collective-permute-start.17
  155.6 1.1 collective-permute-start.18
  156.7 1.6 shrink_sent.1
  158.2 0.7 collective-permute-start.19
  158.9 1.4 collective-permute-start.20
  160.3 0.1 add_bitcast_fusion
  160.4 2.4 %shrink_held.1 = (f32[128,2048]{1,0:T(8,128)S(1)}, f32[128,1024]{1,0:T(8,128)S(1)}, f32[128,1024]{1,0:T(8,128)S(1)}) custom-call(s32[2,2]{1,0:T(2,128)S(1)} %pad_add_fusion.held_ref, bf16[512,1408]{1,0:T(8,128)(2,1)S(1)} %get-tuple-element.58.hid, bf16[2048,1408]{1,0:T(8,128)(2,1)S(1)} %get-tuple-element.59.down), custom_call_target="tpu_custom_call" | custom-call | tf_op jit(solution)/shard_map/shrink_held/pallas_call | solution.py:572
  162.8 0.7 collective-permute-done.17.once_l.l_1
  163.5 1.7 collective-permute-done.18.once_r.r_1
  165.1 0.1 round_sum.2
  165.2 1.4 collective-permute-start.21
  166.6 1.6 collective-permute-done.19.once_l.l_2
  168.2 2.5 %collective-permute-done.20.once_r.r_2 = bf16[256,512]{1,0:T(8,128)(2,1)S(1)} collective-permute-done((bf16[256,512]{1,0:T(8,128)(2,1)S(1)}, bf16[256,512]{1,0:T(8,128)(2,1)S(1)}, u32[]{:S(2)}, u32[]{:S(2)}) %collective-permute-start.20) | collective-permute-done | bytes 262176 | tf_op jit(solution)/shard_map/ppermute | solution.py:640
  170.8 0.1 round_sum.3
  170.8 1.2 collective-permute-start.23
  172.0 0.7 collective-permute-done.21.ll_1
  172.7 4.3 %collective-permute-done.23.ll_2 = bf16[128,512]{1,0:T(8,128)(2,1)S(1)} collective-permute-done((bf16[128,512]{1,0:T(8,128)(2,1)S(1)}, bf16[128,512]{1,0:T(8,128)(2,1)S(1)}, u32[]{:S(2)}, u32[]{:S(2)}) %collective-permute-start.23) | collective-permute-done | bytes 131104 | tf_op jit(solution)/shard_map/ppermute | solution.py:640
  177.0 0.4 collective-permute-done.24.rr_2
  177.4 2.1 %last_norm.1 = bf16[128,2048]{1,0:T(8,128)(2,1)} custom-call(s32[5]{0:T(128)S(1)} %stack.61.place_ref, f32[128,2048]{1,0:T(8,128)S(1)} %get-tuple-element.60.own, bf16[256,512]{1,0:T(8,128)(2,1)S(1)} %collective-permute-done.17.once_l.l_1, bf16[256,512]{1,0:T(8,128)(2,1)S(1)} %collective-permute-done.18.once_r.r_1, ...), custom_call_target="tpu_custom_call" | custom-call | tf_op jit(solution)/shard_map/last_norm/pallas_call | solution.py:621
  (23 shorter events, 0.1 us)
Async XLA Ops:
  6.5 136.8 %all-gather.2.cloned.1.call-start = ((), (), s32[]{:S(2)}) async-start(), calls=%async_computation.2 | async-start | bytes 17571840 | tf_op jit(solution)/shard_map/all_gather | solution.py:691
  10.3 23.9 %collective-permute-start.7 = (bf16[512,1024]{1,0:T(8,128)(2,1)S(1)}, bf16[512,1024]{1,0:T(8,128)(2,1)S(1)}, u32[]{:S(2)}, u32[]{:S(2)}) collective-permute-start(bf16[512,1024]{1,0:T(8,128)(2,1)S(1)} %constant_dynamic-slice_fusion), channel_id=1, source_target_pairs={{0,1},{1,0},{2,3},{3,2},{4,5},{5,4},{6,7},{7,6},{8,9},{9,8},{10,11... | collective-permute-start | bytes 3145736 | tf_op jit(solution)/shard_map/ppermute | solution.py:636
  12.5 24.8 %collective-permute-start.8 = (bf16[512,1024]{1,0:T(8,128)(2,1)S(1)}, bf16[512,1024]{1,0:T(8,128)(2,1)}, u32[]{:S(2)}, u32[]{:S(2)}) collective-permute-start(bf16[512,1024]{1,0:T(8,128)(2,1)S(1)} %constant_dynamic-slice_fusion), channel_id=1, source_target_pairs={{0,3},{3,0},{1,2},{2,1},{4,7},{7,4},{5,6},{6,5},{8,11},{11,8},{9,1... | collective-permute-start | bytes 3145736 | tf_op jit(solution)/shard_map/ppermute | solution.py:640
  14.4 5.0 %collective-permute-start = (bf16[8,768]{1,0:T(8,128)(2,1)S(1)}, bf16[8,768]{1,0:T(8,128)(2,1)S(1)}, u32[]{:S(2)}, u32[]{:S(2)}) collective-permute-start(bf16[8,768]{1,0:T(8,128)(2,1)S(1)} %rim.1), channel_id=1, source_target_pairs={{0,4},{4,8},{8,12},{12,16},{16,20},{20,24},{24,28},{28,32},{32,36}... | collective-permute-start | bytes 36872 | tf_op jit(solution)/shard_map/ppermute | solution.py:655
  34.2 57.2 %copy-start = (bf16[512,1024]{1,0:T(8,128)(2,1)}, bf16[512,1024]{1,0:T(8,128)(2,1)S(1)}, u32[]{:S(2)}) copy-start(bf16[512,1024]{1,0:T(8,128)(2,1)S(1)} %collective-permute-done.7.near_w) | copy-start | bytes 3145732
  38.5 54.2 %collective-permute-start.9 = (bf16[512,1024]{1,0:T(8,128)(2,1)}, bf16[512,1024]{1,0:T(8,128)(2,1)}, u32[]{:S(2)}, u32[]{:S(2)}) collective-permute-start(bf16[512,1024]{1,0:T(8,128)(2,1)} %broadcast_select_fusion), channel_id=1, source_target_pairs={{0,1},{1,0},{2,3},{3,2},{4,7},{7,4},{5,6},{6,5},{8,9},{9,8},{10,11... | collective-permute-start | bytes 3145736 | tf_op jit(solution)/shard_map/ppermute | solution.py:646
  40.6 25.7 %all-to-all-start = ((bf16[64,16,128]{2,1,0:T(8,128)(2,1)}), bf16[64,16,128]{2,1,0:T(8,128)(2,1)S(1)}, u32[]{:S(2)}, u32[]{:S(2)}) async-start(bf16[64,16,128]{2,1,0:T(8,128)(2,1)} %get-tuple-element.44), calls=%async_computation | async-start | bytes 524288 | tf_op jit(solution)/shard_map/all_to_all | solution.py:714
  53.2 35.4 %collective-permute-start.13 = (bf16[128,2048]{1,0:T(8,128)(2,1)}, bf16[128,2048]{1,0:T(8,128)(2,1)S(1)}, u32[]{:S(2)}, u32[]{:S(2)}) collective-permute-start(bf16[128,2048]{1,0:T(8,128)(2,1)} %own_res), channel_id=1, source_target_pairs={{0,1},{1,0},{2,3},{3,2},{4,5},{5,4},{6,7},{7,6},{8,9},{9,8},{10,11... | collective-permute-start | bytes 1572872 | tf_op jit(solution)/shard_map/ppermute | solution.py:636
  55.1 33.6 %collective-permute-start.14 = (bf16[128,2048]{1,0:T(8,128)(2,1)}, bf16[128,2048]{1,0:T(8,128)(2,1)S(1)}, u32[]{:S(2)}, u32[]{:S(2)}) collective-permute-start(bf16[128,2048]{1,0:T(8,128)(2,1)} %own_res), channel_id=1, source_target_pairs={{0,3},{3,0},{1,2},{2,1},{4,7},{7,4},{5,6},{6,5},{8,11},{11,8},{9,1... | collective-permute-start | bytes 1572872 | tf_op jit(solution)/shard_map/ppermute | solution.py:640
  86.9 8.2 %collective-permute-start.1 = (bf16[512,256]{1,0:T(8,128)(2,1)}, bf16[512,256]{1,0:T(8,128)(2,1)S(1)}, u32[]{:S(2)}, u32[]{:S(2)}) collective-permute-start(bf16[512,256]{1,0:T(8,128)(2,1)} %get-tuple-element.45.own_l), channel_id=1, source_target_pairs={{0,1},{1,0},{2,3},{3,2},{4,5},{5,4},{6,7},{7,6},{8,9},{9,8},{10,11... | collective-permute-start | bytes 786440 | tf_op jit(solution)/shard_map/ppermute | solution.py:636
  88.6 32.9 %copy-start.1 = (bf16[128,2048]{1,0:T(8,128)(2,1)}, bf16[128,2048]{1,0:T(8,128)(2,1)S(1)}, u32[]{:S(2)}) copy-start(bf16[128,2048]{1,0:T(8,128)(2,1)S(1)} %collective-permute-done.13.near_res) | copy-start | bytes 1572868
  88.6 16.3 %copy-start.2 = (bf16[128,2048]{1,0:T(8,128)(2,1)}, bf16[128,2048]{1,0:T(8,128)(2,1)S(1)}, u32[]{:S(2)}) copy-start(bf16[128,2048]{1,0:T(8,128)(2,1)S(1)} %collective-permute-done.14.far_res) | copy-start | bytes 1572868
  88.6 16.3 %collective-permute-start.3 = (bf16[512,256]{1,0:T(8,128)(2,1)}, bf16[512,256]{1,0:T(8,128)(2,1)S(1)}, u32[]{:S(2)}, u32[]{:S(2)}) collective-permute-start(bf16[512,256]{1,0:T(8,128)(2,1)} %get-tuple-element.45.own_l), channel_id=1, source_target_pairs={{0,3},{3,0},{1,2},{2,1},{4,7},{7,4},{5,6},{6,5},{8,11},{11,8},{9,1... | collective-permute-start | bytes 786440 | tf_op jit(solution)/shard_map/ppermute | solution.py:640
  90.6 12.4 %collective-permute-start.2 = (bf16[512,256]{1,0:T(8,128)(2,1)}, bf16[512,256]{1,0:T(8,128)(2,1)S(1)}, u32[]{:S(2)}, u32[]{:S(2)}) collective-permute-start(bf16[512,256]{1,0:T(8,128)(2,1)} %get-tuple-element.46.own_r), channel_id=1, source_target_pairs={{0,3},{3,0},{1,2},{2,1},{4,7},{7,4},{5,6},{6,5},{8,11},{11,8},{9,1... | collective-permute-start | bytes 786440 | tf_op jit(solution)/shard_map/ppermute | solution.py:640
  91.4 30.1 %collective-permute-start.10 = (bf16[512,1024]{1,0:T(8,128)(2,1)S(1)}, bf16[512,1024]{1,0:T(8,128)(2,1)}, u32[]{:S(2)}, u32[]{:S(2)}) collective-permute-start(bf16[512,1024]{1,0:T(8,128)(2,1)S(1)} %collective-permute-done.7.near_w), channel_id=1, source_target_pairs={{0,4},{4,0},{1,5},{5,1},{2,6},{6,2},{3,7},{7,3},{8,12},{12,8},{9,1... | collective-permute-start | bytes 3145736 | tf_op jit(solution)/shard_map/ppermute | solution.py:650
  92.7 28.8 %collective-permute-start.11 = (bf16[512,1024]{1,0:T(8,128)(2,1)}, bf16[512,1024]{1,0:T(8,128)(2,1)}, u32[]{:S(2)}, u32[]{:S(2)}) collective-permute-start(bf16[512,1024]{1,0:T(8,128)(2,1)} %collective-permute-done.8.far_w), channel_id=1, source_target_pairs={{0,4},{4,0},{1,5},{5,1},{2,6},{6,2},{3,7},{7,3},{8,12},{12,8},{9,1... | collective-permute-start | bytes 3145736 | tf_op jit(solution)/shard_map/ppermute | solution.py:650
  95.1 26.4 %collective-permute-start.12 = (bf16[512,1024]{1,0:T(8,128)(2,1)}, bf16[512,1024]{1,0:T(8,128)(2,1)}, u32[]{:S(2)}, u32[]{:S(2)}) collective-permute-start(bf16[512,1024]{1,0:T(8,128)(2,1)} %collective-permute-done.9.across_w), channel_id=1, source_target_pairs={{0,4},{4,0},{1,5},{5,1},{2,6},{6,2},{3,7},{7,3},{8,12},{12,8},{9,1... | collective-permute-start | bytes 3145736 | tf_op jit(solution)/shard_map/ppermute | solution.py:650
  103.0 10.6 %collective-permute-start.15 = (bf16[128,2048]{1,0:T(8,128)(2,1)S(1)}, bf16[128,2048]{1,0:T(8,128)(2,1)}, u32[]{:S(2)}, u32[]{:S(2)}) collective-permute-start(bf16[128,2048]{1,0:T(8,128)(2,1)S(1)} %broadcast_select_fusion.1), channel_id=1, source_target_pairs={{0,1},{1,0},{2,3},{3,2},{4,7},{7,4},{5,6},{6,5},{8,9},{9,8},{10,11... | collective-permute-start | bytes 1572872 | tf_op jit(solution)/shard_map/ppermute | solution.py:646
  104.9 16.6 %copy-start.3 = (bf16[512,256]{1,0:T(8,128)(2,1)}, bf16[512,256]{1,0:T(8,128)(2,1)S(1)}, u32[]{:S(2)}) copy-start(bf16[512,256]{1,0:T(8,128)(2,1)S(1)} %collective-permute-done.3.far_l) | copy-start | bytes 786436
  105.0 8.6 %collective-permute-start.5 = (bf16[512,256]{1,0:T(8,128)(2,1)}, bf16[512,256]{1,0:T(8,128)(2,1)S(1)}, u32[]{:S(2)}, u32[]{:S(2)}) collective-permute-start(bf16[512,256]{1,0:T(8,128)(2,1)} %get-tuple-element.46.own_r), channel_id=1, source_target_pairs={{0,1},{1,0},{2,3},{3,2},{4,5},{5,4},{6,7},{7,6},{8,9},{9,8},{10,11... | collective-permute-start | bytes 786440 | tf_op jit(solution)/shard_map/ppermute | solution.py:636
  113.6 7.9 %copy-start.4 = (bf16[512,256]{1,0:T(8,128)(2,1)}, bf16[512,256]{1,0:T(8,128)(2,1)S(1)}, u32[]{:S(2)}) copy-start(bf16[512,256]{1,0:T(8,128)(2,1)S(1)} %collective-permute-done.5.near_r) | copy-start | bytes 786436
  113.6 7.9 %collective-permute-start.4 = (bf16[512,256]{1,0:T(8,128)(2,1)S(1)}, bf16[512,256]{1,0:T(8,128)(2,1)S(1)}, u32[]{:S(2)}, u32[]{:S(2)}) collective-permute-start(bf16[512,256]{1,0:T(8,128)(2,1)S(1)} %collective-permute-done.3.far_l), channel_id=1, source_target_pairs={{0,1},{1,0},{2,3},{3,2},{4,5},{5,4},{6,7},{7,6},{8,9},{9,8},{10,11... | collective-permute-start | bytes 786440 | tf_op jit(solution)/shard_map/ppermute | solution.py:636
  113.6 7.9 %collective-permute-start.6 = (bf16[512,256]{1,0:T(8,128)(2,1)S(1)}, bf16[512,256]{1,0:T(8,128)(2,1)S(1)}, u32[]{:S(2)}, u32[]{:S(2)}) collective-permute-start(bf16[512,256]{1,0:T(8,128)(2,1)S(1)} %collective-permute-done.5.near_r), channel_id=1, source_target_pairs={{0,3},{3,0},{1,2},{2,1},{4,7},{7,4},{5,6},{6,5},{8,11},{11,8},{9,1... | collective-permute-start | bytes 786440 | tf_op jit(solution)/shard_map/ppermute | solution.py:640
  131.8 11.6 %collective-permute-start.16 = (bf16[16,2048]{1,0:T(8,128)(2,1)S(1)}, bf16[16,2048]{1,0:T(8,128)(2,1)S(1)}, u32[]{:S(2)}, u32[]{:S(2)}) collective-permute-start(bf16[16,2048]{1,0:T(8,128)(2,1)S(1)} %get-tuple-element.57), channel_id=1, source_target_pairs={{0,4},{4,8},{8,12},{12,16},{16,20},{20,24},{24,28},{28,32},{32,36}... | collective-permute-start | bytes 196616 | tf_op jit(solution)/shard_map/ppermute | solution.py:655
  155.1 8.4 %collective-permute-start.17 = (bf16[256,512]{1,0:T(8,128)(2,1)S(1)}, bf16[256,512]{1,0:T(8,128)(2,1)S(1)}, u32[]{:S(2)}, u32[]{:S(2)}) collective-permute-start(bf16[256,512]{1,0:T(8,128)(2,1)S(1)} %get-tuple-element.61), channel_id=1, source_target_pairs={{0,1},{1,0},{2,3},{3,2},{4,5},{5,4},{6,7},{7,6},{8,9},{9,8},{10,11... | collective-permute-start | bytes 786440 | tf_op jit(solution)/shard_map/ppermute | solution.py:636
  155.6 9.5 %collective-permute-start.18 = (bf16[256,512]{1,0:T(8,128)(2,1)S(1)}, bf16[256,512]{1,0:T(8,128)(2,1)S(1)}, u32[]{:S(2)}, u32[]{:S(2)}) collective-permute-start(bf16[256,512]{1,0:T(8,128)(2,1)S(1)} %get-tuple-element.62), channel_id=1, source_target_pairs={{0,3},{3,0},{1,2},{2,1},{4,7},{7,4},{5,6},{6,5},{8,11},{11,8},{9,1... | collective-permute-start | bytes 786440 | tf_op jit(solution)/shard_map/ppermute | solution.py:640
  158.2 10.0 %collective-permute-start.19 = (bf16[256,512]{1,0:T(8,128)(2,1)S(1)}, bf16[256,512]{1,0:T(8,128)(2,1)S(1)}, u32[]{:S(2)}, u32[]{:S(2)}) collective-permute-start(bf16[256,512]{1,0:T(8,128)(2,1)S(1)} %get-tuple-element.63), channel_id=1, source_target_pairs={{0,1},{1,0},{2,3},{3,2},{4,5},{5,4},{6,7},{7,6},{8,9},{9,8},{10,11... | collective-permute-start | bytes 786440 | tf_op jit(solution)/shard_map/ppermute | solution.py:636
  158.9 11.8 %collective-permute-start.20 = (bf16[256,512]{1,0:T(8,128)(2,1)S(1)}, bf16[256,512]{1,0:T(8,128)(2,1)S(1)}, u32[]{:S(2)}, u32[]{:S(2)}) collective-permute-start(bf16[256,512]{1,0:T(8,128)(2,1)S(1)} %get-tuple-element.64), channel_id=1, source_target_pairs={{0,3},{3,0},{1,2},{2,1},{4,7},{7,4},{5,6},{6,5},{8,11},{11,8},{9,1... | collective-permute-start | bytes 786440 | tf_op jit(solution)/shard_map/ppermute | solution.py:640
  165.2 7.5 %collective-permute-start.21 = (bf16[128,512]{1,0:T(8,128)(2,1)S(1)}, bf16[128,512]{1,0:T(8,128)(2,1)S(1)}, u32[]{:S(2)}, u32[]{:S(2)}) collective-permute-start(bf16[128,512]{1,0:T(8,128)(2,1)S(1)} %get-tuple-element.66), channel_id=1, source_target_pairs={{0,3},{3,0},{1,2},{2,1},{4,7},{7,4},{5,6},{6,5},{8,11},{11,8},{9,1... | collective-permute-start | bytes 393224 | tf_op jit(solution)/shard_map/ppermute | solution.py:640
  166.6 6.1 %collective-permute-start.22 = (bf16[128,512]{1,0:T(8,128)(2,1)S(1)}, bf16[128,512]{1,0:T(8,128)(2,1)S(1)}, u32[]{:S(2)}, u32[]{:S(2)}) collective-permute-start(bf16[128,512]{1,0:T(8,128)(2,1)S(1)} %get-tuple-element.67), channel_id=1, source_target_pairs={{0,1},{1,0},{2,3},{3,2},{4,5},{5,4},{6,7},{7,6},{8,9},{9,8},{10,11... | collective-permute-start | bytes 393224 | tf_op jit(solution)/shard_map/ppermute | solution.py:636
  170.8 6.2 %collective-permute-start.23 = (bf16[128,512]{1,0:T(8,128)(2,1)S(1)}, bf16[128,512]{1,0:T(8,128)(2,1)S(1)}, u32[]{:S(2)}, u32[]{:S(2)}) collective-permute-start(bf16[128,512]{1,0:T(8,128)(2,1)S(1)} %get-tuple-element.69), channel_id=1, source_target_pairs={{0,3},{3,0},{1,2},{2,1},{4,7},{7,4},{5,6},{6,5},{8,11},{11,8},{9,1... | collective-permute-start | bytes 393224 | tf_op jit(solution)/shard_map/ppermute | solution.py:640
  172.0 5.4 %collective-permute-start.24 = (bf16[128,512]{1,0:T(8,128)(2,1)S(1)}, bf16[128,512]{1,0:T(8,128)(2,1)S(1)}, u32[]{:S(2)}, u32[]{:S(2)}) collective-permute-start(bf16[128,512]{1,0:T(8,128)(2,1)S(1)} %get-tuple-element.70), channel_id=1, source_target_pairs={{0,1},{1,0},{2,3},{3,2},{4,5},{5,4},{6,7},{7,6},{8,9},{9,8},{10,11... | collective-permute-start | bytes 393224 | tf_op jit(solution)/shard_map/ppermute | solution.py:636
Sparse Core Ops, SparseCore 0:
  10.1 106.0 all-gather.1
